TPU v7x, 256 devices: a whole 4x4x8 slice. The times are simulated.
256 devices in a mesh: sp: 128 (over z, y, x), tp: 2 (over core).
Axes of the slice: x: 4, y: 4, z: 8, core: 2. Of those that a mesh axis runs over, the one named last changes fastest.
Arguments:
- block_input: bfloat16 [16384, 2048], P('sp'), may hold values from -6 to 6
- value_weight: bfloat16 [2048, 384], P(None, 'tp'), may hold values from -0.125 to 0.125
- query_pre: bfloat16 [16384, 384], P('sp', 'tp'), may hold values from -6 to 6
- forget_pre: bfloat16 [16384, 384], P('sp', 'tp'), may hold values from -5.5 to 5.5
- lower_bound: float32 [384], P('tp'), may hold values from 0.94 to 1, as said below
- out_grad: bfloat16 [16384, 384], P('sp', 'tp'), may hold values from -6 to 6
Outputs:
- grad_query_pre: bfloat16 [16384, 384], P('sp', 'tp')
- grad_forget_pre: bfloat16 [16384, 384], P('sp', 'tp')
- grad_block_input: bfloat16 [16384, 2048], P(('sp', 'tp'))
- grad_value_weight: float32 [2048, 384], P('sp', 'tp')
Inputs may be any that keep to these rules, and one draw needn't show every extreme that they name: `lower_bound`: each channel's floor is below 1 and at least 0.94.
All inputs are finite; a program needn't handle non-finite values.
Results may differ from a plain program's by a relative error of at most 0.009.
Values may be sent and summed in bfloat16 or wider, within the bound.
A program may use at most 64 MiB of HBM per device.

v0:
```python
import jax
import jax.numpy as jnp
from jax import lax
from jax.sharding import Mesh
from jax.sharding import PartitionSpec as P

HEAD = 64
BLOCK = 64
SP = ("sp_0", "sp_1", "sp_2")
SP_TP = ("sp_0", "sp_1", "sp_2", "tp")


def nothing_yet(array, identity):
    return jax.tree.map(
        lambda a, e: jnp.broadcast_to(jnp.asarray(e, a.dtype), a.shape), array, identity
    )


def all_in_one(array, axis):
    leaves = jax.tree.leaves(array)
    turns = sorted(range(len(leaves)), key=lambda k: -leaves[k].size)
    width = (1, *leaves[turns[0]].shape)[-1]
    lines = [
        jnp.pad(leaves[k].reshape(-1), (0, -leaves[k].size % width)).reshape(-1, width)
        for k in turns
    ]
    both, at, found = (lax.all_gather(jnp.concatenate(lines), axis), 0, {})
    for k, line in zip(turns, lines):
        section = both[:, at : at + len(line)].reshape(len(both), -1)
        found[k] = section[:, : leaves[k].size].reshape(-1, *leaves[k].shape)
        at += len(line)
    numbers = iter(range(len(leaves)))
    return jax.tree.map(lambda _: found[next(numbers)], array)


def entering(array, axes, combine, identity, reverse):
    before = start = nothing_yet(array, identity)
    running = array
    for axis in reversed(axes):
        size, position = (lax.axis_size(axis), lax.axis_index(axis))
        pieces = all_in_one(
            jax.tree.map(
                lambda part, kind: part.astype(kind), running, (jnp.bfloat16, jnp.bfloat16)
            ),
            axis,
        )
        inside, running = (start, start)
        for k in reversed(range(size)) if reverse else range(size):
            passed = k > position if reverse else k < position
            running = combine(
                running, jax.tree.map(lambda part, own: part[k].astype(own.dtype), pieces, array)
            )
            inside = jax.tree.map(lambda new, old: jnp.where(passed, new, old), running, inside)
        before = combine(inside, before)
    return before


def sum_by_axis(running, axes):
    for axis in axes:
        running = lax.psum_scatter(running, axis, scatter_dimension=0, tiled=True)
    return running


def split_up(array, dim, size):
    shape = array.shape
    parts = array.reshape(*shape[:dim], size, shape[dim] // size, *shape[dim + 1 :])
    return jnp.moveaxis(parts, dim, 0)


def summed_on_arrival(array, axis, dim):
    size = lax.axis_size(axis)
    parts = lax.all_to_all(split_up(array, dim, size), axis, 0, 0, tiled=True)
    return jnp.sum(parts.astype(jnp.float32), axis=0)


def combine(earlier, latter):
    return (earlier[0] * latter[0], latter[0][..., None] * earlier[1] + latter[1])


def blocked(array, head_count, block_count):
    return jnp.transpose(array.reshape(block_count, BLOCK, head_count, HEAD), (0, 2, 1, 3))


def unblocked(array):
    block_count, head_count = (array.shape[0], array.shape[1])
    return jnp.transpose(array, (0, 2, 1, 3)).reshape(block_count * BLOCK, head_count * HEAD)


def carry_step(carried, pieces):
    decay_b, update_b = pieces
    return (decay_b[..., None] * carried + update_b, carried)


def on_device(block_input, value_weight, query_pre, forget_pre, lower_bound, out_grad):
    token_count = block_input.shape[0]
    group_width = value_weight.shape[1]
    head_count = group_width // HEAD
    block_count = token_count // BLOCK
    value_rows = jnp.dot(block_input, value_weight, preferred_element_type=jnp.float32).astype(
        jnp.bfloat16
    )
    query_f = query_pre.astype(jnp.float32)
    forget_f = forget_pre.astype(jnp.float32)
    query_sig = jax.nn.sigmoid(query_f)
    query = query_f * query_sig
    forget_sig = jax.nn.sigmoid(forget_f)
    key_rate = (1.0 - lower_bound) * jax.nn.sigmoid(-forget_f)
    decay_log = jnp.log1p(-key_rate)
    query_b = blocked(query, head_count, block_count)
    key_b = blocked(key_rate, head_count, block_count)
    value_b = blocked(value_rows.astype(jnp.float32), head_count, block_count)
    decay_b = blocked(decay_log, head_count, block_count)
    grad_b = blocked(out_grad.astype(jnp.float32), head_count, block_count)
    cumulative = jnp.cumsum(decay_b, axis=2)
    closing = cumulative[:, :, -1:, :]
    growth = jnp.exp(cumulative)
    shrinking = jnp.exp(-cumulative)
    remaining = jnp.exp(closing - cumulative)
    query_dec = query_b * growth
    key_dec = key_b * shrinking
    key_end = key_b * remaining
    block_decay = jnp.exp(closing[:, :, 0, :])
    update = jnp.einsum("bhsd,bhsv->bhdv", key_end, value_b)
    reach = jnp.einsum("bhtd,bhtv->bhdv", query_dec, grad_b)
    empty = jnp.zeros((head_count, HEAD, HEAD), jnp.float32)
    unit = jnp.ones((head_count, HEAD), jnp.float32)
    dev_state, starts_local = lax.scan(carry_step, empty, (block_decay, update))
    dev_grad, ends_local = lax.scan(carry_step, empty, (block_decay, reach), reverse=True)
    dev_decay = jnp.prod(block_decay, axis=0)
    running = jnp.cumprod(block_decay, axis=0)
    before = jnp.concatenate([unit[None], running[:-1]], axis=0)
    backward = jnp.flip(jnp.cumprod(jnp.flip(block_decay, 0), axis=0), 0)
    after = jnp.concatenate([backward[1:], unit[None]], axis=0)
    incoming = entering((dev_decay, dev_state), SP, combine, (unit, empty), False)[1]
    outgoing = entering((dev_decay, dev_grad), SP, combine, (unit, empty), True)[1]
    starts = starts_local + before[..., None] * incoming[None]
    device_end = dev_decay[..., None] * incoming + dev_state
    ends = jnp.concatenate([starts[1:], device_end[None]], axis=0)
    end_grads = ends_local + after[..., None] * outgoing[None]
    causal = (jnp.arange(BLOCK)[:, None] >= jnp.arange(BLOCK)[None, :]).astype(jnp.float32)
    pairing = jnp.einsum("bhtv,bhsv->bhts", grad_b, value_b) * causal
    mixing = jnp.einsum("bhtd,bhsd->bhts", query_dec, key_dec) * causal
    grad_query = growth * (
        jnp.einsum("bhts,bhsd->bhtd", pairing, key_dec)
        + jnp.einsum("bhdv,bhtv->bhtd", starts, grad_b)
    )
    grad_key = shrinking * jnp.einsum("bhts,bhtd->bhsd", pairing, query_dec)
    grad_key = grad_key + remaining * jnp.einsum("bhdv,bhsv->bhsd", end_grads, value_b)
    grad_value = jnp.einsum("bhts,bhtv->bhsv", mixing, grad_b)
    grad_value = grad_value + jnp.einsum("bhsd,bhdv->bhsv", key_end, end_grads)
    boundary = jnp.sum(end_grads * ends, axis=3)
    is_last = (jnp.arange(BLOCK) == BLOCK - 1).astype(jnp.float32)
    grad_cum = (
        query_b * grad_query
        - key_b * grad_key
        + is_last[None, None, :, None] * boundary[:, :, None, :]
    )
    grad_decay = jnp.einsum("ut,bhud->bhtd", causal, grad_cum)
    grad_key_total = grad_key - grad_decay / (1.0 - key_b)
    grad_query_rows = unblocked(grad_query)
    grad_query_pre = grad_query_rows * (query_sig * (1.0 + query_f * (1.0 - query_sig)))
    grad_forget = -unblocked(grad_key_total) * key_rate * forget_sig
    value_grad = unblocked(grad_value).astype(jnp.bfloat16)
    weight_grad = sum_by_axis(
        lax.dot_general(
            block_input, value_grad, (((0,), (0,)), ((), ())), preferred_element_type=jnp.float32
        ),
        SP,
    )
    input_grad = summed_on_arrival(
        lax.dot_general(
            value_grad, value_weight, (((1,), (1,)), ((), ())), preferred_element_type=jnp.float32
        ).astype(jnp.bfloat16),
        "tp",
        0,
    )
    return (
        grad_query_pre.astype(jnp.bfloat16),
        grad_forget.astype(jnp.bfloat16),
        input_grad.astype(jnp.bfloat16),
        weight_grad,
    )


def solution(mesh):
    split = Mesh(mesh.devices.reshape(8, 4, 4, mesh.shape["tp"]), ("sp_0", "sp_1", "sp_2", "tp"))
    in_specs = (P(SP, None), P(None, "tp"), P(SP, "tp"), P(SP, "tp"), P("tp"), P(SP, "tp"))
    out_specs = (P(SP, "tp"), P(SP, "tp"), P(SP_TP, None), P(SP, "tp"))
    return jax.shard_map(
        on_device, mesh=split, in_specs=in_specs, out_specs=out_specs, check_vma=False
    )
```

profile of v0, /device:TPU:1, one launch (start us, length us, event | category | flops | bytes accessed | tf_op | source)
XLA Modules:
  0.0 266.4 jit_solution(7285885923874976526)
XLA Ops:
  7.3 0.8 broadcast_subtract_fusion
  8.1 0.9 fusion.20
  9.6 0.6 rev.5
  10.2 0.4 convolution_convert_fusion.1
  11.4 0.3 while.30
  11.9 10.3 %all-gather.6 = bf16[4,195,64]{1,2,0:T(8,128)(2,1)S(1)} all-gather(bf16[1,195,64]{1,2,0:T(8,128)(2,1)S(1)} %copy.169), channel_id=2, replica_groups=mesh['sp_0'=8,'sp_1'=4,'sp_2'=4,'tp'=2] {'sp_2'}, dimensions={0}, use_global_device_ids=true | all-gather | bytes 124800 | tf_op jit(solution)/shard_map/all_gather | solution.py:27
  23.7 9.6 %all-gather.7 = bf16[4,195,64]{1,2,0:T(8,128)(2,1)S(1)} all-gather(bf16[1,195,64]{1,2,0:T(8,128)(2,1)S(1)} %copy.178), channel_id=3, replica_groups=mesh['sp_0'=8,'sp_1'=4,'sp_2'=4,'tp'=2] {'sp_1'}, dimensions={0}, use_global_device_ids=true | all-gather | bytes 124800 | tf_op jit(solution)/shard_map/all_gather | solution.py:27
  34.6 0.6 fusion.129
  35.6 22.1 %all-gather.8 = bf16[8,195,64]{1,2,0:T(8,128)(2,1)S(1)} all-gather(bf16[1,195,64]{1,2,0:T(8,128)(2,1)S(1)} %copy.187), channel_id=4, replica_groups=mesh['sp_0'=8,'sp_1'=4,'sp_2'=4,'tp'=2] {'sp_0'}, dimensions={0}, use_global_device_ids=true | all-gather | bytes 224640 | tf_op jit(solution)/shard_map/all_gather | solution.py:27
  57.7 0.7 fusion.107
  58.5 0.9 reshape.938
  59.6 0.6 concatenate.27.clone
  60.6 0.6 copy.322
  61.2 1.4 copy.188
  62.7 1.4 copy.194
  64.1 1.4 copy.193
  65.5 1.4 copy.192
  66.9 0.7 copy.191
  68.7 2.0 add_bitcast_fusion
  71.3 0.7 convert_multiply_fusion
  72.3 0.3 fusion
  72.9 0.3 while.31
  73.6 9.1 %all-gather.9 = bf16[4,195,64]{1,2,0:T(8,128)(2,1)S(1)} all-gather(bf16[1,195,64]{1,2,0:T(8,128)(2,1)S(1)} %copy.210), channel_id=5, replica_groups=mesh['sp_0'=8,'sp_1'=4,'sp_2'=4,'tp'=2] {'sp_2'}, dimensions={0}, use_global_device_ids=true | all-gather | bytes 124800 | tf_op jit(solution)/shard_map/all_gather | solution.py:27
  84.3 9.1 %all-gather.10 = bf16[4,195,64]{1,2,0:T(8,128)(2,1)S(1)} all-gather(bf16[1,195,64]{1,2,0:T(8,128)(2,1)S(1)} %copy.219), channel_id=6, replica_groups=mesh['sp_0'=8,'sp_1'=4,'sp_2'=4,'tp'=2] {'sp_1'}, dimensions={0}, use_global_device_ids=true | all-gather | bytes 124800 | tf_op jit(solution)/shard_map/all_gather | solution.py:27
  93.6 0.6 reshape.1007
  94.4 0.7 reshape.1005
  95.1 0.6 reshape.1006
  95.8 0.6 mul.892
  96.9 1.3 fusion.133
  98.3 0.9 fusion.54
  99.2 0.7 copy.228
  99.9 19.1 %all-gather.11 = bf16[8,195,64]{1,2,0:T(8,128)(2,1)S(1)} all-gather(bf16[1,195,64]{1,2,0:T(8,128)(2,1)} %copy.228), channel_id=7, replica_groups=mesh['sp_0'=8,'sp_1'=4,'sp_2'=4,'tp'=2] {'sp_0'}, dimensions={0}, use_global_device_ids=true | all-gather | bytes 224640 | tf_op jit(solution)/shard_map/all_gather | solution.py:27
  119.0 0.7 convert_multiply_fusion.2
  119.7 0.8 fusion.100
  120.5 0.7 fusion.151
  121.2 1.3 reduce_window.15
  122.4 0.8 broadcast_select_fusion
  123.2 1.4 copy.329
  124.6 1.4 copy.229
  126.0 1.4 copy.235
  127.4 1.4 copy.234
  128.8 1.4 copy.233
  130.2 1.4 copy.232
  131.7 1.4 copy.231
  133.1 1.4 copy.230
  134.5 1.5 copy.308
  136.0 1.5 copy.313
  137.4 1.5 copy.312
  138.9 1.5 copy.311
  140.4 1.5 copy.310
  141.9 1.5 copy.309
  143.3 0.7 copy.307
  144.1 0.7 copy.314
  144.8 1.6 fusion.34
  146.9 1.5 convolution_bitcast_fusion
  148.5 1.1 convolution_convert_fusion
  149.6 28.1 %all-to-all-start = ((bf16[2,64,2048]{2,1,0:T(8,128)(2,1)}), bf16[2,64,2048]{2,1,0:T(8,128)(2,1)S(1)}, u32[]{:S(2)}, u32[]{:S(2)}) async-start(bf16[2,64,2048]{2,1,0:T(8,128)(2,1)} %bitcast.105), calls=%async_computation | async-start | bytes 1048576 | tf_op jit(solution)/shard_map/all_to_all | solution.py:72
  178.1 29.1 %reduce-scatter.8.cloned.1.call-done = f32[256,192]{0,1:T(8,128)} async-done(((f32[2048,192]{0,1:T(8,128)}), f32[256,192]{0,1:T(8,128)}) %reduce-scatter.8.cloned.1.call-update) | async-done | bytes 196624 | tf_op jit(solution)/shard_map/reduce_scatter | solution.py:60
  207.1 1.8 copy.261
  209.2 0.3 fusion.4
  209.8 24.1 %reduce-scatter.10.cloned.1.call-done = f32[64,192]{1,0:T(8,128)} async-done(((f32[256,192]{1,0:T(8,128)}), f32[64,192]{1,0:T(8,128)}) %reduce-scatter.10.cloned.1.call-update) | async-done | bytes 49168
  233.9 0.7 fusion.87
  234.7 0.8 reduce_sum.22
  235.5 24.3 %reduce-scatter.12.cloned.1.call-done = f32[16,192]{1,0:T(8,128)} async-done(((f32[64,192]{1,0:T(8,128)}), f32[16,192]{1,0:T(8,128)}) %reduce-scatter.12.cloned.1.call-update) | async-done | bytes 12304
  (193 shorter events, 12.2 us)
Async XLA Ops:
  7.2 3.0 %copy-start = (bf16[2048,192]{0,1:T(8,128)(2,1)S(1)}, bf16[2048,192]{0,1:T(8,128)(2,1)}, u32[]{:S(2)}) copy-start(bf16[2048,192]{0,1:T(8,128)(2,1)} %param.11) | copy-start | bytes 2359300
  7.2 3.0 %copy-start.1 = (bf16[128,2048]{1,0:T(8,128)(2,1)S(1)}, bf16[128,2048]{1,0:T(8,128)(2,1)}, u32[]{:S(2)}) copy-start(bf16[128,2048]{1,0:T(8,128)(2,1)} %param.10) | copy-start | bytes 1572868
  7.2 200.0 %reduce-scatter.8.cloned.1.call-start = ((), (), s32[]{:S(2)}) async-start(), calls=%async_computation.4 | async-start | bytes 1769472 | tf_op jit(solution)/shard_map/reduce_scatter | solution.py:60
  8.1 0.9 copy-start.19
  9.6 1.8 copy-start.14
  11.1 0.6 copy-start.17
  22.7 34.9 %copy-start.5 = (f32[1,3,64]{2,1,0:T(4,128)}, f32[1,3,64]{2,1,0:T(4,128)S(1)}, u32[]{:S(2)}) copy-start(f32[1,3,64]{2,1,0:T(4,128)S(1)} %copy.317) | copy-start | bytes 2308
  33.5 2.0 copy-start.8
  33.8 23.9 %copy-start.9 = (f32[1,3,64]{2,1,0:T(4,128)}, f32[1,3,64]{2,1,0:T(4,128)S(1)}, u32[]{:S(2)}) copy-start(f32[1,3,64]{2,1,0:T(4,128)S(1)} %copy.320) | copy-start | bytes 2308
  33.9 23.7 %copy-start.10 = (f32[1,3,64]{2,1,0:T(4,128)}, f32[1,3,64]{2,1,0:T(4,128)S(1)}, u32[]{:S(2)}) copy-start(f32[1,3,64]{2,1,0:T(4,128)S(1)} %copy.319) | copy-start | bytes 2308
  67.5 3.2 %copy-start.15 = (f32[2,3,64]{2,1,0:T(4,128)S(1)}, f32[2,3,64]{2,1,0:T(4,128)}, u32[]{:S(2)}) copy-start(f32[2,3,64]{2,1,0:T(4,128)} %concatenate.27.clone) | copy-start | bytes 4612
  68.6 2.7 copy-start.7
  72.8 0.6 copy-start.18
  83.0 0.9 copy-start.16
  83.3 37.9 %copy-start.6 = (f32[1,3,64]{2,1,0:T(4,128)}, f32[1,3,64]{2,1,0:T(4,128)S(1)}, u32[]{:S(2)}) copy-start(f32[1,3,64]{2,1,0:T(4,128)S(1)} %copy.323) | copy-start | bytes 2308
  93.6 3.2 %copy-start.11 = (f32[1,3,64]{2,1,0:T(4,128)}, f32[1,3,64]{2,1,0:T(4,128)S(1)}, u32[]{:S(2)}) copy-start(f32[1,3,64]{2,1,0:T(4,128)S(1)} %copy.326) | copy-start | bytes 2308
  93.6 3.1 %copy-start.21 = (bf16[1,3,64]{2,1,0:T(4,128)(2,1)}, bf16[1,3,64]{2,1,0:T(4,128)(2,1)S(1)}, u32[]{:S(2)}) copy-start(bf16[1,3,64]{2,1,0:T(4,128)(2,1)S(1)} %copy.298) | copy-start | bytes 1156
  94.4 2.4 copy-start.12
  95.1 1.7 copy-start.13
  96.9 47.9 %copy-start.2 = (bf16[1,192,64]{2,1,0:T(8,128)(2,1)}, bf16[1,192,64]{2,1,0:T(8,128)(2,1)S(1)}, u32[]{:S(2)}) copy-start(bf16[1,192,64]{2,1,0:T(8,128)(2,1)S(1)} %copy.305) | copy-start | bytes 73732
  149.6 59.4 %copy-start.3 = (f32[1,3,64,64]{3,2,1,0:T(8,128)S(1)}, f32[1,3,64,64]{3,2,1,0:T(8,128)}, u32[]{:S(2)}) copy-start(f32[1,3,64,64]{3,2,1,0:T(8,128)} %get-tuple-element.242) | copy-start | bytes 147460
  149.6 85.1 %all-to-all-start = ((bf16[2,64,2048]{2,1,0:T(8,128)(2,1)}), bf16[2,64,2048]{2,1,0:T(8,128)(2,1)S(1)}, u32[]{:S(2)}, u32[]{:S(2)}) async-start(bf16[2,64,2048]{2,1,0:T(8,128)(2,1)} %bitcast.105), calls=%async_computation | async-start | bytes 1048576 | tf_op jit(solution)/shard_map/all_to_all | solution.py:72
  177.7 56.2 %reduce-scatter.10.cloned.1.call-start = ((), (), s32[]{:S(2)}) async-start(), calls=%async_computation.5 | async-start | bytes 327680
  208.9 25.0 %copy-start.4 = (bf16[128,192]{0,1:T(8,128)(2,1)S(1)}, bf16[128,192]{0,1:T(8,128)(2,1)}, u32[]{:S(2)}) copy-start(bf16[128,192]{0,1:T(8,128)(2,1)} %param.13) | copy-start | bytes 147460
  208.9 25.0 %copy-start.20 = (f32[192]{0:T(256)S(1)}, f32[192]{0:T(256)}, u32[]{:S(2)}) copy-start(f32[192]{0:T(256)} %copy-done.19) | copy-start | bytes 2308
  208.9 50.9 %reduce-scatter.12.cloned.1.call-start = ((), (), s32[]{:S(2)}) async-start(), calls=%async_computation.6 | async-start | bytes 81920
Sparse Core Ops, SparseCore 0:
  148.6 58.5 reduce-scatter.7
  210.2 23.6 reduce-scatter.9
  237.0 22.8 reduce-scatter.11
where the time goes:
time: 270 us; the launch traced here: 266 us
  blocking collectives  79.3 us (29%)
  waiting for transfers between devices  77.5 us (29%)
  local copies, waits for them, and re-layouts  44.4 us (16%)
  starting transfers between devices  28.1 us (10%)
  other arithmetic  16.9 us (6%)
  between operations  14.6 us (5%)
  matrix products  5.29 us (2%)
    all_gather x6, blocking collectives, all_in_one(): both, at, found = (lax.all_gather(jnp.concatenate(lines), axis), 0, {})  79.3 us
    unnamed x5, waiting for transfers between devices  48.5 us
    reduce_scatter x1, waiting for transfers between devices, sum_by_axis(): running = lax.psum_scatter(running, axis, scatter_dimension=0, tiled=True)  29.1 us
    all_to_all x1, starting transfers between devices, summed_on_arrival(): parts = lax.all_to_all(split_up(array, dim, size), axis, 0, 0, tiled=True)  28.1 us
    unnamed x103, local copies, waits for them, and re-layouts  19.5 us
    convert_element_type x26, local copies, waits for them, and re-layouts, entering(): part[k].astype(own.dtype)  19 us
  transfers between devices with their start and end apart: 4, of which 3 were waited for; matrix products, arithmetic and copies ran while one was open for 2% of the time, Pallas kernels for 0%

commit v1 on v0

v1 whole, which is shorter than its diff:
```python
import functools

import jax
import jax.numpy as jnp
from jax import lax
from jax.experimental import pallas as pl
from jax.experimental.pallas import tpu as pltpu
from jax.sharding import Mesh
from jax.sharding import PartitionSpec as P

HEAD = 64
SP = ("sp_0", "sp_1", "sp_2")
SP_TP = ("sp_0", "sp_1", "sp_2", "tp")
F32, BF16 = jnp.float32, jnp.bfloat16
LOGICAL = pl.DeviceIdType.MESH


def nn(a, b):
    return lax.dot_general(a, b, (((1,), (0,)), ((), ())), preferred_element_type=F32)


def nt(a, b):
    return lax.dot_general(a, b, (((1,), (1,)), ((), ())), preferred_element_type=F32)


def tn(a, b):
    return lax.dot_general(a, b, (((0,), (0,)), ((), ())), preferred_element_type=F32)


def exact_sum(ones, values):
    high = values.astype(BF16)
    low = (values - high.astype(F32)).astype(BF16)
    return nn(ones, high) + nn(ones, low)


def rcopy(src, dst, send, recv, device):
    return pltpu.make_async_remote_copy(
        src_ref=src, dst_ref=dst, send_sem=send, recv_sem=recv, device_id=device, device_id_type=LOGICAL
    )


def kernel(
    nz, ny, nx,
    x_hbm, w_hbm, q_hbm, f_hbm, go_hbm, lb_ref,
    gq_out, gf_out, gx_out, gw_out,
    x_v, w_v, q_v, f_v, go_v,
    s_send, e_send, s_buf, e_buf, l_buf, fl_buf, t_send, ft_send, t_buf, ft_buf, o_send, p_buf,
    xt, xtl, vg_v, vgl, ig, ig_recv, gx_v, acc, y_send, y_recv, w2, z_send, z_recv,
    gq_v, gf_v, gw_v,
    lsem, s_ss, s_rs, e_ss, e_rs, t_ss, t_rs, ft_ss, ft_rs, p_ss, p_rs,
    xt_ss, xt_rs, vg_ss, vg_rs, y_ss, y_rs, z_ss, z_rs, ig_ss, ig_rs,
):
    pln = ny * nx
    tok, d_model = x_v.shape
    ch = w_v.shape[1]
    heads = ch // HEAD
    z, y, x, c = (lax.axis_index(a) for a in SP_TP)
    me = y * nx + x
    back = (me * 2) // pln

    def plane(i):
        return (z, i // nx, lax.rem(i, nx), c)

    loads = [
        pltpu.make_async_copy(src, dst, lsem.at[k])
        for k, (src, dst) in enumerate(
            ((f_hbm, f_v), (q_hbm, q_v), (go_hbm, go_v), (x_hbm, x_v), (w_hbm, w_v))
        )
    ]
    for copy in loads:
        copy.start()

    barrier = pltpu.get_barrier_semaphore()
    for k in range(1, pln):
        pl.semaphore_signal(barrier, inc=1, device_id=plane(lax.rem(me + k, pln)), device_id_type=LOGICAL)
    for k in range(1, nz):
        pl.semaphore_signal(barrier, inc=1, device_id=(lax.rem(z + k, nz), y, x, c), device_id_type=LOGICAL)
    pl.semaphore_signal(barrier, inc=1, device_id=(z, y, x, 1 - c), device_id_type=LOGICAL)

    lane = lax.broadcasted_iota(jnp.int32, (1, ch), 1)
    mf = [jnp.where((lane >= HEAD * h) & (lane < HEAD * (h + 1)), 1.0, 0.0).astype(F32) for h in range(heads)]
    mb = [m.astype(BF16) for m in mf]
    row = lax.broadcasted_iota(jnp.int32, (tok, tok), 0)
    col = lax.broadcasted_iota(jnp.int32, (tok, tok), 1)
    lower, upper = row >= col, col >= row
    lower_ones = jnp.where(lower, 1.0, 0.0).astype(BF16)
    upper_ones = jnp.where(upper, 1.0, 0.0).astype(BF16)

    def stacked(a):
        return jnp.concatenate([a * m for m in mb], axis=0)

    def folded(full):
        out = full[:HEAD] * mf[0]
        for h in range(1, heads):
            out = out + full[HEAD * h : HEAD * (h + 1)] * mf[h]
        return out

    loads[0].wait()
    f = f_v[...].astype(F32)
    f_neg = 1.0 / (1.0 + jnp.exp(f))
    f_sig = 1.0 / (1.0 + jnp.exp(-f))
    k_rate = (1.0 - lb_ref[...]) * f_neg
    cum = exact_sum(lower_ones, jnp.log1p(-k_rate))
    closing = cum[tok - 1 : tok, :]
    growth = jnp.exp(cum)
    shrink = jnp.exp(-cum)
    remain = jnp.exp(closing - cum)
    total = jnp.exp(closing)
    e_send[...] = total
    k_dec = (k_rate * shrink).astype(BF16)
    k_end = (k_rate * remain).astype(BF16)
    loads[1].wait()
    q = q_v[...].astype(F32)
    q_sig = 1.0 / (1.0 + jnp.exp(-q))
    query = q * q_sig
    q_dec = (query * growth).astype(BF16)
    loads[2].wait()
    go = go_v[...]
    reach = folded(tn(go, q_dec))
    loads[3].wait()
    loads[4].wait()
    v = nn(x_v[...], w_v[...]).astype(BF16)
    update = folded(tn(v, k_end))
    s_send[...] = jnp.concatenate([update, reach], axis=0).reshape(s_send.shape)

    pl.semaphore_wait(barrier, pln + nz - 1)
    sends = []
    for k in range(1, pln):
        to = lax.rem(me + k, pln)
        sends.append(rcopy(e_send, e_buf.at[me], e_ss.at[k], e_rs.at[me], plane(to)))
        sends.append(rcopy(s_send.at[to], s_buf.at[me], s_ss.at[k], s_rs.at[me], plane(to)))
        sends[-2].start()
        sends[-1].start()
    s_buf[me] = s_send[me]
    e_buf[me] = e_send[...]

    rows = d_model // (nz * ny * nx)
    per = tok // rows
    for b in range(d_model // tok):
        turned = x_v[:, tok * b : tok * (b + 1)].T
        for g in range(per):
            at = b * per + g
            zz, yy, xx = at // pln, (at // nx) % ny, at % nx
            xt[xx, pl.ds((yy * nz + zz) * rows, rows), :] = turned[rows * g : rows * (g + 1)]
    for k in range(1, nx):
        to = lax.rem(x + k, nx)
        copy = rcopy(xt.at[to], xtl.at[x], xt_ss.at[k], xt_rs.at[x], (z, y, to, c))
        copy.start()
        sends.append(copy)

    go_st, v_st, qd_st, kd_st = stacked(go), stacked(v), stacked(q_dec), stacked(k_dec)

    def beside(full, keep):
        return jnp.concatenate(
            [jnp.where(keep, full[tok * h : tok * (h + 1)], 0.0).astype(BF16) for h in range(heads)], axis=1
        )

    gv_own = nn(beside(nt(kd_st, q_dec), upper), go_st)

    for k in range(1, pln):
        frm = lax.rem(me + k, pln)
        rcopy(e_send, e_buf.at[frm], e_ss.at[k], e_rs.at[frm], plane(frm)).wait_recv()
        rcopy(s_send.at[0], s_buf.at[frm], s_ss.at[k], s_rs.at[frm], plane(frm)).wait_recv()
    held = jnp.zeros(t_send.shape, F32)
    factor = jnp.ones((1, ch), F32)
    for o in range(pln):
        it = o + back * (pln - 1 - 2 * o)
        l_buf[it] = held
        fl_buf[it] = factor
        decay = e_buf[it]
        held = decay * held + s_buf[it]
        factor = decay * factor
    t_send[...] = held
    ft_send[...] = factor

    z_order = z + back * (nz - 1 - 2 * z)

    def z_sends(k):
        at = z_order + k
        to = at + back * (nz - 1 - 2 * at)
        return (
            rcopy(ft_send, ft_buf.at[z], ft_ss.at[k], ft_rs.at[z], (to, y, x, c)),
            rcopy(t_send, t_buf.at[z], t_ss.at[k], t_rs.at[z], (to, y, x, c)),
        )

    for k in range(1, nz):

        @pl.when(z_order + k < nz)
        def _():
            for copy in z_sends(k):
                copy.start()

    gq_own = nn(beside(nt(go_st, v), lower), kd_st)
    gk_own = nn(beside(nt(v_st, go), upper), qd_st)

    def arriving(o, carried):
        frm = o + back * (nz - 1 - 2 * o)
        rcopy(ft_send, ft_buf.at[frm], ft_ss.at[0], ft_rs.at[frm], (z, y, x, c)).wait_recv()
        rcopy(t_send, t_buf.at[frm], t_ss.at[0], t_rs.at[frm], (z, y, x, c)).wait_recv()
        return ft_buf[frm] * carried + t_buf[frm]

    carried = lax.fori_loop(0, z_order, arriving, jnp.zeros(t_send.shape, F32))

    o_send[...] = l_buf[...] + fl_buf[...] * carried[None]
    for k in range(1, pln):
        to = lax.rem(me + k, pln)
        copy = rcopy(o_send.at[to], p_buf.at[me], p_ss.at[k], p_rs.at[me], plane(to))
        copy.start()
        sends.append(copy)
    p_buf[me] = o_send[me]
    for k in range(1, pln):
        frm = lax.rem(me + k, pln)
        rcopy(o_send.at[0], p_buf.at[frm], p_ss.at[k], p_rs.at[frm], plane(frm)).wait_recv()
    carries = p_buf[...].reshape(2 * HEAD, ch)
    state, grad = carries[:HEAD], carries[HEAD:]
    bd_state = jnp.concatenate([(state * m).astype(BF16) for m in mf], axis=0)
    bd_grad = jnp.concatenate([(grad * m).astype(BF16) for m in mf], axis=0)

    value_grad = (gv_own + nt(k_end, bd_grad)).astype(BF16)
    vg_v[...] = value_grad
    for k in range(1, nx):
        to = lax.rem(x + k, nx)
        copy = rcopy(vg_v, vgl.at[x], vg_ss.at[k], vg_rs.at[x], (z, y, to, c))
        copy.start()
        sends.append(copy)

    width = 512 if d_model % 512 == 0 else d_model
    for j in range(d_model // width):
        cols = pl.ds(j * width, width)
        ig[:, :, cols] = nt(value_grad, w_v[cols, :]).astype(BF16).reshape(2, tok // 2, width)
    ig_copy = rcopy(ig.at[1 - c], ig_recv, ig_ss, ig_rs, (z, y, x, 1 - c))
    ig_copy.start()

    total_w = nn(xt[x], value_grad)
    for k in range(1, nx):
        frm = lax.rem(x + k, nx)
        rcopy(xt.at[0], xtl.at[frm], xt_ss.at[k], xt_rs.at[frm], (z, y, frm, c)).wait_recv()
        rcopy(vg_v, vgl.at[frm], vg_ss.at[k], vg_rs.at[frm], (z, y, frm, c)).wait_recv()
        total_w = total_w + nn(xtl[frm], vgl[frm])
    acc[...] = total_w.reshape(acc.shape)
    y_send[...] = total_w.astype(BF16).reshape(y_send.shape)
    for k in range(1, ny):
        to = lax.rem(y + k, ny)
        copy = rcopy(y_send.at[to], y_recv.at[y], y_ss.at[k], y_rs.at[y], (z, to, x, c))
        copy.start()
        sends.append(copy)

    g_query = growth * (gq_own + nn(go, bd_state))
    g_key = shrink * gk_own + remain * nn(v, bd_grad)
    gq_v[...] = (g_query * (q_sig * (1.0 + q * (1.0 - q_sig)))).astype(BF16)
    out_q = pltpu.make_async_copy(gq_v, gq_out, lsem.at[0])
    out_q.start()
    boundary = jnp.sum(grad * (total * state + update), axis=0, keepdims=True)
    g_decay = exact_sum(upper_ones, query * g_query - k_rate * g_key) + boundary
    gf_v[...] = ((g_decay / (1.0 - k_rate) - g_key) * k_rate * f_sig).astype(BF16)
    out_f = pltpu.make_async_copy(gf_v, gf_out, lsem.at[1])
    out_f.start()

    w_sum = acc[y]
    for k in range(1, ny):
        frm = lax.rem(y + k, ny)
        rcopy(y_send.at[0], y_recv.at[frm], y_ss.at[k], y_rs.at[frm], (z, frm, x, c)).wait_recv()
        w_sum = w_sum + y_recv[frm].astype(F32)
    w2[...] = w_sum.reshape(w2.shape)
    z_send[...] = w_sum.astype(BF16).reshape(z_send.shape)
    for k in range(1, nz):
        to = lax.rem(z + k, nz)
        copy = rcopy(z_send.at[to], z_recv.at[z], z_ss.at[k], z_rs.at[z], (to, y, x, c))
        copy.start()
        sends.append(copy)

    ig_copy.wait_recv()
    gx_v[...] = (ig[c].astype(F32) + ig_recv[...].astype(F32)).astype(BF16)
    out_x = pltpu.make_async_copy(gx_v, gx_out, lsem.at[2])
    out_x.start()

    w_last = w2[z]
    for k in range(1, nz):
        frm = lax.rem(z + k, nz)
        rcopy(z_send.at[0], z_recv.at[frm], z_ss.at[k], z_rs.at[frm], (frm, y, x, c)).wait_recv()
        w_last = w_last + z_recv[frm].astype(F32)
    gw_v[...] = w_last
    out_w = pltpu.make_async_copy(gw_v, gw_out, lsem.at[3])
    out_w.start()

    for copy in sends:
        copy.wait_send()
    ig_copy.wait_send()
    for k in range(1, nz):

        @pl.when(z_order + k < nz)
        def _():
            for copy in z_sends(k):
                copy.wait_send()

    for copy in (out_q, out_f, out_x, out_w):
        copy.wait()


def on_device(nz, ny, nx, block_input, value_weight, query_pre, forget_pre, lower_bound, out_grad):
    tok, d_model = block_input.shape
    ch = value_weight.shape[1]
    pln = ny * nx
    piece = 2 * HEAD // pln
    rows = d_model // (nz * pln)
    vm, dma = pltpu.VMEM, pltpu.SemaphoreType.DMA
    scratch = [
        vm((tok, d_model), BF16), vm((d_model, ch), BF16),
        vm((tok, ch), BF16), vm((tok, ch), BF16), vm((tok, ch), BF16),
        vm((pln, piece, ch), F32), vm((1, ch), F32),
        vm((pln, piece, ch), F32), vm((pln, 1, ch), F32),
        vm((pln, piece, ch), F32), vm((pln, 1, ch), F32),
        vm((piece, ch), F32), vm((1, ch), F32),
        vm((nz, piece, ch), F32), vm((nz, 1, ch), F32),
        vm((pln, piece, ch), F32), vm((pln, piece, ch), F32),
        vm((nx, d_model // nx, tok), BF16), vm((nx, d_model // nx, tok), BF16),
        vm((tok, ch), BF16), vm((nx, tok, ch), BF16),
        vm((2, tok // 2, d_model), BF16), vm((tok // 2, d_model), BF16), vm((tok // 2, d_model), BF16),
        vm((ny, nz * rows, ch), F32), vm((ny, nz * rows, ch), BF16), vm((ny, nz * rows, ch), BF16),
        vm((nz, rows, ch), F32), vm((nz, rows, ch), BF16), vm((nz, rows, ch), BF16),
        vm((tok, ch), BF16), vm((tok, ch), BF16), vm((rows, ch), F32),
        dma((5,)),
        dma((pln,)), dma((pln,)), dma((pln,)), dma((pln,)),
        dma((nz,)), dma((nz,)), dma((nz,)), dma((nz,)),
        dma((pln,)), dma((pln,)),
        dma((nx,)), dma((nx,)), dma((nx,)), dma((nx,)),
        dma((ny,)), dma((ny,)), dma((nz,)), dma((nz,)),
        dma, dma,
    ]
    hbm = pl.BlockSpec(memory_space=pl.ANY)
    return pl.pallas_call(
        functools.partial(kernel, nz, ny, nx),
        out_shape=(
            jax.ShapeDtypeStruct((tok, ch), BF16),
            jax.ShapeDtypeStruct((tok, ch), BF16),
            jax.ShapeDtypeStruct((tok // 2, d_model), BF16),
            jax.ShapeDtypeStruct((rows, ch), F32),
        ),
        in_specs=[hbm] * 5 + [pl.BlockSpec(memory_space=pltpu.VMEM)],
        out_specs=(hbm,) * 4,
        scratch_shapes=scratch,
        compiler_params=pltpu.CompilerParams(collective_id=0, has_side_effects=True),
    )(block_input, value_weight, query_pre, forget_pre, out_grad, lower_bound.reshape(1, ch))


def on_mesh(devices):
    nz, ny, nx = devices.shape[:3]
    split = Mesh(devices, SP_TP)
    in_specs = (P(SP, None), P(None, "tp"), P(SP, "tp"), P(SP, "tp"), P("tp"), P(SP, "tp"))
    out_specs = (P(SP, "tp"), P(SP, "tp"), P(SP_TP, None), P(SP, "tp"))
    return jax.shard_map(
        functools.partial(on_device, nz, ny, nx), mesh=split, in_specs=in_specs, out_specs=out_specs, check_vma=False
    )


def solution(mesh):
    return on_mesh(mesh.devices.reshape(8, 4, 4, mesh.shape["tp"]))
```

time: 270 us -> 53.7 us (0.20)
  the two profiles are of different devices: /device:TPU:1 before, /device:TPU:4 now
where the time goes in v1:
time: 53.7 us; the launch traced here: 53.4 us
  Pallas kernels  42.8 us (80%)
  local copies, waits for them, and re-layouts  9.91 us (18%)
  between operations  0.66 us (1%)
    pallas_call x1, Pallas kernels, on_device(): pl.pallas_call(functools.partial(kernel, nz, ny, nx), out_shape=(jax.Shap...  42.8 us
    unnamed x14, local copies, waits for them, and re-layouts  7.59 us
    pallas_call x2, local copies, waits for them, and re-layouts, on_device(): pl.pallas_call(functools.partial(kernel, nz, ny, nx), out_shape=(jax.Shap...  2.31 us

profile of v1, /device:TPU:4, one launch (start us, length us, event | category | flops | bytes accessed | tf_op | source)
XLA Modules:
  0.0 53.4 jit_solution(13699004305899680551)
XLA Ops:
  0.6 0.0 copy-start.1
  0.6 1.5 %copy.11.q_hbm = bf16[128,192]{1,0:T(8,128)(2,1)} copy(bf16[128,192]{0,1:T(8,128)(2,1)} %param.8) | data formatting | bytes 98304 | tf_op args[2]
  2.2 0.0 copy-done.1
  2.2 0.0 copy-start.2
  2.2 0.7 %copy.12.f_hbm = bf16[128,192]{1,0:T(8,128)(2,1)} copy(bf16[128,192]{0,1:T(8,128)(2,1)S(1)} %copy-done.1) | data formatting | bytes 98304 | tf_op args[3]
  2.9 0.1 copy-done.2
  3.0 0.7 %copy.13.go_hbm = bf16[128,192]{1,0:T(8,128)(2,1)} copy(bf16[128,192]{0,1:T(8,128)(2,1)S(1)} %copy-done.2) | data formatting | bytes 98304 | tf_op args[5]
  3.7 2.2 %copy.10.w_hbm = bf16[2048,192]{1,0:T(8,128)(2,1)} copy(bf16[2048,192]{0,1:T(8,128)(2,1)} %param.7) | data formatting | bytes 1572864 | tf_op args[1]
  5.9 42.8 %shard_map.93 = (bf16[128,192]{1,0:T(8,128)(2,1)}, bf16[128,192]{1,0:T(8,128)(2,1)}, bf16[64,2048]{1,0:T(8,128)(2,1)}, f32[16,192]{1,0:T(8,128)}) custom-call(bf16[128,2048]{1,0:T(8,128)(2,1)} %x_hbm.1, bf16[2048,192]{1,0:T(8,128)(2,1)} %copy.10.w_hbm, bf16[128,192]{1,0:T(8,128)(2,1)} %copy.11.q_hbm, bf16[128,192]{1,0:T(8,128)(2,1)} %copy.12.f_hbm, ...), custom_call_target="tpu_custom_call" | custom-call | tf_op jit(solution)/shard_map/pallas_call | solution.py:331
  48.7 0.0 copy-start
  48.7 1.6 %copy.14 = bf16[128,192]{0,1:T(8,128)(2,1)} copy(bf16[128,192]{1,0:T(8,128)(2,1)} %get-tuple-element.4) | data formatting | bytes 98304 | tf_op jit(solution)/shard_map/pallas_call | solution.py:331
  50.3 0.0 copy-done
  50.3 0.7 %copy.15 = bf16[128,192]{0,1:T(8,128)(2,1)} copy(bf16[128,192]{1,0:T(8,128)(2,1)S(1)} %copy-done) | data formatting | bytes 98304 | tf_op jit(solution)/shard_map/pallas_call | solution.py:331
  51.1 0.0 copy-start.3
  51.1 1.7 %copy.18 = bf16[64,2048]{1,0:T(8,128)(2,1)} copy(bf16[64,2048]{1,0:T(8,128)(2,1)} %get-tuple-element.14) | data formatting | bytes 524288
  52.7 0.0 copy-done.3
  52.7 0.6 %copy.19 = f32[16,192]{1,0:T(8,128)} copy(f32[16,192]{1,0:T(8,128)S(1)} %copy-done.3) | data formatting | bytes 24576
Async XLA Ops:
  0.6 1.6 %copy-start.1 = (bf16[128,192]{0,1:T(8,128)(2,1)S(1)}, bf16[128,192]{0,1:T(8,128)(2,1)}, u32[]{:S(2)}) copy-start(bf16[128,192]{0,1:T(8,128)(2,1)} %param.9) | copy-start | bytes 147460
  2.2 0.8 %copy-start.2 = (bf16[128,192]{0,1:T(8,128)(2,1)S(1)}, bf16[128,192]{0,1:T(8,128)(2,1)}, u32[]{:S(2)}) copy-start(bf16[128,192]{0,1:T(8,128)(2,1)} %param.11) | copy-start | bytes 147460
  48.7 1.6 %copy-start = (bf16[128,192]{1,0:T(8,128)(2,1)S(1)}, bf16[128,192]{1,0:T(8,128)(2,1)}, u32[]{:S(2)}) copy-start(bf16[128,192]{1,0:T(8,128)(2,1)} %get-tuple-element.5) | copy-start | bytes 147460
  51.1 1.7 %copy-start.3 = (f32[16,192]{1,0:T(8,128)S(1)}, f32[16,192]{1,0:T(8,128)}, u32[]{:S(2)}) copy-start(f32[16,192]{1,0:T(8,128)} %get-tuple-element.15) | copy-start | bytes 36868

commit v2 on v1

v2 whole, which is shorter than its diff:
```python
import functools

import jax
import jax.numpy as jnp
from jax import lax
from jax.experimental import pallas as pl
from jax.experimental.pallas import tpu as pltpu
from jax.sharding import Mesh
from jax.sharding import PartitionSpec as P

HEAD = 64
SP = ("sp_0", "sp_1", "sp_2")
SP_TP = ("sp_0", "sp_1", "sp_2", "tp")
F32, BF16 = jnp.float32, jnp.bfloat16
LOGICAL = pl.DeviceIdType.MESH


def nn(a, b):
    return lax.dot_general(a, b, (((1,), (0,)), ((), ())), preferred_element_type=F32)


def nt(a, b):
    return lax.dot_general(a, b, (((1,), (1,)), ((), ())), preferred_element_type=F32)


def tn(a, b):
    return lax.dot_general(a, b, (((0,), (0,)), ((), ())), preferred_element_type=F32)


def rcopy(src, dst, send, recv, device):
    return pltpu.make_async_remote_copy(
        src_ref=src, dst_ref=dst, send_sem=send, recv_sem=recv, device_id=device, device_id_type=LOGICAL
    )


def kernel(
    nz, ny, nx,
    x_hbm, w_hbm, q_hbm, f_hbm, go_hbm, lb_ref,
    gq_out, gf_out, gx_out, gw_out,
    x_v, w_v, q_v, f_v, go_v,
    s_send, e_send, s_buf, e_buf, l_buf, fl_buf, t_send, ft_send, t_buf, ft_buf, o_send, p_buf,
    xt, xtl, vg_v, vgl, ig, ig_recv, acc, y_send, y_recv, w2, z_send, z_recv,
    lsem, s_ss, s_rs, e_ss, e_rs, t_ss, t_rs, ft_ss, ft_rs, p_ss, p_rs,
    xt_ss, xt_rs, vg_ss, vg_rs, y_ss, y_rs, z_ss, z_rs, ig_ss, ig_rs,
):
    pln = ny * nx
    tok, d_model = x_v.shape
    ch = w_v.shape[0]
    heads = ch // HEAD
    z, y, x, c = (lax.axis_index(a) for a in SP_TP)
    me = y * nx + x
    back = (me * 2) // pln

    def plane(i):
        return (z, i // nx, lax.rem(i, nx), c)

    def head_of(a, h):
        return a[HEAD * h : HEAD * (h + 1)]

    def by_head(parts):
        return jnp.concatenate(list(parts), axis=0)

    scope = jax.named_scope
    with scope("loads_barrier"):
        loads = [
            pltpu.make_async_copy(src, dst, lsem.at[k])
            for k, (src, dst) in enumerate(
                ((f_hbm, f_v), (q_hbm, q_v), (go_hbm, go_v), (x_hbm, x_v), (w_hbm, w_v))
            )
        ]
        for copy in loads:
            copy.start()
        barrier = pltpu.get_barrier_semaphore()
        for k in range(1, pln):
            pl.semaphore_signal(barrier, inc=1, device_id=plane(lax.rem(me + k, pln)), device_id_type=LOGICAL)
        for k in range(1, nz):
            pl.semaphore_signal(barrier, inc=1, device_id=(lax.rem(z + k, nz), y, x, c), device_id_type=LOGICAL)
        pl.semaphore_signal(barrier, inc=1, device_id=(z, y, x, 1 - c), device_id_type=LOGICAL)

    lane = lax.broadcasted_iota(jnp.int32, (1, ch), 1)
    mf = [jnp.where((lane >= HEAD * h) & (lane < HEAD * (h + 1)), 1.0, 0.0).astype(F32) for h in range(heads)]
    row = lax.broadcasted_iota(jnp.int32, (tok, tok), 0)
    col = lax.broadcasted_iota(jnp.int32, (tok, tok), 1)
    lower, upper = row >= col, col >= row
    lower_ones = jnp.where(lower, 1.0, 0.0).astype(BF16)
    upper_ones = jnp.where(upper, 1.0, 0.0).astype(BF16)

    def folded(full):
        out = full[:HEAD] * mf[0]
        for h in range(1, heads):
            out = out + head_of(full, h) * mf[h]
        return out

    with scope("gates"):
        gap = jnp.broadcast_to(1.0 - lb_ref[...], (tok, ch)).T
        loads[0].wait()
        f = f_v[...].astype(F32)
        f_neg = 1.0 / (1.0 + jnp.exp(f))
        f_sig = 1.0 / (1.0 + jnp.exp(-f))
        k_rate = gap * f_neg
        logs = jnp.log1p(-k_rate)
        high = logs.astype(BF16)
        low = (logs - high.astype(F32)).astype(BF16)
        cum = nn(high, upper_ones) + nn(low, upper_ones)
        row_ones = jnp.ones((8, tok), BF16)
        total = jnp.exp((nt(row_ones, high) + nt(row_ones, low))[:1])
        closing = cum[:, tok - 1 : tok]
        growth = jnp.exp(cum)
        shrink = jnp.exp(-cum)
        remain = jnp.exp(closing - cum)
        e_send[...] = total
        k_dec = (k_rate * shrink).astype(BF16)
        k_end = (k_rate * remain).astype(BF16)
        loads[1].wait()
        q = q_v[...].astype(F32)
        q_sig = 1.0 / (1.0 + jnp.exp(-q))
        query = q * q_sig
        q_dec = (query * growth).astype(BF16)
        loads[2].wait()
        go = go_v[...]
        reach = folded(nt(go, q_dec))
    with scope("values"):
        loads[3].wait()
        loads[4].wait()
        v = nt(w_v[...], x_v[...]).astype(BF16)
        update = folded(nt(v, k_end))
        s_send[...] = jnp.concatenate([update, reach], axis=0).reshape(s_send.shape).astype(BF16)

    with scope("barrier_wait"):
        pl.semaphore_wait(barrier, pln + nz - 1)
    with scope("send1"):
        sends = []
        for k in range(1, pln):
            to = lax.rem(me + k, pln)
            sends.append(rcopy(e_send, e_buf.at[me], e_ss.at[k], e_rs.at[me], plane(to)))
            sends.append(rcopy(s_send.at[to], s_buf.at[me], s_ss.at[k], s_rs.at[me], plane(to)))
            sends[-2].start()
            sends[-1].start()
        s_buf[me] = s_send[me]
        e_buf[me] = e_send[...]

    with scope("turn"):
        rows = d_model // (nz * ny * nx)
        per = tok // rows
        for b in range(d_model // tok):
            turned = x_v[:, tok * b : tok * (b + 1)].T
            for g in range(per):
                at = b * per + g
                zz, yy, xx = at // pln, (at // nx) % ny, at % nx
                xt[xx, pl.ds((yy * nz + zz) * rows, rows), :] = turned[rows * g : rows * (g + 1)]
        for k in range(1, nx):
            to = lax.rem(x + k, nx)
            copy = rcopy(xt.at[to], xtl.at[x], xt_ss.at[k], xt_rs.at[x], (z, y, to, c))
            copy.start()
            sends.append(copy)

    with scope("pairs_value"):
        mixing = [jnp.where(lower, tn(head_of(q_dec, h), head_of(k_dec, h)), 0.0).astype(BF16) for h in range(heads)]
        gv_own = by_head(nn(head_of(go, h), mixing[h]) for h in range(heads))

    with scope("wait1"):
        for k in range(1, pln):
            frm = lax.rem(me + k, pln)
            rcopy(e_send, e_buf.at[frm], e_ss.at[k], e_rs.at[frm], plane(frm)).wait_recv()
            rcopy(s_send.at[0], s_buf.at[frm], s_ss.at[k], s_rs.at[frm], plane(frm)).wait_recv()
    with scope("scan1"):
        held = jnp.zeros(t_send.shape, F32)
        factor = jnp.ones((1, ch), F32)
        for o in range(pln):
            it = o + back * (pln - 1 - 2 * o)
            l_buf[it] = held
            fl_buf[it] = factor
            decay = e_buf[it]
            held = decay * held + s_buf[it].astype(F32)
            factor = decay * factor
        t_send[...] = held.astype(BF16)
        ft_send[...] = factor

    z_order = z + back * (nz - 1 - 2 * z)

    def z_sends(k):
        at = z_order + k
        to = at + back * (nz - 1 - 2 * at)
        return (
            rcopy(ft_send, ft_buf.at[z], ft_ss.at[k], ft_rs.at[z], (to, y, x, c)),
            rcopy(t_send, t_buf.at[z], t_ss.at[k], t_rs.at[z], (to, y, x, c)),
        )

    with scope("send2"):
        for k in range(1, nz):

            @pl.when(z_order + k < nz)
            def _():
                for copy in z_sends(k):
                    copy.start()

    with scope("pairs_query"):
        pairing = [jnp.where(upper, tn(head_of(v, h), head_of(go, h)), 0.0).astype(BF16) for h in range(heads)]
        gq_own = by_head(nn(head_of(k_dec, h), pairing[h]) for h in range(heads))
        gk_own = by_head(nt(head_of(q_dec, h), pairing[h]) for h in range(heads))

    def arriving(o, carried):
        frm = o + back * (nz - 1 - 2 * o)
        rcopy(ft_send, ft_buf.at[frm], ft_ss.at[0], ft_rs.at[frm], (z, y, x, c)).wait_recv()
        rcopy(t_send, t_buf.at[frm], t_ss.at[0], t_rs.at[frm], (z, y, x, c)).wait_recv()
        return ft_buf[frm] * carried + t_buf[frm].astype(F32)

    with scope("wait2"):
        carried = lax.fori_loop(0, z_order, arriving, jnp.zeros(t_send.shape, F32))

    with scope("send3"):
        o_send[...] = (l_buf[...] + fl_buf[...] * carried[None]).astype(BF16)
        for k in range(1, pln):
            to = lax.rem(me + k, pln)
            copy = rcopy(o_send.at[to], p_buf.at[me], p_ss.at[k], p_rs.at[me], plane(to))
            copy.start()
            sends.append(copy)
        p_buf[me] = o_send[me]
    with scope("wait3"):
        for k in range(1, pln):
            frm = lax.rem(me + k, pln)
            rcopy(o_send.at[0], p_buf.at[frm], p_ss.at[k], p_rs.at[frm], plane(frm)).wait_recv()
    with scope("value_grad"):
        carries = p_buf[...].astype(F32).reshape(2 * HEAD, ch)
        state, grad = carries[:HEAD], carries[HEAD:]
        bd_state = by_head((state * m).astype(BF16) for m in mf)
        bd_grad = by_head((grad * m).astype(BF16) for m in mf)
        value_grad = (gv_own + nn(bd_grad, k_end)).astype(BF16)
        vg_v[...] = value_grad
        for k in range(1, nx):
            to = lax.rem(x + k, nx)
            copy = rcopy(vg_v, vgl.at[x], vg_ss.at[k], vg_rs.at[x], (z, y, to, c))
            copy.start()
            sends.append(copy)

    with scope("input_grad"):
        width = 512 if d_model % 512 == 0 else d_model
        turned = value_grad.T
        for j in range(d_model // width):
            cols = pl.ds(j * width, width)
            ig[:, :, cols] = nn(turned, w_v[:, cols]).astype(BF16).reshape(2, tok // 2, width)
        ig_copy = rcopy(ig.at[1 - c], ig_recv, ig_ss, ig_rs, (z, y, x, 1 - c))
        ig_copy.start()

    with scope("weight_own"):
        total_w = nt(xt[x], value_grad)
    for k in range(1, nx):
        frm = lax.rem(x + k, nx)
        with scope(f"wait_vg{k}"):
            rcopy(xt.at[0], xtl.at[frm], xt_ss.at[k], xt_rs.at[frm], (z, y, frm, c)).wait_recv()
            rcopy(vg_v, vgl.at[frm], vg_ss.at[k], vg_rs.at[frm], (z, y, frm, c)).wait_recv()
        total_w = total_w + nt(xtl[frm], vgl[frm])
    with scope("send_y"):
        acc[...] = total_w.reshape(acc.shape)
        y_send[...] = total_w.astype(BF16).reshape(y_send.shape)
        for k in range(1, ny):
            to = lax.rem(y + k, ny)
            copy = rcopy(y_send.at[to], y_recv.at[y], y_ss.at[k], y_rs.at[y], (z, to, x, c))
            copy.start()
            sends.append(copy)

    with scope("query_forget"):
        g_query = growth * (gq_own + tn(bd_state, go))
        g_key = shrink * gk_own + remain * tn(bd_grad, v)
        gq_out[...] = (g_query * (q_sig * (1.0 + q * (1.0 - q_sig)))).astype(BF16)
        ends = grad * (total * state + update)
        ends_high = ends.astype(BF16)
        ends_low = (ends - ends_high.astype(F32)).astype(BF16)
        tall_ones = jnp.ones((HEAD, tok), BF16)
        boundary = tn(ends_high, tall_ones) + tn(ends_low, tall_ones)
        flow = query * g_query - k_rate * g_key
        flow_high = flow.astype(BF16)
        flow_low = (flow - flow_high.astype(F32)).astype(BF16)
        g_decay = nn(flow_high, lower_ones) + nn(flow_low, lower_ones) + boundary
        gf_out[...] = ((g_decay / (1.0 - k_rate) - g_key) * k_rate * f_sig).astype(BF16)

    w_sum = acc[y]
    with scope("wait_y"):
        for k in range(1, ny):
            frm = lax.rem(y + k, ny)
            rcopy(y_send.at[0], y_recv.at[frm], y_ss.at[k], y_rs.at[frm], (z, frm, x, c)).wait_recv()
            w_sum = w_sum + y_recv[frm].astype(F32)
    with scope("send_z"):
        w2[...] = w_sum.reshape(w2.shape)
        z_send[...] = w_sum.astype(BF16).reshape(z_send.shape)
        for k in range(1, nz):
            to = lax.rem(z + k, nz)
            copy = rcopy(z_send.at[to], z_recv.at[z], z_ss.at[k], z_rs.at[z], (to, y, x, c))
            copy.start()
            sends.append(copy)
    with scope("input_sum"):
        ig_copy.wait_recv()
        gx_out[...] = (ig[c].astype(F32) + ig_recv[...].astype(F32)).astype(BF16)

    w_last = w2[z]
    with scope("wait_z"):
        for k in range(1, nz):
            frm = lax.rem(z + k, nz)
            rcopy(z_send.at[0], z_recv.at[frm], z_ss.at[k], z_rs.at[frm], (frm, y, x, c)).wait_recv()
            w_last = w_last + z_recv[frm].astype(F32)
        gw_out[...] = w_last

    with scope("drain"):
        for copy in sends:
            copy.wait_send()
        ig_copy.wait_send()
        for k in range(1, nz):

            @pl.when(z_order + k < nz)
            def _():
                for copy in z_sends(k):
                    copy.wait_send()


def on_device(nz, ny, nx, block_input, value_weight, query_pre, forget_pre, lower_bound, out_grad):
    tok, d_model = block_input.shape
    ch = value_weight.shape[1]
    pln = ny * nx
    piece = 2 * HEAD // pln
    rows = d_model // (nz * pln)
    vm, dma = pltpu.VMEM, pltpu.SemaphoreType.DMA
    scratch = [
        vm((tok, d_model), BF16), vm((ch, d_model), BF16),
        vm((ch, tok), BF16), vm((ch, tok), BF16), vm((ch, tok), BF16),
        vm((pln, piece, ch), BF16), vm((1, ch), F32),
        vm((pln, piece, ch), BF16), vm((pln, 1, ch), F32),
        vm((pln, piece, ch), F32), vm((pln, 1, ch), F32),
        vm((piece, ch), BF16), vm((1, ch), F32),
        vm((nz, piece, ch), BF16), vm((nz, 1, ch), F32),
        vm((pln, piece, ch), BF16), vm((pln, piece, ch), BF16),
        vm((nx, d_model // nx, tok), BF16), vm((nx, d_model // nx, tok), BF16),
        vm((ch, tok), BF16), vm((nx, ch, tok), BF16),
        vm((2, tok // 2, d_model), BF16), vm((tok // 2, d_model), BF16),
        vm((ny, nz * rows, ch), F32), vm((ny, nz * rows, ch), BF16), vm((ny, nz * rows, ch), BF16),
        vm((nz, rows, ch), F32), vm((nz, rows, ch), BF16), vm((nz, rows, ch), BF16),
        dma((5,)),
        dma((pln,)), dma((pln,)), dma((pln,)), dma((pln,)),
        dma((nz,)), dma((nz,)), dma((nz,)), dma((nz,)),
        dma((pln,)), dma((pln,)),
        dma((nx,)), dma((nx,)), dma((nx,)), dma((nx,)),
        dma((ny,)), dma((ny,)), dma((nz,)), dma((nz,)),
        dma, dma,
    ]
    hbm, near = pl.BlockSpec(memory_space=pl.ANY), pl.BlockSpec(memory_space=pltpu.VMEM)
    g_query, g_forget, g_input, g_weight = pl.pallas_call(
        functools.partial(kernel, nz, ny, nx),
        out_shape=(
            vm((ch, tok), BF16),
            vm((ch, tok), BF16),
            vm((tok // 2, d_model), BF16),
            vm((rows, ch), F32),
        ),
        in_specs=[hbm] * 5 + [near],
        out_specs=(near,) * 4,
        scratch_shapes=scratch,
        compiler_params=pltpu.CompilerParams(collective_id=0, has_side_effects=True),
    )(block_input, value_weight.T, query_pre.T, forget_pre.T, out_grad.T, lower_bound.reshape(1, ch))
    return g_query.T, g_forget.T, g_input, g_weight


def on_mesh(devices):
    nz, ny, nx = devices.shape[:3]
    split = Mesh(devices, SP_TP)
    in_specs = (P(SP, None), P(None, "tp"), P(SP, "tp"), P(SP, "tp"), P("tp"), P(SP, "tp"))
    out_specs = (P(SP, "tp"), P(SP, "tp"), P(SP_TP, None), P(SP, "tp"))
    return jax.shard_map(
        functools.partial(on_device, nz, ny, nx), mesh=split, in_specs=in_specs, out_specs=out_specs, check_vma=False
    )


def solution(mesh):
    return on_mesh(mesh.devices.reshape(8, 4, 4, mesh.shape["tp"]))
```

time: 53.7 us -> 44.4 us (0.83)
  the two profiles are of different devices: /device:TPU:4 before, /device:TPU:2 now
where the time goes in v2:
time: 44.4 us; the launch traced here: 44.2 us
  Pallas kernels  41 us (92%)
  local copies, waits for them, and re-layouts  2.55 us (6%)
  between operations  0.64 us (1%)
    pallas_call x1, Pallas kernels, on_device(): pl.pallas_call(functools.partial(kernel, nz, ny, nx), out_shape=(vm((ch,...  41 us
    unnamed x4, local copies, waits for them, and re-layouts  2.55 us

profile of v2, /device:TPU:2, one launch (start us, length us, event | category | flops | bytes accessed | tf_op | source)
XLA Modules:
  0.0 44.2 jit_solution(2371979094987071659)
XLA Ops:
  0.6 41.0 %shard_map.93 = (bf16[192,128]{1,0:T(8,128)(2,1)S(1)}, bf16[192,128]{1,0:T(8,128)(2,1)S(1)}, bf16[64,2048]{1,0:T(8,128)(2,1)S(1)}, f32[16,192]{1,0:T(8,128)S(1)}) custom-call(bf16[128,2048]{1,0:T(8,128)(2,1)} %x_hbm.1, bf16[192,2048]{1,0:T(8,128)(2,1)} %bitcast.9, bf16[192,128]{1,0:T(8,128)(2,1)} %bitcast.10, bf16[192,128]{1,0:T(8,128)(2,1)} %bitcast.11, ...), custom_call_target="tpu_custom_call" | custom-call | tf_op jit(solution)/shard_map/pallas_call | solution.py:345
  41.7 0.6 %copy.14 = bf16[128,192]{0,1:T(8,128)(2,1)} copy(bf16[128,192]{0,1:T(8,128)(2,1)S(1)} %bitcast.8) | data formatting | bytes 98304
  42.3 0.6 %copy.15 = bf16[128,192]{0,1:T(8,128)(2,1)} copy(bf16[128,192]{0,1:T(8,128)(2,1)S(1)} %bitcast.7) | data formatting | bytes 98304
  42.9 0.6 %copy.17 = f32[16,192]{1,0:T(8,128)} copy(f32[16,192]{1,0:T(8,128)S(1)} %get-tuple-element.15) | data formatting | bytes 24576
  43.5 0.7 %copy.16 = bf16[64,2048]{1,0:T(8,128)(2,1)} copy(bf16[64,2048]{1,0:T(8,128)(2,1)S(1)} %get-tuple-element.14) | data formatting | bytes 524288

commit v3 on v2

--- a/solution.py
+++ b/solution.py
@@ -35,9 +35,9 @@
 
 def kernel(
     nz, ny, nx,
-    x_hbm, w_hbm, q_hbm, f_hbm, go_hbm, lb_ref,
+    x_hbm, w_hbm, q_hbm, f_hbm, go_hbm, lb_hbm,
     gq_out, gf_out, gx_out, gw_out,
-    x_v, w_v, q_v, f_v, go_v,
+    x_v, w_v, q_v, f_v, go_v, lb_v,
     s_send, e_send, s_buf, e_buf, l_buf, fl_buf, t_send, ft_send, t_buf, ft_buf, o_send, p_buf,
     xt, xtl, vg_v, vgl, ig, ig_recv, acc, y_send, y_recv, w2, z_send, z_recv,
     lsem, s_ss, s_rs, e_ss, e_rs, t_ss, t_rs, ft_ss, ft_rs, p_ss, p_rs,
@@ -65,7 +65,7 @@
         loads = [
             pltpu.make_async_copy(src, dst, lsem.at[k])
             for k, (src, dst) in enumerate(
-                ((f_hbm, f_v), (q_hbm, q_v), (go_hbm, go_v), (x_hbm, x_v), (w_hbm, w_v))
+                ((f_hbm, f_v), (q_hbm, q_v), (go_hbm, go_v), (x_hbm, x_v), (w_hbm, w_v), (lb_hbm, lb_v))
             )
         ]
         for copy in loads:
@@ -92,7 +92,8 @@
         return out
 
     with scope("gates"):
-        gap = jnp.broadcast_to(1.0 - lb_ref[...], (tok, ch)).T
+        loads[5].wait()
+        gap = jnp.broadcast_to(1.0 - lb_v[...], (tok, ch)).T
         loads[0].wait()
         f = f_v[...].astype(F32)
         f_neg = 1.0 / (1.0 + jnp.exp(f))
@@ -312,6 +313,14 @@
                     copy.wait_send()
 
 
+def write_out(*refs):
+    copies = [pltpu.make_async_copy(refs[k], refs[4 + k], refs[8].at[k]) for k in range(4)]
+    for copy in copies:
+        copy.start()
+    for copy in copies:
+        copy.wait()
+
+
 def on_device(nz, ny, nx, block_input, value_weight, query_pre, forget_pre, lower_bound, out_grad):
     tok, d_model = block_input.shape
     ch = value_weight.shape[1]
@@ -321,7 +330,7 @@
     vm, dma = pltpu.VMEM, pltpu.SemaphoreType.DMA
     scratch = [
         vm((tok, d_model), BF16), vm((ch, d_model), BF16),
-        vm((ch, tok), BF16), vm((ch, tok), BF16), vm((ch, tok), BF16),
+        vm((ch, tok), BF16), vm((ch, tok), BF16), vm((ch, tok), BF16), vm((1, ch), F32),
         vm((pln, piece, ch), BF16), vm((1, ch), F32),
         vm((pln, piece, ch), BF16), vm((pln, 1, ch), F32),
         vm((pln, piece, ch), F32), vm((pln, 1, ch), F32),
@@ -333,7 +342,7 @@
         vm((2, tok // 2, d_model), BF16), vm((tok // 2, d_model), BF16),
         vm((ny, nz * rows, ch), F32), vm((ny, nz * rows, ch), BF16), vm((ny, nz * rows, ch), BF16),
         vm((nz, rows, ch), F32), vm((nz, rows, ch), BF16), vm((nz, rows, ch), BF16),
-        dma((5,)),
+        dma((6,)),
         dma((pln,)), dma((pln,)), dma((pln,)), dma((pln,)),
         dma((nz,)), dma((nz,)), dma((nz,)), dma((nz,)),
         dma((pln,)), dma((pln,)),
@@ -342,7 +351,7 @@
         dma, dma,
     ]
     hbm, near = pl.BlockSpec(memory_space=pl.ANY), pl.BlockSpec(memory_space=pltpu.VMEM)
-    g_query, g_forget, g_input, g_weight = pl.pallas_call(
+    results = pl.pallas_call(
         functools.partial(kernel, nz, ny, nx),
         out_shape=(
             vm((ch, tok), BF16),
@@ -350,11 +359,18 @@
             vm((tok // 2, d_model), BF16),
             vm((rows, ch), F32),
         ),
-        in_specs=[hbm] * 5 + [near],
+        in_specs=[hbm] * 6,
         out_specs=(near,) * 4,
         scratch_shapes=scratch,
         compiler_params=pltpu.CompilerParams(collective_id=0, has_side_effects=True),
     )(block_input, value_weight.T, query_pre.T, forget_pre.T, out_grad.T, lower_bound.reshape(1, ch))
+    g_query, g_forget, g_input, g_weight = pl.pallas_call(
+        write_out,
+        out_shape=tuple(jax.ShapeDtypeStruct(a.shape, a.dtype) for a in results),
+        in_specs=[near] * 4,
+        out_specs=(hbm,) * 4,
+        scratch_shapes=[dma((4,))],
+    )(*(pltpu.with_memory_space_constraint(a, pltpu.VMEM) for a in results))
     return g_query.T, g_forget.T, g_input, g_weight
 
 

time: 44.4 us -> 42.1 us (0.948)
  local copies, waits for them, and re-layouts: 2.55 us -> 0 us
    unnamed x4 -> x0, local copies, waits for them, and re-layouts: 2.55 us -> none
    pallas_call x0 -> x1, Pallas kernels: none -> 0.77 us  [on_device(): pl.pallas_call(write_out, out_shape=tuple((jax.ShapeDtypeStruct(a.shape,...]
    pallas_call x1, Pallas kernels: 41 us -> 40.6 us  [on_device(): pl.pallas_call(functools.partial(kernel, nz, ny, nx), out_shape=(vm((ch,...]
where the time goes in v3:
time: 42.1 us; the launch traced here: 42 us
  Pallas kernels  41.4 us (98%)
  between operations  0.64 us (2%)
    pallas_call x1, Pallas kernels, on_device(): pl.pallas_call(functools.partial(kernel, nz, ny, nx), out_shape=(vm((ch,...  40.6 us

profile of v3, /device:TPU:2, one launch (start us, length us, event | category | flops | bytes accessed | tf_op | source)
XLA Modules:
  0.0 42.0 jit_solution(17236313011156323645)
XLA Ops:
  0.6 40.6 %shard_map.93 = (bf16[192,128]{1,0:T(8,128)(2,1)S(1)}, bf16[192,128]{1,0:T(8,128)(2,1)S(1)}, bf16[64,2048]{1,0:T(8,128)(2,1)S(1)}, f32[16,192]{1,0:T(8,128)S(1)}) custom-call(bf16[128,2048]{1,0:T(8,128)(2,1)} %x_hbm.1, bf16[192,2048]{1,0:T(8,128)(2,1)} %bitcast.7, bf16[192,128]{1,0:T(8,128)(2,1)} %bitcast.8, bf16[192,128]{1,0:T(8,128)(2,1)} %bitcast.9, ...), custom_call_target="tpu_custom_call" | custom-call | tf_op jit(solution)/shard_map/pallas_call | solution.py:354
  41.2 0.8 %shard_map.94 = (bf16[192,128]{1,0:T(8,128)(2,1)}, bf16[192,128]{1,0:T(8,128)(2,1)}, bf16[64,2048]{1,0:T(8,128)(2,1)}, f32[16,192]{1,0:T(8,128)}) custom-call(bf16[192,128]{1,0:T(8,128)(2,1)S(1)} %get-tuple-element.12.refs_0_, bf16[192,128]{1,0:T(8,128)(2,1)S(1)} %get-tuple-element.13.refs_1_, bf16[64,2048]{1,0:T(8,128)(2,1)S(1)} %get-tuple-element.14.refs_2_, ...), custom_call_target="tpu_custom_call" | custom-call | tf_op jit(solution)/shard_map/pallas_call | solution.py:367

commit v4 on v3

--- a/solution.py
+++ b/solution.py
@@ -38,10 +38,12 @@
     x_hbm, w_hbm, q_hbm, f_hbm, go_hbm, lb_hbm,
     gq_out, gf_out, gx_out, gw_out,
     x_v, w_v, q_v, f_v, go_v, lb_v,
-    s_send, e_send, s_buf, e_buf, l_buf, fl_buf, t_send, ft_send, t_buf, ft_buf, o_send, p_buf,
-    xt, xtl, vg_v, vgl, ig, ig_recv, acc, y_send, y_recv, w2, z_send, z_recv,
-    lsem, s_ss, s_rs, e_ss, e_rs, t_ss, t_rs, ft_ss, ft_rs, p_ss, p_rs,
-    xt_ss, xt_rs, vg_ss, vg_rs, y_ss, y_rs, z_ss, z_rs, ig_ss, ig_rs,
+    s_send, e_send, s_buf, e_buf, l_buf, l_send, q_buf, t_send, ft_send, t_buf, ft_buf, o_send, p_buf,
+    xt, xtl, r_send, rl, k_send, kl, own_send, ownl, ig, ig_recv,
+    m_send, m_recv, aacc, a_send, a_recv, w2, z_send, z_recv,
+    lsem, s_ss, s_rs, e_ss, e_rs, q_ss, q_rs, t_ss, t_rs, ft_ss, ft_rs, p_ss, p_rs,
+    xt_ss, xt_rs, xd_ss, xd_rs, r_ss, r_rs, k_ss, k_rs, own_ss, own_rs,
+    m_ss, m_rs, a_ss, a_rs, z_ss, z_rs, ig_ss, ig_rs,
 ):
     pln = ny * nx
     tok, d_model = x_v.shape
@@ -126,38 +128,73 @@
         v = nt(w_v[...], x_v[...]).astype(BF16)
         update = folded(nt(v, k_end))
         s_send[...] = jnp.concatenate([update, reach], axis=0).reshape(s_send.shape).astype(BF16)
-
-    with scope("barrier_wait"):
-        pl.semaphore_wait(barrier, pln + nz - 1)
-    with scope("send1"):
-        sends = []
-        for k in range(1, pln):
-            to = lax.rem(me + k, pln)
-            sends.append(rcopy(e_send, e_buf.at[me], e_ss.at[k], e_rs.at[me], plane(to)))
-            sends.append(rcopy(s_send.at[to], s_buf.at[me], s_ss.at[k], s_rs.at[me], plane(to)))
-            sends[-2].start()
-            sends[-1].start()
-        s_buf[me] = s_send[me]
-        e_buf[me] = e_send[...]
+        r_send[...] = reach.astype(BF16)
+        k_send[...] = k_end
 
     with scope("turn"):
         rows = d_model // (nz * ny * nx)
         per = tok // rows
+        half = xt.shape[2]
         for b in range(d_model // tok):
             turned = x_v[:, tok * b : tok * (b + 1)].T
             for g in range(per):
                 at = b * per + g
                 zz, yy, xx = at // pln, (at // nx) % ny, at % nx
-                xt[xx, pl.ds((yy * nz + zz) * rows, rows), :] = turned[rows * g : rows * (g + 1)]
+                into = (yy * nz + zz) * rows
+                xt[xx, into // half, pl.ds(into % half, rows), :] = turned[rows * g : rows * (g + 1)]
+
+    with scope("barrier_wait"):
+        pl.semaphore_wait(barrier, pln + nz - 1)
+
+    sends = []
+
+    def start(copy):
+        copy.start()
+        sends.append(copy)
+
+    def to_line(source, target, send_sem, recv_sem):
+        for k in range(1, nx):
+            start(rcopy(source, target.at[x], send_sem.at[k], recv_sem.at[x], (z, y, lax.rem(x + k, nx), c)))
+
+    def from_line(source, target, send_sem, recv_sem):
+        for k in range(1, nx):
+            frm = lax.rem(x + k, nx)
+            rcopy(source, target.at[frm], send_sem.at[k], recv_sem.at[frm], (z, y, frm, c)).wait_recv()
+
+    def to_column(source, target, send_sem, recv_sem):
+        for k in range(1, ny):
+            to = lax.rem(y + k, ny)
+            start(rcopy(source.at[to], target.at[y], send_sem.at[k], recv_sem.at[y], (z, to, x, c)))
+
+    def from_column(own, source, target, send_sem, recv_sem):
+        out = own[...].astype(F32)
+        for k in range(1, ny):
+            frm = lax.rem(y + k, ny)
+            rcopy(source.at[0], target.at[frm], send_sem.at[k], recv_sem.at[frm], (z, frm, x, c)).wait_recv()
+            out = out + target[frm].astype(F32)
+        return out
+
+    with scope("send1"):
+        for k in range(1, pln):
+            to = lax.rem(me + k, pln)
+            start(rcopy(e_send, e_buf.at[me], e_ss.at[k], e_rs.at[me], plane(to)))
+            start(rcopy(s_send.at[to], s_buf.at[me], s_ss.at[k], s_rs.at[me], plane(to)))
         for k in range(1, nx):
             to = lax.rem(x + k, nx)
-            copy = rcopy(xt.at[to], xtl.at[x], xt_ss.at[k], xt_rs.at[x], (z, y, to, c))
-            copy.start()
-            sends.append(copy)
+            start(rcopy(xt.at[to, c], xtl.at[x, c], xt_ss.at[k], xt_rs.at[x], (z, y, to, c)))
+        to_line(k_send, kl, k_ss, k_rs)
+        to_line(r_send, rl, r_ss, r_rs)
+        s_buf[me] = s_send[me]
+        e_buf[me] = e_send[...]
+        xtl[x] = xt[x]
+        kl[x] = k_end
+        rl[x] = r_send[...]
 
     with scope("pairs_value"):
         mixing = [jnp.where(lower, tn(head_of(q_dec, h), head_of(k_dec, h)), 0.0).astype(BF16) for h in range(heads)]
         gv_own = by_head(nn(head_of(go, h), mixing[h]) for h in range(heads))
+        own_send[...] = gv_own.astype(BF16)
+        ownl[x] = own_send[...]
 
     with scope("wait1"):
         for k in range(1, pln):
@@ -170,7 +207,6 @@
         for o in range(pln):
             it = o + back * (pln - 1 - 2 * o)
             l_buf[it] = held
-            fl_buf[it] = factor
             decay = e_buf[it]
             held = decay * held + s_buf[it].astype(F32)
             factor = decay * factor
@@ -195,10 +231,31 @@
                 for copy in z_sends(k):
                     copy.start()
 
+        l_send[...] = l_buf[...].astype(BF16)
+
+        def within(i):
+            return i + back * ((i // nx) * nx + nx - 1 - i)
+
+        for k in range(1, pln):
+            to = lax.rem(me + k, pln)
+            start(rcopy(l_send.at[within(to)], q_buf.at[me], q_ss.at[k], q_rs.at[me], plane(to)))
+        q_buf[me] = l_send[within(me)]
+        to_line(own_send, ownl, own_ss, own_rs)
+
     with scope("pairs_query"):
         pairing = [jnp.where(upper, tn(head_of(v, h), head_of(go, h)), 0.0).astype(BF16) for h in range(heads)]
         gq_own = by_head(nn(head_of(k_dec, h), pairing[h]) for h in range(heads))
         gk_own = by_head(nt(head_of(q_dec, h), pairing[h]) for h in range(heads))
+
+    def swaps(k, part):
+        frm = lax.rem(x + k, nx)
+        return rcopy(xtl.at[frm, part], xtl.at[frm, part], xd_ss.at[k], xd_rs.at[frm], (z, y, x, 1 - c))
+
+    with scope("swap"):
+        for k in range(1, nx):
+            frm = lax.rem(x + k, nx)
+            rcopy(xt.at[0, c], xtl.at[frm, c], xt_ss.at[k], xt_rs.at[frm], (z, y, frm, c)).wait_recv()
+            start(swaps(k, c))
 
     def arriving(o, carried):
         frm = o + back * (nz - 1 - 2 * o)
@@ -210,29 +267,87 @@
         carried = lax.fori_loop(0, z_order, arriving, jnp.zeros(t_send.shape, F32))
 
     with scope("send3"):
-        o_send[...] = (l_buf[...] + fl_buf[...] * carried[None]).astype(BF16)
-        for k in range(1, pln):
-            to = lax.rem(me + k, pln)
-            copy = rcopy(o_send.at[to], p_buf.at[me], p_ss.at[k], p_rs.at[me], plane(to))
-            copy.start()
-            sends.append(copy)
-        p_buf[me] = o_send[me]
+        o_send[...] = carried.astype(BF16)
+        for k in range(1, pln):
+            start(rcopy(o_send, p_buf.at[me], p_ss.at[k], p_rs.at[me], plane(lax.rem(me + k, pln))))
+        p_buf[me] = o_send[...]
+
+    with scope("decays"):
+        ones_row = jnp.ones((1, ch), F32)
+        line_after, line_before = ones_row, ones_row
+        for i in range(pln):
+            line_after = line_after * jnp.where(i // nx > y, e_buf[i], 1.0)
+            line_before = line_before * jnp.where(i < me, e_buf[i], 1.0)
+        line_decay = [e_buf[y * nx + i] for i in range(nx)]
+        after = [line_after] * nx
+        for i in range(nx - 2, -1, -1):
+            after[i] = after[i + 1] * line_decay[i + 1]
+
+    with scope("wait_swap"):
+        from_line(k_send, kl, k_ss, k_rs)
+        for k in range(1, nx):
+            swaps(k, 1 - c).wait_recv()
+    with scope("line_m"):
+        all_rows = d_model // nx
+        turned_of = [xtl[i].reshape(all_rows, tok) for i in range(nx)]
+        m_sum = nt(turned_of[0], kl[0]) * after[0]
+        for i in range(1, nx):
+            m_sum = m_sum + nt(turned_of[i], kl[i]) * after[i]
+        m_sum = m_sum.reshape(ny, nz * rows, ch)
+        m_send[...] = m_sum.astype(BF16)
+        to_column(m_send, m_recv, m_ss, m_rs)
+
+    with scope("wait_1b"):
+        from_line(r_send, rl, r_ss, r_rs)
+        for k in range(1, pln):
+            frm = lax.rem(me + k, pln)
+            rcopy(l_send.at[0], q_buf.at[frm], q_ss.at[k], q_rs.at[frm], plane(frm)).wait_recv()
+        from_line(own_send, ownl, own_ss, own_rs)
+    with scope("line_a"):
+        inner = q_buf[...].astype(F32).reshape(2 * HEAD, ch)
+        state_in, grad_at = inner[:HEAD], inner[HEAD:]
+        grad_in = grad_at
+        a_sum = None
+        for i in range(nx - 1, -1, -1):
+            if i < nx - 1:
+                grad_at = line_decay[i + 1] * grad_at + rl[i + 1].astype(F32)
+            grad_in = jnp.where(x == i, grad_at, grad_in)
+            bd_in = by_head((grad_at * m).astype(BF16) for m in mf)
+            part = (ownl[i].astype(F32) + nn(bd_in, kl[i])).astype(BF16)
+            term = nt(turned_of[i], part)
+            a_sum = term if a_sum is None else a_sum + term
+        aacc[...] = a_sum.reshape(aacc.shape)
+        a_send[...] = a_sum.astype(BF16).reshape(a_send.shape)
+        to_column(a_send, a_recv, a_ss, a_rs)
+
+    with scope("wait_m"):
+        m_plane = from_column(m_send.at[y], m_send, m_recv, m_ss, m_rs).astype(BF16)
     with scope("wait3"):
         for k in range(1, pln):
             frm = lax.rem(me + k, pln)
-            rcopy(o_send.at[0], p_buf.at[frm], p_ss.at[k], p_rs.at[frm], plane(frm)).wait_recv()
+            rcopy(o_send, p_buf.at[frm], p_ss.at[k], p_rs.at[frm], plane(frm)).wait_recv()
+    with scope("wait_a"):
+        a_plane = from_column(aacc.at[y], a_send, a_recv, a_ss, a_rs)
+    with scope("send_z"):
+        outer = p_buf[...].astype(F32).reshape(2 * HEAD, ch)
+        state_out, grad_out = outer[:HEAD], outer[HEAD:]
+        bd_out = by_head((grad_out * m).astype(BF16) for m in mf)
+        w_sum = a_plane + nt(m_plane, bd_out)
+        w2[...] = w_sum.reshape(w2.shape)
+        z_send[...] = w_sum.astype(BF16).reshape(z_send.shape)
+        for k in range(1, nz):
+            to = lax.rem(z + k, nz)
+            start(rcopy(z_send.at[to], z_recv.at[z], z_ss.at[k], z_rs.at[z], (to, y, x, c)))
+
     with scope("value_grad"):
-        carries = p_buf[...].astype(F32).reshape(2 * HEAD, ch)
-        state, grad = carries[:HEAD], carries[HEAD:]
+        own_after = after[nx - 1]
+        for i in range(nx - 1):
+            own_after = jnp.where(x == i, after[i], own_after)
+        state = state_in + line_before * state_out
+        grad = grad_in + own_after * grad_out
         bd_state = by_head((state * m).astype(BF16) for m in mf)
         bd_grad = by_head((grad * m).astype(BF16) for m in mf)
         value_grad = (gv_own + nn(bd_grad, k_end)).astype(BF16)
-        vg_v[...] = value_grad
-        for k in range(1, nx):
-            to = lax.rem(x + k, nx)
-            copy = rcopy(vg_v, vgl.at[x], vg_ss.at[k], vg_rs.at[x], (z, y, to, c))
-            copy.start()
-            sends.append(copy)
 
     with scope("input_grad"):
         width = 512 if d_model % 512 == 0 else d_model
@@ -242,23 +357,6 @@
             ig[:, :, cols] = nn(turned, w_v[:, cols]).astype(BF16).reshape(2, tok // 2, width)
         ig_copy = rcopy(ig.at[1 - c], ig_recv, ig_ss, ig_rs, (z, y, x, 1 - c))
         ig_copy.start()
-
-    with scope("weight_own"):
-        total_w = nt(xt[x], value_grad)
-    for k in range(1, nx):
-        frm = lax.rem(x + k, nx)
-        with scope(f"wait_vg{k}"):
-            rcopy(xt.at[0], xtl.at[frm], xt_ss.at[k], xt_rs.at[frm], (z, y, frm, c)).wait_recv()
-            rcopy(vg_v, vgl.at[frm], vg_ss.at[k], vg_rs.at[frm], (z, y, frm, c)).wait_recv()
-        total_w = total_w + nt(xtl[frm], vgl[frm])
-    with scope("send_y"):
-        acc[...] = total_w.reshape(acc.shape)
-        y_send[...] = total_w.astype(BF16).reshape(y_send.shape)
-        for k in range(1, ny):
-            to = lax.rem(y + k, ny)
-            copy = rcopy(y_send.at[to], y_recv.at[y], y_ss.at[k], y_rs.at[y], (z, to, x, c))
-            copy.start()
-            sends.append(copy)
 
     with scope("query_forget"):
         g_query = growth * (gq_own + tn(bd_state, go))
@@ -275,26 +373,12 @@
         g_decay = nn(flow_high, lower_ones) + nn(flow_low, lower_ones) + boundary
         gf_out[...] = ((g_decay / (1.0 - k_rate) - g_key) * k_rate * f_sig).astype(BF16)
 
-    w_sum = acc[y]
-    with scope("wait_y"):
-        for k in range(1, ny):
-            frm = lax.rem(y + k, ny)
-            rcopy(y_send.at[0], y_recv.at[frm], y_ss.at[k], y_rs.at[frm], (z, frm, x, c)).wait_recv()
-            w_sum = w_sum + y_recv[frm].astype(F32)
-    with scope("send_z"):
-        w2[...] = w_sum.reshape(w2.shape)
-        z_send[...] = w_sum.astype(BF16).reshape(z_send.shape)
-        for k in range(1, nz):
-            to = lax.rem(z + k, nz)
-            copy = rcopy(z_send.at[to], z_recv.at[z], z_ss.at[k], z_rs.at[z], (to, y, x, c))
-            copy.start()
-            sends.append(copy)
     with scope("input_sum"):
         ig_copy.wait_recv()
         gx_out[...] = (ig[c].astype(F32) + ig_recv[...].astype(F32)).astype(BF16)
 
-    w_last = w2[z]
     with scope("wait_z"):
+        w_last = w2[z]
         for k in range(1, nz):
             frm = lax.rem(z + k, nz)
             rcopy(z_send.at[0], z_recv.at[frm], z_ss.at[k], z_rs.at[frm], (frm, y, x, c)).wait_recv()
@@ -333,21 +417,25 @@
         vm((ch, tok), BF16), vm((ch, tok), BF16), vm((ch, tok), BF16), vm((1, ch), F32),
         vm((pln, piece, ch), BF16), vm((1, ch), F32),
         vm((pln, piece, ch), BF16), vm((pln, 1, ch), F32),
-        vm((pln, piece, ch), F32), vm((pln, 1, ch), F32),
+        vm((pln, piece, ch), F32), vm((pln, piece, ch), BF16), vm((pln, piece, ch), BF16),
         vm((piece, ch), BF16), vm((1, ch), F32),
         vm((nz, piece, ch), BF16), vm((nz, 1, ch), F32),
-        vm((pln, piece, ch), BF16), vm((pln, piece, ch), BF16),
-        vm((nx, d_model // nx, tok), BF16), vm((nx, d_model // nx, tok), BF16),
+        vm((piece, ch), BF16), vm((pln, piece, ch), BF16),
+        vm((nx, 2, d_model // nx // 2, tok), BF16), vm((nx, 2, d_model // nx // 2, tok), BF16),
+        vm((HEAD, ch), BF16), vm((nx, HEAD, ch), BF16),
+        vm((ch, tok), BF16), vm((nx, ch, tok), BF16),
         vm((ch, tok), BF16), vm((nx, ch, tok), BF16),
         vm((2, tok // 2, d_model), BF16), vm((tok // 2, d_model), BF16),
+        vm((ny, nz * rows, ch), BF16), vm((ny, nz * rows, ch), BF16),
         vm((ny, nz * rows, ch), F32), vm((ny, nz * rows, ch), BF16), vm((ny, nz * rows, ch), BF16),
         vm((nz, rows, ch), F32), vm((nz, rows, ch), BF16), vm((nz, rows, ch), BF16),
         dma((6,)),
-        dma((pln,)), dma((pln,)), dma((pln,)), dma((pln,)),
+        dma((pln,)), dma((pln,)), dma((pln,)), dma((pln,)), dma((pln,)), dma((pln,)),
         dma((nz,)), dma((nz,)), dma((nz,)), dma((nz,)),
         dma((pln,)), dma((pln,)),
-        dma((nx,)), dma((nx,)), dma((nx,)), dma((nx,)),
-        dma((ny,)), dma((ny,)), dma((nz,)), dma((nz,)),
+        *(dma((nx,)) for _ in range(10)),
+        *(dma((ny,)) for _ in range(4)),
+        dma((nz,)), dma((nz,)),
         dma, dma,
     ]
     hbm, near = pl.BlockSpec(memory_space=pl.ANY), pl.BlockSpec(memory_space=pltpu.VMEM)

time: 42.1 us -> 36 us (0.86)
  the two profiles are of different devices: /device:TPU:2 before, /device:TPU:1 now
where the time goes in v4:
time: 36 us; the launch traced here: 35.3 us
  Pallas kernels  34.7 us (96%)
  between operations  0.64 us (2%)
    pallas_call x1, Pallas kernels, on_device(): pl.pallas_call(functools.partial(kernel, nz, ny, nx), out_shape=(vm((ch,...  33.9 us
    pallas_call x1, Pallas kernels, on_device(): pl.pallas_call(write_out, out_shape=tuple((jax.ShapeDtypeStruct(a.shape,...  0.77 us

profile of v4, /device:TPU:1, one launch (start us, length us, event | category | flops | bytes accessed | tf_op | source)
XLA Modules:
  0.0 35.3 jit_solution(8997089413347221075)
XLA Ops:
  0.6 33.9 %shard_map.93 = (bf16[192,128]{1,0:T(8,128)(2,1)S(1)}, bf16[192,128]{1,0:T(8,128)(2,1)S(1)}, bf16[64,2048]{1,0:T(8,128)(2,1)S(1)}, f32[16,192]{1,0:T(8,128)S(1)}) custom-call(bf16[128,2048]{1,0:T(8,128)(2,1)} %x_hbm.1, bf16[192,2048]{1,0:T(8,128)(2,1)} %bitcast.7, bf16[192,128]{1,0:T(8,128)(2,1)} %bitcast.8, bf16[192,128]{1,0:T(8,128)(2,1)} %bitcast.9, ...), custom_call_target="tpu_custom_call" | custom-call | tf_op jit(solution)/shard_map/pallas_call | solution.py:442
  34.6 0.8 %shard_map.94 = (bf16[192,128]{1,0:T(8,128)(2,1)}, bf16[192,128]{1,0:T(8,128)(2,1)}, bf16[64,2048]{1,0:T(8,128)(2,1)}, f32[16,192]{1,0:T(8,128)}) custom-call(bf16[192,128]{1,0:T(8,128)(2,1)S(1)} %get-tuple-element.12.refs_0_, bf16[192,128]{1,0:T(8,128)(2,1)S(1)} %get-tuple-element.13.refs_1_, bf16[64,2048]{1,0:T(8,128)(2,1)S(1)} %get-tuple-element.14.refs_2_, ...), custom_call_target="tpu_custom_call" | custom-call | tf_op jit(solution)/shard_map/pallas_call | solution.py:455

commit v5 on v4

--- a/solution.py
+++ b/solution.py
@@ -38,11 +38,11 @@
     x_hbm, w_hbm, q_hbm, f_hbm, go_hbm, lb_hbm,
     gq_out, gf_out, gx_out, gw_out,
     x_v, w_v, q_v, f_v, go_v, lb_v,
-    s_send, e_send, s_buf, e_buf, l_buf, l_send, q_buf, t_send, ft_send, t_buf, ft_buf, o_send, p_buf,
-    xt, xtl, r_send, rl, k_send, kl, own_send, ownl, ig, ig_recv,
+    s_send, e_send, s_buf, e_buf, l_send, q_state, q_grad, t_send, ft_send, t_buf, ft_buf, o_send, p_buf,
+    xt, xtl, k_send, kl, own_send, ownl, ig, ig_recv,
     m_send, m_recv, aacc, a_send, a_recv, w2, z_send, z_recv,
     lsem, s_ss, s_rs, e_ss, e_rs, q_ss, q_rs, t_ss, t_rs, ft_ss, ft_rs, p_ss, p_rs,
-    xt_ss, xt_rs, xd_ss, xd_rs, r_ss, r_rs, k_ss, k_rs, own_ss, own_rs,
+    xt_ss, xt_rs, k_ss, k_rs, own_ss, own_rs,
     m_ss, m_rs, a_ss, a_rs, z_ss, z_rs, ig_ss, ig_rs,
 ):
     pln = ny * nx
@@ -51,7 +51,20 @@
     heads = ch // HEAD
     z, y, x, c = (lax.axis_index(a) for a in SP_TP)
     me = y * nx + x
-    back = (me * 2) // pln
+    back = lax.rem(me, 2)
+    at_line, at_col = x * (1 - c) + y * c, y * (1 - c) + x * c
+
+    def line(i):
+        return (z, y * (1 - c) + i * c, i * (1 - c) + x * c, c)
+
+    def column(i):
+        return (z, i * (1 - c) + y * c, x * (1 - c) + i * c, c)
+
+    def by_lines(i):
+        return i * (1 - c) + (lax.rem(i, nx) * ny + i // nx) * c
+
+    def piece_of(i):
+        return i // 2 + lax.rem(i, 2) * (pln // 2)
 
     def plane(i):
         return (z, i // nx, lax.rem(i, nx), c)
@@ -128,20 +141,18 @@
         v = nt(w_v[...], x_v[...]).astype(BF16)
         update = folded(nt(v, k_end))
         s_send[...] = jnp.concatenate([update, reach], axis=0).reshape(s_send.shape).astype(BF16)
-        r_send[...] = reach.astype(BF16)
         k_send[...] = k_end
 
     with scope("turn"):
         rows = d_model // (nz * ny * nx)
         per = tok // rows
-        half = xt.shape[2]
         for b in range(d_model // tok):
             turned = x_v[:, tok * b : tok * (b + 1)].T
             for g in range(per):
                 at = b * per + g
                 zz, yy, xx = at // pln, (at // nx) % ny, at % nx
-                into = (yy * nz + zz) * rows
-                xt[xx, into // half, pl.ds(into % half, rows), :] = turned[rows * g : rows * (g + 1)]
+                group, into = xx * (1 - c) + yy * c, yy * (1 - c) + xx * c
+                xt[group, into, zz] = turned[rows * g : rows * (g + 1)]
 
     with scope("barrier_wait"):
         pl.semaphore_wait(barrier, pln + nz - 1)
@@ -154,23 +165,23 @@
 
     def to_line(source, target, send_sem, recv_sem):
         for k in range(1, nx):
-            start(rcopy(source, target.at[x], send_sem.at[k], recv_sem.at[x], (z, y, lax.rem(x + k, nx), c)))
+            start(rcopy(source, target.at[at_line], send_sem.at[k], recv_sem.at[at_line], line(lax.rem(at_line + k, nx))))
 
     def from_line(source, target, send_sem, recv_sem):
         for k in range(1, nx):
-            frm = lax.rem(x + k, nx)
-            rcopy(source, target.at[frm], send_sem.at[k], recv_sem.at[frm], (z, y, frm, c)).wait_recv()
+            frm = lax.rem(at_line + k, nx)
+            rcopy(source, target.at[frm], send_sem.at[k], recv_sem.at[frm], line(frm)).wait_recv()
 
     def to_column(source, target, send_sem, recv_sem):
         for k in range(1, ny):
-            to = lax.rem(y + k, ny)
-            start(rcopy(source.at[to], target.at[y], send_sem.at[k], recv_sem.at[y], (z, to, x, c)))
+            to = lax.rem(at_col + k, ny)
+            start(rcopy(source.at[to], target.at[at_col], send_sem.at[k], recv_sem.at[at_col], column(to)))
 
     def from_column(own, source, target, send_sem, recv_sem):
         out = own[...].astype(F32)
         for k in range(1, ny):
-            frm = lax.rem(y + k, ny)
-            rcopy(source.at[0], target.at[frm], send_sem.at[k], recv_sem.at[frm], (z, frm, x, c)).wait_recv()
+            frm = lax.rem(at_col + k, ny)
+            rcopy(source.at[0], target.at[frm], send_sem.at[k], recv_sem.at[frm], column(frm)).wait_recv()
             out = out + target[frm].astype(F32)
         return out
 
@@ -178,23 +189,21 @@
         for k in range(1, pln):
             to = lax.rem(me + k, pln)
             start(rcopy(e_send, e_buf.at[me], e_ss.at[k], e_rs.at[me], plane(to)))
-            start(rcopy(s_send.at[to], s_buf.at[me], s_ss.at[k], s_rs.at[me], plane(to)))
+            start(rcopy(s_send.at[piece_of(to)], s_buf.at[me], s_ss.at[k], s_rs.at[me], plane(to)))
         for k in range(1, nx):
-            to = lax.rem(x + k, nx)
-            start(rcopy(xt.at[to, c], xtl.at[x, c], xt_ss.at[k], xt_rs.at[x], (z, y, to, c)))
+            to = lax.rem(at_line + k, nx)
+            start(rcopy(xt.at[to], xtl.at[at_line], xt_ss.at[k], xt_rs.at[at_line], line(to)))
         to_line(k_send, kl, k_ss, k_rs)
-        to_line(r_send, rl, r_ss, r_rs)
-        s_buf[me] = s_send[me]
+        s_buf[me] = s_send[piece_of(me)]
         e_buf[me] = e_send[...]
-        xtl[x] = xt[x]
-        kl[x] = k_end
-        rl[x] = r_send[...]
+        xtl[at_line] = xt[at_line]
+        kl[at_line] = k_end
 
     with scope("pairs_value"):
         mixing = [jnp.where(lower, tn(head_of(q_dec, h), head_of(k_dec, h)), 0.0).astype(BF16) for h in range(heads)]
         gv_own = by_head(nn(head_of(go, h), mixing[h]) for h in range(heads))
         own_send[...] = gv_own.astype(BF16)
-        ownl[x] = own_send[...]
+        ownl[at_line] = own_send[...]
 
     with scope("wait1"):
         for k in range(1, pln):
@@ -206,7 +215,7 @@
         factor = jnp.ones((1, ch), F32)
         for o in range(pln):
             it = o + back * (pln - 1 - 2 * o)
-            l_buf[it] = held
+            l_send[by_lines(it)] = held.astype(BF16)
             decay = e_buf[it]
             held = decay * held + s_buf[it].astype(F32)
             factor = decay * factor
@@ -223,6 +232,13 @@
             rcopy(t_send, t_buf.at[z], t_ss.at[k], t_rs.at[z], (to, y, x, c)),
         )
 
+    def state_sends(k, to):
+        return rcopy(l_send.at[by_lines(to)], q_state.at[me // 2], q_ss.at[k], q_rs.at[me], plane(to))
+
+    def grad_sends(k, to):
+        first = by_lines(to) // nx * nx
+        return rcopy(l_send.at[pl.ds(first, nx)], q_grad.at[me // 2], q_ss.at[k], q_rs.at[me], plane(to))
+
     with scope("send2"):
         for k in range(1, nz):
 
@@ -231,15 +247,25 @@
                 for copy in z_sends(k):
                     copy.start()
 
-        l_send[...] = l_buf[...].astype(BF16)
-
-        def within(i):
-            return i + back * ((i // nx) * nx + nx - 1 - i)
-
         for k in range(1, pln):
             to = lax.rem(me + k, pln)
-            start(rcopy(l_send.at[within(to)], q_buf.at[me], q_ss.at[k], q_rs.at[me], plane(to)))
-        q_buf[me] = l_send[within(me)]
+
+            @pl.when(back == 0)
+            def _():
+                state_sends(k, to).start()
+
+            @pl.when(back == 1)
+            def _():
+                grad_sends(k, to).start()
+
+        @pl.when(back == 0)
+        def _():
+            q_state[me // 2] = l_send[by_lines(me)]
+
+        @pl.when(back == 1)
+        def _():
+            q_grad[me // 2] = l_send[pl.ds(at_col * nx, nx)]
+
         to_line(own_send, ownl, own_ss, own_rs)
 
     with scope("pairs_query"):
@@ -247,71 +273,63 @@
         gq_own = by_head(nn(head_of(k_dec, h), pairing[h]) for h in range(heads))
         gk_own = by_head(nt(head_of(q_dec, h), pairing[h]) for h in range(heads))
 
-    def swaps(k, part):
-        frm = lax.rem(x + k, nx)
-        return rcopy(xtl.at[frm, part], xtl.at[frm, part], xd_ss.at[k], xd_rs.at[frm], (z, y, x, 1 - c))
-
-    with scope("swap"):
+    with scope("decays"):
+        before, after = jnp.ones((1, ch), F32), [jnp.ones((1, ch), F32)] * nx
+        ids = [line(i)[1] * nx + line(i)[2] for i in range(nx)]
+        for i in range(pln):
+            before = before * jnp.where(i < me, e_buf[i], 1.0)
+            after = [a * jnp.where(i > n, e_buf[i], 1.0) for a, n in zip(after, ids)]
+
+    with scope("wait_line"):
         for k in range(1, nx):
-            frm = lax.rem(x + k, nx)
-            rcopy(xt.at[0, c], xtl.at[frm, c], xt_ss.at[k], xt_rs.at[frm], (z, y, frm, c)).wait_recv()
-            start(swaps(k, c))
-
-    def arriving(o, carried):
-        frm = o + back * (nz - 1 - 2 * o)
-        rcopy(ft_send, ft_buf.at[frm], ft_ss.at[0], ft_rs.at[frm], (z, y, x, c)).wait_recv()
-        rcopy(t_send, t_buf.at[frm], t_ss.at[0], t_rs.at[frm], (z, y, x, c)).wait_recv()
-        return ft_buf[frm] * carried + t_buf[frm].astype(F32)
-
-    with scope("wait2"):
-        carried = lax.fori_loop(0, z_order, arriving, jnp.zeros(t_send.shape, F32))
-
-    with scope("send3"):
-        o_send[...] = carried.astype(BF16)
-        for k in range(1, pln):
-            start(rcopy(o_send, p_buf.at[me], p_ss.at[k], p_rs.at[me], plane(lax.rem(me + k, pln))))
-        p_buf[me] = o_send[...]
-
-    with scope("decays"):
-        ones_row = jnp.ones((1, ch), F32)
-        line_after, line_before = ones_row, ones_row
-        for i in range(pln):
-            line_after = line_after * jnp.where(i // nx > y, e_buf[i], 1.0)
-            line_before = line_before * jnp.where(i < me, e_buf[i], 1.0)
-        line_decay = [e_buf[y * nx + i] for i in range(nx)]
-        after = [line_after] * nx
-        for i in range(nx - 2, -1, -1):
-            after[i] = after[i + 1] * line_decay[i + 1]
-
-    with scope("wait_swap"):
+            frm = lax.rem(at_line + k, nx)
+            rcopy(xt.at[0], xtl.at[frm], xt_ss.at[k], xt_rs.at[frm], line(frm)).wait_recv()
         from_line(k_send, kl, k_ss, k_rs)
-        for k in range(1, nx):
-            swaps(k, 1 - c).wait_recv()
     with scope("line_m"):
         all_rows = d_model // nx
         turned_of = [xtl[i].reshape(all_rows, tok) for i in range(nx)]
         m_sum = nt(turned_of[0], kl[0]) * after[0]
         for i in range(1, nx):
             m_sum = m_sum + nt(turned_of[i], kl[i]) * after[i]
-        m_sum = m_sum.reshape(ny, nz * rows, ch)
-        m_send[...] = m_sum.astype(BF16)
+        m_send[...] = m_sum.reshape(ny, nz * rows, ch).astype(BF16)
         to_column(m_send, m_recv, m_ss, m_rs)
 
+    def arriving(o, carried):
+        frm = o + back * (nz - 1 - 2 * o)
+        rcopy(ft_send, ft_buf.at[frm], ft_ss.at[0], ft_rs.at[frm], (z, y, x, c)).wait_recv()
+        rcopy(t_send, t_buf.at[frm], t_ss.at[0], t_rs.at[frm], (z, y, x, c)).wait_recv()
+        return ft_buf[frm] * carried + t_buf[frm].astype(F32)
+
+    with scope("wait2"):
+        carried = lax.fori_loop(0, z_order, arriving, jnp.zeros(t_send.shape, F32))
+
+    with scope("send3"):
+        o_send[...] = carried.astype(BF16)
+        mine = piece_of(me)
+        for k in range(1, pln):
+            start(rcopy(o_send, p_buf.at[mine], p_ss.at[k], p_rs.at[mine], plane(lax.rem(me + k, pln))))
+        p_buf[mine] = o_send[...]
+
     with scope("wait_1b"):
-        from_line(r_send, rl, r_ss, r_rs)
-        for k in range(1, pln):
-            frm = lax.rem(me + k, pln)
-            rcopy(l_send.at[0], q_buf.at[frm], q_ss.at[k], q_rs.at[frm], plane(frm)).wait_recv()
+        for j in range(pln // 2):
+
+            @pl.when(me != 2 * j)
+            def _():
+                rcopy(l_send.at[0], q_state.at[j], q_ss.at[0], q_rs.at[2 * j], plane(2 * j)).wait_recv()
+
+            @pl.when(me != 2 * j + 1)
+            def _():
+                rcopy(
+                    l_send.at[pl.ds(0, nx)], q_grad.at[j], q_ss.at[0], q_rs.at[2 * j + 1], plane(2 * j + 1)
+                ).wait_recv()
+
         from_line(own_send, ownl, own_ss, own_rs)
     with scope("line_a"):
-        inner = q_buf[...].astype(F32).reshape(2 * HEAD, ch)
-        state_in, grad_at = inner[:HEAD], inner[HEAD:]
-        grad_in = grad_at
-        a_sum = None
-        for i in range(nx - 1, -1, -1):
-            if i < nx - 1:
-                grad_at = line_decay[i + 1] * grad_at + rl[i + 1].astype(F32)
-            grad_in = jnp.where(x == i, grad_at, grad_in)
+        state_in = q_state[...].astype(F32).reshape(HEAD, ch)
+        a_sum, grad_in = None, None
+        for i in range(nx):
+            grad_at = q_grad[:, i].astype(F32).reshape(HEAD, ch)
+            grad_in = grad_at if i == 0 else jnp.where(at_line == i, grad_at, grad_in)
             bd_in = by_head((grad_at * m).astype(BF16) for m in mf)
             part = (ownl[i].astype(F32) + nn(bd_in, kl[i])).astype(BF16)
             term = nt(turned_of[i], part)
@@ -321,13 +339,14 @@
         to_column(a_send, a_recv, a_ss, a_rs)
 
     with scope("wait_m"):
-        m_plane = from_column(m_send.at[y], m_send, m_recv, m_ss, m_rs).astype(BF16)
+        m_plane = from_column(m_send.at[at_col], m_send, m_recv, m_ss, m_rs).astype(BF16)
     with scope("wait3"):
         for k in range(1, pln):
             frm = lax.rem(me + k, pln)
-            rcopy(o_send, p_buf.at[frm], p_ss.at[k], p_rs.at[frm], plane(frm)).wait_recv()
+            part = piece_of(frm)
+            rcopy(o_send, p_buf.at[part], p_ss.at[k], p_rs.at[part], plane(frm)).wait_recv()
     with scope("wait_a"):
-        a_plane = from_column(aacc.at[y], a_send, a_recv, a_ss, a_rs)
+        a_plane = from_column(aacc.at[at_col], a_send, a_recv, a_ss, a_rs)
     with scope("send_z"):
         outer = p_buf[...].astype(F32).reshape(2 * HEAD, ch)
         state_out, grad_out = outer[:HEAD], outer[HEAD:]
@@ -342,8 +361,8 @@
     with scope("value_grad"):
         own_after = after[nx - 1]
         for i in range(nx - 1):
-            own_after = jnp.where(x == i, after[i], own_after)
-        state = state_in + line_before * state_out
+            own_after = jnp.where(at_line == i, after[i], own_after)
+        state = state_in + before * state_out
         grad = grad_in + own_after * grad_out
         bd_state = by_head((state * m).astype(BF16) for m in mf)
         bd_grad = by_head((grad * m).astype(BF16) for m in mf)
@@ -389,6 +408,17 @@
         for copy in sends:
             copy.wait_send()
         ig_copy.wait_send()
+        for k in range(1, pln):
+            to = lax.rem(me + k, pln)
+
+            @pl.when(back == 0)
+            def _():
+                state_sends(k, to).wait_send()
+
+            @pl.when(back == 1)
+            def _():
+                grad_sends(k, to).wait_send()
+
         for k in range(1, nz):
 
             @pl.when(z_order + k < nz)
@@ -417,12 +447,11 @@
         vm((ch, tok), BF16), vm((ch, tok), BF16), vm((ch, tok), BF16), vm((1, ch), F32),
         vm((pln, piece, ch), BF16), vm((1, ch), F32),
         vm((pln, piece, ch), BF16), vm((pln, 1, ch), F32),
-        vm((pln, piece, ch), F32), vm((pln, piece, ch), BF16), vm((pln, piece, ch), BF16),
+        vm((pln, piece, ch), BF16), vm((pln // 2, piece, ch), BF16), vm((pln // 2, nx, piece, ch), BF16),
         vm((piece, ch), BF16), vm((1, ch), F32),
         vm((nz, piece, ch), BF16), vm((nz, 1, ch), F32),
         vm((piece, ch), BF16), vm((pln, piece, ch), BF16),
-        vm((nx, 2, d_model // nx // 2, tok), BF16), vm((nx, 2, d_model // nx // 2, tok), BF16),
-        vm((HEAD, ch), BF16), vm((nx, HEAD, ch), BF16),
+        vm((nx, ny, nz, rows, tok), BF16), vm((nx, ny, nz, rows, tok), BF16),
         vm((ch, tok), BF16), vm((nx, ch, tok), BF16),
         vm((ch, tok), BF16), vm((nx, ch, tok), BF16),
         vm((2, tok // 2, d_model), BF16), vm((tok // 2, d_model), BF16),
@@ -433,7 +462,7 @@
         dma((pln,)), dma((pln,)), dma((pln,)), dma((pln,)), dma((pln,)), dma((pln,)),
         dma((nz,)), dma((nz,)), dma((nz,)), dma((nz,)),
         dma((pln,)), dma((pln,)),
-        *(dma((nx,)) for _ in range(10)),
+        *(dma((nx,)) for _ in range(6)),
         *(dma((ny,)) for _ in range(4)),
         dma((nz,)), dma((nz,)),
         dma, dma,

time: 36 us -> 35.5 us (0.986)
  no operation moved by 1% of the time
where the time goes in v5:
time: 35.5 us; the launch traced here: 35.1 us
  Pallas kernels  34.5 us (97%)
  between operations  0.64 us (2%)
    pallas_call x1, Pallas kernels, on_device(): pl.pallas_call(functools.partial(kernel, nz, ny, nx), out_shape=(vm((ch,...  33.7 us
    pallas_call x1, Pallas kernels, on_device(): pl.pallas_call(write_out, out_shape=tuple((jax.ShapeDtypeStruct(a.shape,...  0.77 us

profile of v5, /device:TPU:1, one launch (start us, length us, event | category | flops | bytes accessed | tf_op | source)
XLA Modules:
  0.0 35.1 jit_solution(15298114870958275072)
XLA Ops:
  0.6 33.7 %shard_map.93 = (bf16[192,128]{1,0:T(8,128)(2,1)S(1)}, bf16[192,128]{1,0:T(8,128)(2,1)S(1)}, bf16[64,2048]{1,0:T(8,128)(2,1)S(1)}, f32[16,192]{1,0:T(8,128)S(1)}) custom-call(bf16[128,2048]{1,0:T(8,128)(2,1)} %x_hbm.1, bf16[192,2048]{1,0:T(8,128)(2,1)} %bitcast.7, bf16[192,128]{1,0:T(8,128)(2,1)} %bitcast.8, bf16[192,128]{1,0:T(8,128)(2,1)} %bitcast.9, ...), custom_call_target="tpu_custom_call" | custom-call | tf_op jit(solution)/shard_map/pallas_call | solution.py:471
  34.4 0.8 %shard_map.94 = (bf16[192,128]{1,0:T(8,128)(2,1)}, bf16[192,128]{1,0:T(8,128)(2,1)}, bf16[64,2048]{1,0:T(8,128)(2,1)}, f32[16,192]{1,0:T(8,128)}) custom-call(bf16[192,128]{1,0:T(8,128)(2,1)S(1)} %get-tuple-element.12.refs_0_, bf16[192,128]{1,0:T(8,128)(2,1)S(1)} %get-tuple-element.13.refs_1_, bf16[64,2048]{1,0:T(8,128)(2,1)S(1)} %get-tuple-element.14.refs_2_, ...), custom_call_target="tpu_custom_call" | custom-call | tf_op jit(solution)/shard_map/pallas_call | solution.py:484

commit v6 on v5

--- a/solution.py
+++ b/solution.py
@@ -38,11 +38,11 @@
     x_hbm, w_hbm, q_hbm, f_hbm, go_hbm, lb_hbm,
     gq_out, gf_out, gx_out, gw_out,
     x_v, w_v, q_v, f_v, go_v, lb_v,
-    s_send, e_send, s_buf, e_buf, l_send, q_state, q_grad, t_send, ft_send, t_buf, ft_buf, o_send, p_buf,
-    xt, xtl, k_send, kl, own_send, ownl, ig, ig_recv,
+    s_send, e_send, s_buf, e_buf, l_send, q_state, q_grad, q_line, t_send, ft_send, t_buf, ft_buf, o_send, p_buf,
+    xt, xtl, r_send, rl, k_send, kl, own_send, ownl, g_all, ig, ig_recv,
     m_send, m_recv, aacc, a_send, a_recv, w2, z_send, z_recv,
     lsem, s_ss, s_rs, e_ss, e_rs, q_ss, q_rs, t_ss, t_rs, ft_ss, ft_rs, p_ss, p_rs,
-    xt_ss, xt_rs, k_ss, k_rs, own_ss, own_rs,
+    xt_ss, xt_rs, r_ss, r_rs, k_ss, k_rs, own_ss, own_rs,
     m_ss, m_rs, a_ss, a_rs, z_ss, z_rs, ig_ss, ig_rs,
 ):
     pln = ny * nx
@@ -141,6 +141,7 @@
         v = nt(w_v[...], x_v[...]).astype(BF16)
         update = folded(nt(v, k_end))
         s_send[...] = jnp.concatenate([update, reach], axis=0).reshape(s_send.shape).astype(BF16)
+        r_send[...] = reach.astype(BF16)
         k_send[...] = k_end
 
     with scope("turn"):
@@ -185,6 +186,10 @@
             out = out + target[frm].astype(F32)
         return out
 
+    def reach_sends(k):
+        to = lax.rem(at_line + k, nx)
+        return rcopy(r_send, rl.at[at_line], r_ss.at[k], r_rs.at[at_line], line(to))
+
     with scope("send1"):
         for k in range(1, pln):
             to = lax.rem(me + k, pln)
@@ -194,10 +199,17 @@
             to = lax.rem(at_line + k, nx)
             start(rcopy(xt.at[to], xtl.at[at_line], xt_ss.at[k], xt_rs.at[at_line], line(to)))
         to_line(k_send, kl, k_ss, k_rs)
+
+        @pl.when(c == 0)
+        def _():
+            for k in range(1, nx):
+                reach_sends(k).start()
+
         s_buf[me] = s_send[piece_of(me)]
         e_buf[me] = e_send[...]
         xtl[at_line] = xt[at_line]
         kl[at_line] = k_end
+        rl[at_line] = r_send[...]
 
     with scope("pairs_value"):
         mixing = [jnp.where(lower, tn(head_of(q_dec, h), head_of(k_dec, h)), 0.0).astype(BF16) for h in range(heads)]
@@ -235,6 +247,10 @@
     def state_sends(k, to):
         return rcopy(l_send.at[by_lines(to)], q_state.at[me // 2], q_ss.at[k], q_rs.at[me], plane(to))
 
+    def line_sends(k, to):
+        last = to // nx * nx + nx - 1
+        return rcopy(l_send.at[last], q_line.at[me // 2], q_ss.at[k], q_rs.at[me], plane(to))
+
     def grad_sends(k, to):
         first = by_lines(to) // nx * nx
         return rcopy(l_send.at[pl.ds(first, nx)], q_grad.at[me // 2], q_ss.at[k], q_rs.at[me], plane(to))
@@ -254,7 +270,11 @@
             def _():
                 state_sends(k, to).start()
 
-            @pl.when(back == 1)
+            @pl.when((back == 1) & (c == 0))
+            def _():
+                line_sends(k, to).start()
+
+            @pl.when((back == 1) & (c == 1))
             def _():
                 grad_sends(k, to).start()
 
@@ -265,6 +285,7 @@
         @pl.when(back == 1)
         def _():
             q_grad[me // 2] = l_send[pl.ds(at_col * nx, nx)]
+            q_line[me // 2] = l_send[at_col * nx + nx - 1]
 
         to_line(own_send, ownl, own_ss, own_rs)
 
@@ -285,14 +306,21 @@
             frm = lax.rem(at_line + k, nx)
             rcopy(xt.at[0], xtl.at[frm], xt_ss.at[k], xt_rs.at[frm], line(frm)).wait_recv()
         from_line(k_send, kl, k_ss, k_rs)
+    def pairs(parts):
+        return [jnp.concatenate(parts[i : i + 2], axis=1) for i in range(0, nx, 2)]
+
+    def to_chunks(ref, total):
+        for i in range(ny):
+            ref[i] = total[:, i * nz * rows : (i + 1) * nz * rows].astype(ref.dtype)
+
     with scope("line_m"):
-        all_rows = d_model // nx
-        turned_of = [xtl[i].reshape(all_rows, tok) for i in range(nx)]
-        m_sum = nt(turned_of[0], kl[0]) * after[0]
-        for i in range(1, nx):
-            m_sum = m_sum + nt(turned_of[i], kl[i]) * after[i]
-        m_send[...] = m_sum.reshape(ny, nz * rows, ch).astype(BF16)
-        to_column(m_send, m_recv, m_ss, m_rs)
+        turned_of = pairs([xtl[i].reshape(d_model // nx, tok) for i in range(nx)])
+        tall_after = jnp.concatenate(after + [jnp.ones((8 - nx, ch), F32)], axis=0).T
+        scaled = pairs([(kl[i].astype(F32) * tall_after[:, i : i + 1]).astype(BF16) for i in range(nx)])
+        m_sum = nt(scaled[0], turned_of[0])
+        for a, b in zip(scaled[1:], turned_of[1:]):
+            m_sum = m_sum + nt(a, b)
+        to_chunks(m_send, m_sum)
 
     def arriving(o, carried):
         frm = o + back * (nz - 1 - 2 * o)
@@ -309,6 +337,7 @@
         for k in range(1, pln):
             start(rcopy(o_send, p_buf.at[mine], p_ss.at[k], p_rs.at[mine], plane(lax.rem(me + k, pln))))
         p_buf[mine] = o_send[...]
+        to_column(m_send, m_recv, m_ss, m_rs)
 
     with scope("wait_1b"):
         for j in range(pln // 2):
@@ -317,36 +346,62 @@
             def _():
                 rcopy(l_send.at[0], q_state.at[j], q_ss.at[0], q_rs.at[2 * j], plane(2 * j)).wait_recv()
 
-            @pl.when(me != 2 * j + 1)
+            @pl.when((me != 2 * j + 1) & (c == 0))
+            def _():
+                rcopy(
+                    l_send.at[0], q_line.at[j], q_ss.at[0], q_rs.at[2 * j + 1], plane(2 * j + 1)
+                ).wait_recv()
+
+            @pl.when((me != 2 * j + 1) & (c == 1))
             def _():
                 rcopy(
                     l_send.at[pl.ds(0, nx)], q_grad.at[j], q_ss.at[0], q_rs.at[2 * j + 1], plane(2 * j + 1)
                 ).wait_recv()
 
+        @pl.when(c == 0)
+        def _():
+            from_line(r_send, rl, r_ss, r_rs)
+
+    with scope("wait_own"):
         from_line(own_send, ownl, own_ss, own_rs)
     with scope("line_a"):
         state_in = q_state[...].astype(F32).reshape(HEAD, ch)
-        a_sum, grad_in = None, None
+
+        @pl.when(c == 0)
+        def _():
+            grad_at = q_line[...].astype(F32).reshape(HEAD, ch)
+            g_all[nx - 1] = grad_at
+            for i in range(nx - 2, -1, -1):
+                grad_at = e_buf[y * nx + i + 1] * grad_at + rl[i + 1].astype(F32)
+                g_all[i] = grad_at
+
+        @pl.when(c == 1)
+        def _():
+            for i in range(nx):
+                g_all[i] = q_grad[:, i].astype(F32).reshape(HEAD, ch)
+
+        parts = []
         for i in range(nx):
-            grad_at = q_grad[:, i].astype(F32).reshape(HEAD, ch)
-            grad_in = grad_at if i == 0 else jnp.where(at_line == i, grad_at, grad_in)
+            grad_at = g_all[i]
             bd_in = by_head((grad_at * m).astype(BF16) for m in mf)
-            part = (ownl[i].astype(F32) + nn(bd_in, kl[i])).astype(BF16)
-            term = nt(turned_of[i], part)
-            a_sum = term if a_sum is None else a_sum + term
-        aacc[...] = a_sum.reshape(aacc.shape)
-        a_send[...] = a_sum.astype(BF16).reshape(a_send.shape)
+            parts.append((ownl[i].astype(F32) + nn(bd_in, kl[i])).astype(BF16))
+        parts = pairs(parts)
+        a_sum = nt(parts[0], turned_of[0])
+        for a, b in zip(parts[1:], turned_of[1:]):
+            a_sum = a_sum + nt(a, b)
+        to_chunks(aacc, a_sum)
+        to_chunks(a_send, a_sum)
         to_column(a_send, a_recv, a_ss, a_rs)
 
     with scope("wait_m"):
-        m_plane = from_column(m_send.at[at_col], m_send, m_recv, m_ss, m_rs).astype(BF16)
+        m_plane = from_column(m_send.at[at_col], m_send, m_recv, m_ss, m_rs).T.astype(BF16)
     with scope("wait3"):
         for k in range(1, pln):
             frm = lax.rem(me + k, pln)
             part = piece_of(frm)
             rcopy(o_send, p_buf.at[part], p_ss.at[k], p_rs.at[part], plane(frm)).wait_recv()
     with scope("wait_a"):
-        a_plane = from_column(aacc.at[at_col], a_send, a_recv, a_ss, a_rs)
+        a_plane = from_column(aacc.at[at_col], a_send, a_recv, a_ss, a_rs).T
     with scope("send_z"):
         outer = p_buf[...].astype(F32).reshape(2 * HEAD, ch)
         state_out, grad_out = outer[:HEAD], outer[HEAD:]
@@ -363,7 +418,7 @@
         for i in range(nx - 1):
             own_after = jnp.where(at_line == i, after[i], own_after)
         state = state_in + before * state_out
-        grad = grad_in + own_after * grad_out
+        grad = g_all[at_line] + own_after * grad_out
         bd_state = by_head((state * m).astype(BF16) for m in mf)
         bd_grad = by_head((grad * m).astype(BF16) for m in mf)
         value_grad = (gv_own + nn(bd_grad, k_end)).astype(BF16)
@@ -415,9 +470,18 @@
             def _():
                 state_sends(k, to).wait_send()
 
-            @pl.when(back == 1)
+            @pl.when((back == 1) & (c == 0))
+            def _():
+                line_sends(k, to).wait_send()
+
+            @pl.when((back == 1) & (c == 1))
             def _():
                 grad_sends(k, to).wait_send()
+
+        @pl.when(c == 0)
+        def _():
+            for k in range(1, nx):
+                reach_sends(k).wait_send()
 
         for k in range(1, nz):
 
@@ -448,21 +512,24 @@
         vm((pln, piece, ch), BF16), vm((1, ch), F32),
         vm((pln, piece, ch), BF16), vm((pln, 1, ch), F32),
         vm((pln, piece, ch), BF16), vm((pln // 2, piece, ch), BF16), vm((pln // 2, nx, piece, ch), BF16),
+        vm((pln // 2, piece, ch), BF16),
         vm((piece, ch), BF16), vm((1, ch), F32),
         vm((nz, piece, ch), BF16), vm((nz, 1, ch), F32),
         vm((piece, ch), BF16), vm((pln, piece, ch), BF16),
         vm((nx, ny, nz, rows, tok), BF16), vm((nx, ny, nz, rows, tok), BF16),
+        vm((HEAD, ch), BF16), vm((nx, HEAD, ch), BF16),
         vm((ch, tok), BF16), vm((nx, ch, tok), BF16),
         vm((ch, tok), BF16), vm((nx, ch, tok), BF16),
+        vm((nx, HEAD, ch), F32),
         vm((2, tok // 2, d_model), BF16), vm((tok // 2, d_model), BF16),
-        vm((ny, nz * rows, ch), BF16), vm((ny, nz * rows, ch), BF16),
-        vm((ny, nz * rows, ch), F32), vm((ny, nz * rows, ch), BF16), vm((ny, nz * rows, ch), BF16),
+        vm((ny, ch, nz * rows), BF16), vm((ny, ch, nz * rows), BF16),
+        vm((ny, ch, nz * rows), F32), vm((ny, ch, nz * rows), BF16), vm((ny, ch, nz * rows), BF16),
         vm((nz, rows, ch), F32), vm((nz, rows, ch), BF16), vm((nz, rows, ch), BF16),
         dma((6,)),
         dma((pln,)), dma((pln,)), dma((pln,)), dma((pln,)), dma((pln,)), dma((pln,)),
         dma((nz,)), dma((nz,)), dma((nz,)), dma((nz,)),
         dma((pln,)), dma((pln,)),
-        *(dma((nx,)) for _ in range(6)),
+        *(dma((nx,)) for _ in range(8)),
         *(dma((ny,)) for _ in range(4)),
         dma((nz,)), dma((nz,)),
         dma, dma,

time: 35.5 us -> 34.3 us (0.966)
  the two profiles are of different devices: /device:TPU:1 before, /device:TPU:6 now
where the time goes in v6:
time: 34.3 us; the launch traced here: 34.2 us
  Pallas kernels  33.6 us (98%)
  between operations  0.64 us (2%)
    pallas_call x1, Pallas kernels, on_device(): pl.pallas_call(functools.partial(kernel, nz, ny, nx), out_shape=(vm((ch,...  32.8 us
    pallas_call x1, Pallas kernels, on_device(): pl.pallas_call(write_out, out_shape=tuple((jax.ShapeDtypeStruct(a.shape,...  0.77 us

profile of v6, /device:TPU:6, one launch (start us, length us, event | category | flops | bytes accessed | tf_op | source)
XLA Modules:
  0.0 34.2 jit_solution(156414478162711997)
XLA Ops:
  0.6 32.8 %shard_map.93 = (bf16[192,128]{1,0:T(8,128)(2,1)S(1)}, bf16[192,128]{1,0:T(8,128)(2,1)S(1)}, bf16[64,2048]{1,0:T(8,128)(2,1)S(1)}, f32[16,192]{1,0:T(8,128)S(1)}) custom-call(bf16[128,2048]{1,0:T(8,128)(2,1)} %x_hbm.1, bf16[192,2048]{1,0:T(8,128)(2,1)} %bitcast.7, bf16[192,128]{1,0:T(8,128)(2,1)} %bitcast.8, bf16[192,128]{1,0:T(8,128)(2,1)} %bitcast.9, ...), custom_call_target="tpu_custom_call" | custom-call | tf_op jit(solution)/shard_map/pallas_call | solution.py:538
  33.4 0.8 %shard_map.94 = (bf16[192,128]{1,0:T(8,128)(2,1)}, bf16[192,128]{1,0:T(8,128)(2,1)}, bf16[64,2048]{1,0:T(8,128)(2,1)}, f32[16,192]{1,0:T(8,128)}) custom-call(bf16[192,128]{1,0:T(8,128)(2,1)S(1)} %get-tuple-element.12.refs_0_, bf16[192,128]{1,0:T(8,128)(2,1)S(1)} %get-tuple-element.13.refs_1_, bf16[64,2048]{1,0:T(8,128)(2,1)S(1)} %get-tuple-element.14.refs_2_, ...), custom_call_target="tpu_custom_call" | custom-call | tf_op jit(solution)/shard_map/pallas_call | solution.py:551

commit v7 on v6

--- a/solution.py
+++ b/solution.py
@@ -41,7 +41,7 @@
     s_send, e_send, s_buf, e_buf, l_send, q_state, q_grad, q_line, t_send, ft_send, t_buf, ft_buf, o_send, p_buf,
     xt, xtl, r_send, rl, k_send, kl, own_send, ownl, g_all, ig, ig_recv,
     m_send, m_recv, aacc, a_send, a_recv, w2, z_send, z_recv,
-    lsem, s_ss, s_rs, e_ss, e_rs, q_ss, q_rs, t_ss, t_rs, ft_ss, ft_rs, p_ss, p_rs,
+    lsem, s_ss, s_rs, e_ss, e_rs, ea_ss, ea_rs, q_ss, q_rs, t_ss, t_rs, ft_ss, ft_rs, p_ss, p_rs,
     xt_ss, xt_rs, r_ss, r_rs, k_ss, k_rs, own_ss, own_rs,
     m_ss, m_rs, a_ss, a_rs, z_ss, z_rs, ig_ss, ig_rs,
 ):
@@ -60,8 +60,11 @@
     def column(i):
         return (z, i * (1 - c) + y * c, x * (1 - c) + i * c, c)
 
-    def by_lines(i):
-        return i * (1 - c) + (lax.rem(i, nx) * ny + i // nx) * c
+    def spot(g, i):
+        return lax.rem(i, nx) * ny + i // nx if g else i
+
+    def owner(i):
+        return (z, i // nx, lax.rem(i, nx), 1)
 
     def piece_of(i):
         return i // 2 + lax.rem(i, 2) * (pln // 2)
@@ -77,6 +80,22 @@
 
     scope = jax.named_scope
     with scope("loads_barrier"):
+        barrier = pltpu.get_barrier_semaphore()
+
+        def greet(device):
+            pl.semaphore_signal(barrier, inc=1, device_id=device, device_id_type=LOGICAL)
+
+        for k in range(1, nz):
+            greet((lax.rem(z + k, nz), y, x, c))
+        for k in range(1, pln):
+            to = lax.rem(me + k, pln)
+            greet((z, to // nx, lax.rem(to, nx), 1 - c))
+
+            @pl.when((c == 1) | (to // nx == y) | (lax.rem(to, nx) == x))
+            def _():
+                greet(plane(to))
+
+        greet((z, y, x, 1 - c))
         loads = [
             pltpu.make_async_copy(src, dst, lsem.at[k])
             for k, (src, dst) in enumerate(
@@ -85,12 +104,6 @@
         ]
         for copy in loads:
             copy.start()
-        barrier = pltpu.get_barrier_semaphore()
-        for k in range(1, pln):
-            pl.semaphore_signal(barrier, inc=1, device_id=plane(lax.rem(me + k, pln)), device_id_type=LOGICAL)
-        for k in range(1, nz):
-            pl.semaphore_signal(barrier, inc=1, device_id=(lax.rem(z + k, nz), y, x, c), device_id_type=LOGICAL)
-        pl.semaphore_signal(barrier, inc=1, device_id=(z, y, x, 1 - c), device_id_type=LOGICAL)
 
     lane = lax.broadcasted_iota(jnp.int32, (1, ch), 1)
     mf = [jnp.where((lane >= HEAD * h) & (lane < HEAD * (h + 1)), 1.0, 0.0).astype(F32) for h in range(heads)]
@@ -156,7 +169,7 @@
                 xt[group, into, zz] = turned[rows * g : rows * (g + 1)]
 
     with scope("barrier_wait"):
-        pl.semaphore_wait(barrier, pln + nz - 1)
+        pl.semaphore_wait(barrier, pln + nz - 1 + c * (pln - 1) + (1 - c) * (nx + ny - 2))
 
     sends = []
 
@@ -190,11 +203,28 @@
         to = lax.rem(at_line + k, nx)
         return rcopy(r_send, rl.at[at_line], r_ss.at[k], r_rs.at[at_line], line(to))
 
+    def piece_sends(k):
+        to = lax.rem(me + k, pln)
+        return (
+            rcopy(e_send, e_buf.at[c, me], e_ss.at[k], e_rs.at[c, me], owner(to)),
+            rcopy(s_send.at[piece_of(to)], s_buf.at[c, me], s_ss.at[k], s_rs.at[c, me], owner(to)),
+        )
+
     with scope("send1"):
         for k in range(1, pln):
-            to = lax.rem(me + k, pln)
-            start(rcopy(e_send, e_buf.at[me], e_ss.at[k], e_rs.at[me], plane(to)))
-            start(rcopy(s_send.at[piece_of(to)], s_buf.at[me], s_ss.at[k], s_rs.at[me], plane(to)))
+            for copy in piece_sends(k):
+                start(copy)
+
+        @pl.when(c == 0)
+        def _():
+            for copy in piece_sends(0):
+                copy.start()
+
+        @pl.when(c == 1)
+        def _():
+            s_buf[1, me] = s_send[piece_of(me)]
+            e_buf[1, me] = e_send[...]
+
         for k in range(1, nx):
             to = lax.rem(at_line + k, nx)
             start(rcopy(xt.at[to], xtl.at[at_line], xt_ss.at[k], xt_rs.at[at_line], line(to)))
@@ -205,8 +235,6 @@
             for k in range(1, nx):
                 reach_sends(k).start()
 
-        s_buf[me] = s_send[piece_of(me)]
-        e_buf[me] = e_send[...]
         xtl[at_line] = xt[at_line]
         kl[at_line] = k_end
         rl[at_line] = r_send[...]
@@ -216,23 +244,7 @@
         gv_own = by_head(nn(head_of(go, h), mixing[h]) for h in range(heads))
         own_send[...] = gv_own.astype(BF16)
         ownl[at_line] = own_send[...]
-
-    with scope("wait1"):
-        for k in range(1, pln):
-            frm = lax.rem(me + k, pln)
-            rcopy(e_send, e_buf.at[frm], e_ss.at[k], e_rs.at[frm], plane(frm)).wait_recv()
-            rcopy(s_send.at[0], s_buf.at[frm], s_ss.at[k], s_rs.at[frm], plane(frm)).wait_recv()
-    with scope("scan1"):
-        held = jnp.zeros(t_send.shape, F32)
-        factor = jnp.ones((1, ch), F32)
-        for o in range(pln):
-            it = o + back * (pln - 1 - 2 * o)
-            l_send[by_lines(it)] = held.astype(BF16)
-            decay = e_buf[it]
-            held = decay * held + s_buf[it].astype(F32)
-            factor = decay * factor
-        t_send[...] = held.astype(BF16)
-        ft_send[...] = factor
+        to_line(own_send, ownl, own_ss, own_rs)
 
     z_order = z + back * (nz - 1 - 2 * z)
 
@@ -240,54 +252,66 @@
         at = z_order + k
         to = at + back * (nz - 1 - 2 * at)
         return (
-            rcopy(ft_send, ft_buf.at[z], ft_ss.at[k], ft_rs.at[z], (to, y, x, c)),
-            rcopy(t_send, t_buf.at[z], t_ss.at[k], t_rs.at[z], (to, y, x, c)),
+            rcopy(ft_send, ft_buf.at[z], ft_ss.at[k], ft_rs.at[z], (to, y, x, 1)),
+            rcopy(t_send, t_buf.at[z], t_ss.at[k], t_rs.at[z], (to, y, x, 1)),
         )
 
-    def state_sends(k, to):
-        return rcopy(l_send.at[by_lines(to)], q_state.at[me // 2], q_ss.at[k], q_rs.at[me], plane(to))
-
-    def line_sends(k, to):
-        last = to // nx * nx + nx - 1
-        return rcopy(l_send.at[last], q_line.at[me // 2], q_ss.at[k], q_rs.at[me], plane(to))
-
-    def grad_sends(k, to):
-        first = by_lines(to) // nx * nx
-        return rcopy(l_send.at[pl.ds(first, nx)], q_grad.at[me // 2], q_ss.at[k], q_rs.at[me], plane(to))
-
-    with scope("send2"):
-        for k in range(1, nz):
-
-            @pl.when(z_order + k < nz)
-            def _():
-                for copy in z_sends(k):
-                    copy.start()
-
-        for k in range(1, pln):
-            to = lax.rem(me + k, pln)
+    def carry_send(g, k, backward):
+        to = lax.rem(me + k, pln)
+        sems = (q_ss.at[g, k], q_rs.at[me], (z, to // nx, lax.rem(to, nx), g))
+        if not backward:
+            return rcopy(l_send.at[g, spot(g, to)], q_state.at[me // 2], *sems)
+        if g == 0:
+            return rcopy(l_send.at[0, to // nx * nx + nx - 1], q_line.at[me // 2], *sems)
+        return rcopy(l_send.at[1, pl.ds(lax.rem(to, nx) * ny, ny)], q_grad.at[me // 2], *sems)
+
+    targets = [(0, k) for k in range(pln)] + [(1, k) for k in range(1, pln)]
+    e_all = rcopy(e_buf.at[0], e_buf.at[0], ea_ss, ea_rs, (z, y, x, 1 - c))
+
+    @pl.when(c == 1)
+    def _():
+        with scope("wait1"):
+            for g, k in targets:
+                frm = lax.rem(me + k, pln)
+                device = (z, frm // nx, lax.rem(frm, nx), g)
+                rcopy(e_send, e_buf.at[g, frm], e_ss.at[k], e_rs.at[g, frm], device).wait_recv()
+                rcopy(s_send.at[0], s_buf.at[g, frm], s_ss.at[k], s_rs.at[g, frm], device).wait_recv()
+        with scope("scan1"):
+            for g in (0, 1):
+                held = jnp.zeros(t_send.shape[1:], F32)
+                factor = jnp.ones((1, ch), F32)
+                for o in range(pln):
+                    it = o + back * (pln - 1 - 2 * o)
+                    l_send[g, spot(g, it)] = held.astype(BF16)
+                    decay = e_buf[g, it]
+                    held = decay * held + s_buf[g, it].astype(F32)
+                    factor = decay * factor
+                t_send[g] = held.astype(BF16)
+                ft_send[g] = factor
+        with scope("send2"):
+            for k in range(1, nz):
+
+                @pl.when(z_order + k < nz)
+                def _():
+                    for copy in z_sends(k):
+                        copy.start()
+
+            for backward in (0, 1):
+
+                @pl.when(back == backward)
+                def _():
+                    for g, k in targets:
+                        carry_send(g, k, backward).start()
+
+            e_all.start()
 
             @pl.when(back == 0)
             def _():
-                state_sends(k, to).start()
-
-            @pl.when((back == 1) & (c == 0))
+                q_state[me // 2] = l_send[1, spot(1, me)]
+
+            @pl.when(back == 1)
             def _():
-                line_sends(k, to).start()
-
-            @pl.when((back == 1) & (c == 1))
-            def _():
-                grad_sends(k, to).start()
-
-        @pl.when(back == 0)
-        def _():
-            q_state[me // 2] = l_send[by_lines(me)]
-
-        @pl.when(back == 1)
-        def _():
-            q_grad[me // 2] = l_send[pl.ds(at_col * nx, nx)]
-            q_line[me // 2] = l_send[at_col * nx + nx - 1]
-
-        to_line(own_send, ownl, own_ss, own_rs)
+                q_grad[me // 2] = l_send[1, pl.ds(x * ny, ny)]
 
     with scope("pairs_query"):
         pairing = [jnp.where(upper, tn(head_of(v, h), head_of(go, h)), 0.0).astype(BF16) for h in range(heads)]
@@ -295,11 +319,16 @@
         gk_own = by_head(nt(head_of(q_dec, h), pairing[h]) for h in range(heads))
 
     with scope("decays"):
+        @pl.when(c == 0)
+        def _():
+            e_all.wait_recv()
+
+        decays = e_buf[c]
         before, after = jnp.ones((1, ch), F32), [jnp.ones((1, ch), F32)] * nx
         ids = [line(i)[1] * nx + line(i)[2] for i in range(nx)]
         for i in range(pln):
-            before = before * jnp.where(i < me, e_buf[i], 1.0)
-            after = [a * jnp.where(i > n, e_buf[i], 1.0) for a, n in zip(after, ids)]
+            before = before * jnp.where(i < me, decays[i], 1.0)
+            after = [a * jnp.where(i > n, decays[i], 1.0) for a, n in zip(after, ids)]
 
     with scope("wait_line"):
         for k in range(1, nx):
@@ -324,38 +353,47 @@
 
     def arriving(o, carried):
         frm = o + back * (nz - 1 - 2 * o)
-        rcopy(ft_send, ft_buf.at[frm], ft_ss.at[0], ft_rs.at[frm], (z, y, x, c)).wait_recv()
-        rcopy(t_send, t_buf.at[frm], t_ss.at[0], t_rs.at[frm], (z, y, x, c)).wait_recv()
+        rcopy(ft_send, ft_buf.at[frm], ft_ss.at[0], ft_rs.at[frm], (frm, y, x, 1)).wait_recv()
+        rcopy(t_send, t_buf.at[frm], t_ss.at[0], t_rs.at[frm], (frm, y, x, 1)).wait_recv()
         return ft_buf[frm] * carried + t_buf[frm].astype(F32)
 
-    with scope("wait2"):
-        carried = lax.fori_loop(0, z_order, arriving, jnp.zeros(t_send.shape, F32))
-
-    with scope("send3"):
-        o_send[...] = carried.astype(BF16)
-        mine = piece_of(me)
-        for k in range(1, pln):
-            start(rcopy(o_send, p_buf.at[mine], p_ss.at[k], p_rs.at[mine], plane(lax.rem(me + k, pln))))
-        p_buf[mine] = o_send[...]
+    mine = piece_of(me)
+
+    def plane_send(g, k):
+        to = lax.rem(me + k, pln)
+        device = (z, to // nx, lax.rem(to, nx), g)
+        return rcopy(o_send.at[g], p_buf.at[mine], p_ss.at[g, k], p_rs.at[mine], device)
+
+    @pl.when(c == 1)
+    def _():
+        with scope("wait2"):
+            carried = lax.fori_loop(0, z_order, arriving, jnp.zeros(t_send.shape, F32))
+        with scope("send3"):
+            o_send[...] = carried.astype(BF16)
+            for g, k in targets:
+                plane_send(g, k).start()
+            p_buf[mine] = o_send[1]
+
+    with scope("send_m"):
         to_column(m_send, m_recv, m_ss, m_rs)
 
     with scope("wait_1b"):
         for j in range(pln // 2):
 
-            @pl.when(me != 2 * j)
+            @pl.when((me != 2 * j) | (c == 0))
             def _():
-                rcopy(l_send.at[0], q_state.at[j], q_ss.at[0], q_rs.at[2 * j], plane(2 * j)).wait_recv()
-
-            @pl.when((me != 2 * j + 1) & (c == 0))
+                rcopy(l_send.at[0, 0], q_state.at[j], q_ss.at[0, 0], q_rs.at[2 * j], owner(2 * j)).wait_recv()
+
+            @pl.when(c == 0)
             def _():
                 rcopy(
-                    l_send.at[0], q_line.at[j], q_ss.at[0], q_rs.at[2 * j + 1], plane(2 * j + 1)
+                    l_send.at[0, 0], q_line.at[j], q_ss.at[0, 0], q_rs.at[2 * j + 1], owner(2 * j + 1)
                 ).wait_recv()
 
             @pl.when((me != 2 * j + 1) & (c == 1))
             def _():
                 rcopy(
-                    l_send.at[pl.ds(0, nx)], q_grad.at[j], q_ss.at[0], q_rs.at[2 * j + 1], plane(2 * j + 1)
+                    l_send.at[0, pl.ds(0, ny)], q_grad.at[j], q_ss.at[0, 0], q_rs.at[2 * j + 1], owner(2 * j + 1)
                 ).wait_recv()
 
         @pl.when(c == 0)
@@ -372,7 +410,7 @@
             grad_at = q_line[...].astype(F32).reshape(HEAD, ch)
             g_all[nx - 1] = grad_at
             for i in range(nx - 2, -1, -1):
-                grad_at = e_buf[y * nx + i + 1] * grad_at + rl[i + 1].astype(F32)
+                grad_at = e_buf[0, y * nx + i + 1] * grad_at + rl[i + 1].astype(F32)
                 g_all[i] = grad_at
 
         @pl.when(c == 1)
@@ -399,7 +437,11 @@
         for k in range(1, pln):
             frm = lax.rem(me + k, pln)
             part = piece_of(frm)
-            rcopy(o_send, p_buf.at[part], p_ss.at[k], p_rs.at[part], plane(frm)).wait_recv()
+            rcopy(o_send.at[0], p_buf.at[part], p_ss.at[0, k], p_rs.at[part], owner(frm)).wait_recv()
+
+        @pl.when(c == 0)
+        def _():
+            rcopy(o_send.at[0], p_buf.at[mine], p_ss.at[0, 0], p_rs.at[mine], owner(me)).wait_recv()
     with scope("wait_a"):
         a_plane = from_column(aacc.at[at_col], a_send, a_recv, a_ss, a_rs).T
     with scope("send_z"):
@@ -451,6 +493,38 @@
         ig_copy.wait_recv()
         gx_out[...] = (ig[c].astype(F32) + ig_recv[...].astype(F32)).astype(BF16)
 
+    with scope("drain"):
+        for copy in sends[: 1 - nz]:
+            copy.wait_send()
+        ig_copy.wait_send()
+
+        @pl.when(c == 0)
+        def _():
+            for copy in piece_sends(0):
+                copy.wait_send()
+            for k in range(1, nx):
+                reach_sends(k).wait_send()
+
+        @pl.when(c == 1)
+        def _():
+            for k in range(1, nz):
+
+                @pl.when(z_order + k < nz)
+                def _():
+                    for copy in z_sends(k):
+                        copy.wait_send()
+
+            for backward in (0, 1):
+
+                @pl.when(back == backward)
+                def _():
+                    for g, k in targets:
+                        carry_send(g, k, backward).wait_send()
+
+            e_all.wait_send()
+            for g, k in targets:
+                plane_send(g, k).wait_send()
+
     with scope("wait_z"):
         w_last = w2[z]
         for k in range(1, nz):
@@ -458,37 +532,8 @@
             rcopy(z_send.at[0], z_recv.at[frm], z_ss.at[k], z_rs.at[frm], (frm, y, x, c)).wait_recv()
             w_last = w_last + z_recv[frm].astype(F32)
         gw_out[...] = w_last
-
-    with scope("drain"):
-        for copy in sends:
+        for copy in sends[1 - nz :]:
             copy.wait_send()
-        ig_copy.wait_send()
-        for k in range(1, pln):
-            to = lax.rem(me + k, pln)
-
-            @pl.when(back == 0)
-            def _():
-                state_sends(k, to).wait_send()
-
-            @pl.when((back == 1) & (c == 0))
-            def _():
-                line_sends(k, to).wait_send()
-
-            @pl.when((back == 1) & (c == 1))
-            def _():
-                grad_sends(k, to).wait_send()
-
-        @pl.when(c == 0)
-        def _():
-            for k in range(1, nx):
-                reach_sends(k).wait_send()
-
-        for k in range(1, nz):
-
-            @pl.when(z_order + k < nz)
-            def _():
-                for copy in z_sends(k):
-                    copy.wait_send()
 
 
 def write_out(*refs):
@@ -510,12 +555,12 @@
         vm((tok, d_model), BF16), vm((ch, d_model), BF16),
         vm((ch, tok), BF16), vm((ch, tok), BF16), vm((ch, tok), BF16), vm((1, ch), F32),
         vm((pln, piece, ch), BF16), vm((1, ch), F32),
-        vm((pln, piece, ch), BF16), vm((pln, 1, ch), F32),
-        vm((pln, piece, ch), BF16), vm((pln // 2, piece, ch), BF16), vm((pln // 2, nx, piece, ch), BF16),
+        vm((2, pln, piece, ch), BF16), vm((2, pln, 1, ch), F32),
+        vm((2, pln, piece, ch), BF16), vm((pln // 2, piece, ch), BF16), vm((pln // 2, nx, piece, ch), BF16),
         vm((pln // 2, piece, ch), BF16),
-        vm((piece, ch), BF16), vm((1, ch), F32),
-        vm((nz, piece, ch), BF16), vm((nz, 1, ch), F32),
-        vm((piece, ch), BF16), vm((pln, piece, ch), BF16),
+        vm((2, piece, ch), BF16), vm((2, 1, ch), F32),
+        vm((nz, 2, piece, ch), BF16), vm((nz, 2, 1, ch), F32),
+        vm((2, piece, ch), BF16), vm((pln, piece, ch), BF16),
         vm((nx, ny, nz, rows, tok), BF16), vm((nx, ny, nz, rows, tok), BF16),
         vm((HEAD, ch), BF16), vm((nx, HEAD, ch), BF16),
         vm((ch, tok), BF16), vm((nx, ch, tok), BF16),
@@ -526,9 +571,9 @@
         vm((ny, ch, nz * rows), F32), vm((ny, ch, nz * rows), BF16), vm((ny, ch, nz * rows), BF16),
         vm((nz, rows, ch), F32), vm((nz, rows, ch), BF16), vm((nz, rows, ch), BF16),
         dma((6,)),
-        dma((pln,)), dma((pln,)), dma((pln,)), dma((pln,)), dma((pln,)), dma((pln,)),
+        dma((pln,)), dma((2, pln)), dma((pln,)), dma((2, pln)), dma, dma, dma((2, pln)), dma((pln,)),
         dma((nz,)), dma((nz,)), dma((nz,)), dma((nz,)),
-        dma((pln,)), dma((pln,)),
+        dma((2, pln)), dma((pln,)),
         *(dma((nx,)) for _ in range(8)),
         *(dma((ny,)) for _ in range(4)),
         dma((nz,)), dma((nz,)),

time: 34.3 us -> 34.1 us (level)
  the two profiles are of different devices: /device:TPU:6 before, /device:TPU:1 now
where the time goes in v7:
time: 34.1 us; the launch traced here: 34 us
  Pallas kernels  33.3 us (98%)
  between operations  0.64 us (2%)
    pallas_call x1, Pallas kernels, on_device(): pl.pallas_call(functools.partial(kernel, nz, ny, nx), out_shape=(vm((ch,...  32.5 us
    pallas_call x1, Pallas kernels, on_device(): pl.pallas_call(write_out, out_shape=tuple((jax.ShapeDtypeStruct(a.shape,...  0.77 us

profile of v7, /device:TPU:1, one launch (start us, length us, event | category | flops | bytes accessed | tf_op | source)
XLA Modules:
  0.0 34.0 jit_solution(15729211252888714982)
XLA Ops:
  0.6 32.5 %shard_map.93 = (bf16[192,128]{1,0:T(8,128)(2,1)S(1)}, bf16[192,128]{1,0:T(8,128)(2,1)S(1)}, bf16[64,2048]{1,0:T(8,128)(2,1)S(1)}, f32[16,192]{1,0:T(8,128)S(1)}) custom-call(bf16[128,2048]{1,0:T(8,128)(2,1)} %x_hbm.1, bf16[192,2048]{1,0:T(8,128)(2,1)} %bitcast.7, bf16[192,128]{1,0:T(8,128)(2,1)} %bitcast.8, bf16[192,128]{1,0:T(8,128)(2,1)} %bitcast.9, ...), custom_call_target="tpu_custom_call" | custom-call | tf_op jit(solution)/shard_map/pallas_call | solution.py:583
  33.2 0.8 %shard_map.94 = (bf16[192,128]{1,0:T(8,128)(2,1)}, bf16[192,128]{1,0:T(8,128)(2,1)}, bf16[64,2048]{1,0:T(8,128)(2,1)}, f32[16,192]{1,0:T(8,128)}) custom-call(bf16[192,128]{1,0:T(8,128)(2,1)S(1)} %get-tuple-element.12.refs_0_, bf16[192,128]{1,0:T(8,128)(2,1)S(1)} %get-tuple-element.13.refs_1_, bf16[64,2048]{1,0:T(8,128)(2,1)S(1)} %get-tuple-element.14.refs_2_, ...), custom_call_target="tpu_custom_call" | custom-call | tf_op jit(solution)/shard_map/pallas_call | solution.py:596

commit v8 on v7

--- a/solution.py
+++ b/solution.py
@@ -37,7 +37,7 @@
     nz, ny, nx,
     x_hbm, w_hbm, q_hbm, f_hbm, go_hbm, lb_hbm,
     gq_out, gf_out, gx_out, gw_out,
-    x_v, w_v, q_v, f_v, go_v, lb_v,
+    x_v, w_v, q_v, f_v, go_v, lb_v, wide, thin,
     s_send, e_send, s_buf, e_buf, l_send, q_state, q_grad, q_line, t_send, ft_send, t_buf, ft_buf, o_send, p_buf,
     xt, xtl, r_send, rl, k_send, kl, own_send, ownl, g_all, ig, ig_recv,
     m_send, m_recv, aacc, a_send, a_recv, w2, z_send, z_recv,
@@ -77,6 +77,14 @@
 
     def by_head(parts):
         return jnp.concatenate(list(parts), axis=0)
+
+    def arrived(ref, n, sem):
+        part = ref.at[pl.ds(0, n)]
+        rcopy(part, part, sem, sem, (z, y, x, 1 - c)).wait_recv()
+
+    def left(ref, n, sem):
+        part = ref.at[pl.ds(0, n)]
+        rcopy(part, part, sem, sem, (z, y, x, 1 - c)).wait_send()
 
     scope = jax.named_scope
     with scope("loads_barrier"):
@@ -171,49 +179,33 @@
     with scope("barrier_wait"):
         pl.semaphore_wait(barrier, pln + nz - 1 + c * (pln - 1) + (1 - c) * (nx + ny - 2))
 
-    sends = []
-
-    def start(copy):
-        copy.start()
-        sends.append(copy)
-
     def to_line(source, target, send_sem, recv_sem):
         for k in range(1, nx):
-            start(rcopy(source, target.at[at_line], send_sem.at[k], recv_sem.at[at_line], line(lax.rem(at_line + k, nx))))
-
-    def from_line(source, target, send_sem, recv_sem):
-        for k in range(1, nx):
-            frm = lax.rem(at_line + k, nx)
-            rcopy(source, target.at[frm], send_sem.at[k], recv_sem.at[frm], line(frm)).wait_recv()
+            rcopy(source, target.at[at_line], send_sem, recv_sem, line(lax.rem(at_line + k, nx))).start()
 
     def to_column(source, target, send_sem, recv_sem):
         for k in range(1, ny):
             to = lax.rem(at_col + k, ny)
-            start(rcopy(source.at[to], target.at[at_col], send_sem.at[k], recv_sem.at[at_col], column(to)))
-
-    def from_column(own, source, target, send_sem, recv_sem):
+            rcopy(source.at[to], target.at[at_col], send_sem, recv_sem, column(to)).start()
+
+    def from_column(own, target, recv_sem):
+        arrived(target, ny - 1, recv_sem)
         out = own[...].astype(F32)
         for k in range(1, ny):
-            frm = lax.rem(at_col + k, ny)
-            rcopy(source.at[0], target.at[frm], send_sem.at[k], recv_sem.at[frm], column(frm)).wait_recv()
-            out = out + target[frm].astype(F32)
+            out = out + target[lax.rem(at_col + k, ny)].astype(F32)
         return out
-
-    def reach_sends(k):
-        to = lax.rem(at_line + k, nx)
-        return rcopy(r_send, rl.at[at_line], r_ss.at[k], r_rs.at[at_line], line(to))
 
     def piece_sends(k):
         to = lax.rem(me + k, pln)
         return (
-            rcopy(e_send, e_buf.at[c, me], e_ss.at[k], e_rs.at[c, me], owner(to)),
-            rcopy(s_send.at[piece_of(to)], s_buf.at[c, me], s_ss.at[k], s_rs.at[c, me], owner(to)),
+            rcopy(e_send, e_buf.at[c * pln + me], e_ss, e_rs, owner(to)),
+            rcopy(s_send.at[piece_of(to)], s_buf.at[c * pln + me], s_ss, s_rs, owner(to)),
         )
 
     with scope("send1"):
         for k in range(1, pln):
             for copy in piece_sends(k):
-                start(copy)
+                copy.start()
 
         @pl.when(c == 0)
         def _():
@@ -222,18 +214,17 @@
 
         @pl.when(c == 1)
         def _():
-            s_buf[1, me] = s_send[piece_of(me)]
-            e_buf[1, me] = e_send[...]
+            s_buf[pln + me] = s_send[piece_of(me)]
+            e_buf[pln + me] = e_send[...]
 
         for k in range(1, nx):
             to = lax.rem(at_line + k, nx)
-            start(rcopy(xt.at[to], xtl.at[at_line], xt_ss.at[k], xt_rs.at[at_line], line(to)))
+            rcopy(xt.at[to], xtl.at[at_line], xt_ss, xt_rs, line(to)).start()
         to_line(k_send, kl, k_ss, k_rs)
 
         @pl.when(c == 0)
         def _():
-            for k in range(1, nx):
-                reach_sends(k).start()
+            to_line(r_send, rl, r_ss, r_rs)
 
         xtl[at_line] = xt[at_line]
         kl[at_line] = k_end
@@ -252,39 +243,38 @@
         at = z_order + k
         to = at + back * (nz - 1 - 2 * at)
         return (
-            rcopy(ft_send, ft_buf.at[z], ft_ss.at[k], ft_rs.at[z], (to, y, x, 1)),
-            rcopy(t_send, t_buf.at[z], t_ss.at[k], t_rs.at[z], (to, y, x, 1)),
+            rcopy(ft_send, ft_buf.at[z], ft_ss, ft_rs, (to, y, x, 1)),
+            rcopy(t_send, t_buf.at[z], t_ss, t_rs, (to, y, x, 1)),
         )
 
     def carry_send(g, k, backward):
         to = lax.rem(me + k, pln)
-        sems = (q_ss.at[g, k], q_rs.at[me], (z, to // nx, lax.rem(to, nx), g))
+        device = (z, to // nx, lax.rem(to, nx), g)
         if not backward:
-            return rcopy(l_send.at[g, spot(g, to)], q_state.at[me // 2], *sems)
+            return rcopy(l_send.at[g * pln + spot(g, to)], q_state.at[me // 2], q_ss.at[g], q_rs.at[0], device)
         if g == 0:
-            return rcopy(l_send.at[0, to // nx * nx + nx - 1], q_line.at[me // 2], *sems)
-        return rcopy(l_send.at[1, pl.ds(lax.rem(to, nx) * ny, ny)], q_grad.at[me // 2], *sems)
+            return rcopy(l_send.at[to // nx * nx + nx - 1], q_line.at[me // 2], q_ss.at[0], q_rs.at[1], device)
+        first = pln + lax.rem(to, nx) * ny
+        return rcopy(l_send.at[pl.ds(first, ny)], q_grad.at[pl.ds(me // 2 * ny, ny)], q_ss.at[1], q_rs.at[1], device)
 
     targets = [(0, k) for k in range(pln)] + [(1, k) for k in range(1, pln)]
-    e_all = rcopy(e_buf.at[0], e_buf.at[0], ea_ss, ea_rs, (z, y, x, 1 - c))
+    plane_decays = e_buf.at[pl.ds(0, pln)]
+    e_all = rcopy(plane_decays, plane_decays, ea_ss, ea_rs, (z, y, x, 1 - c))
 
     @pl.when(c == 1)
     def _():
         with scope("wait1"):
-            for g, k in targets:
-                frm = lax.rem(me + k, pln)
-                device = (z, frm // nx, lax.rem(frm, nx), g)
-                rcopy(e_send, e_buf.at[g, frm], e_ss.at[k], e_rs.at[g, frm], device).wait_recv()
-                rcopy(s_send.at[0], s_buf.at[g, frm], s_ss.at[k], s_rs.at[g, frm], device).wait_recv()
+            arrived(e_buf, 2 * pln - 1, e_rs)
+            arrived(s_buf, 2 * pln - 1, s_rs)
         with scope("scan1"):
             for g in (0, 1):
                 held = jnp.zeros(t_send.shape[1:], F32)
                 factor = jnp.ones((1, ch), F32)
                 for o in range(pln):
                     it = o + back * (pln - 1 - 2 * o)
-                    l_send[g, spot(g, it)] = held.astype(BF16)
-                    decay = e_buf[g, it]
-                    held = decay * held + s_buf[g, it].astype(F32)
+                    l_send[g * pln + spot(g, it)] = held.astype(BF16)
+                    decay = e_buf[g * pln + it]
+                    held = decay * held + s_buf[g * pln + it].astype(F32)
                     factor = decay * factor
                 t_send[g] = held.astype(BF16)
                 ft_send[g] = factor
@@ -307,11 +297,11 @@
 
             @pl.when(back == 0)
             def _():
-                q_state[me // 2] = l_send[1, spot(1, me)]
+                q_state[me // 2] = l_send[pln + spot(1, me)]
 
             @pl.when(back == 1)
             def _():
-                q_grad[me // 2] = l_send[1, pl.ds(x * ny, ny)]
+                q_grad[pl.ds(me // 2 * ny, ny)] = l_send[pl.ds(pln + x * ny, ny)]
 
     with scope("pairs_query"):
         pairing = [jnp.where(upper, tn(head_of(v, h), head_of(go, h)), 0.0).astype(BF16) for h in range(heads)]
@@ -323,7 +313,7 @@
         def _():
             e_all.wait_recv()
 
-        decays = e_buf[c]
+        decays = e_buf[pl.ds(c * pln, pln)]
         before, after = jnp.ones((1, ch), F32), [jnp.ones((1, ch), F32)] * nx
         ids = [line(i)[1] * nx + line(i)[2] for i in range(nx)]
         for i in range(pln):
@@ -331,10 +321,9 @@
             after = [a * jnp.where(i > n, decays[i], 1.0) for a, n in zip(after, ids)]
 
     with scope("wait_line"):
-        for k in range(1, nx):
-            frm = lax.rem(at_line + k, nx)
-            rcopy(xt.at[0], xtl.at[frm], xt_ss.at[k], xt_rs.at[frm], line(frm)).wait_recv()
-        from_line(k_send, kl, k_ss, k_rs)
+        arrived(xtl, nx - 1, xt_rs)
+        arrived(kl, nx - 1, k_rs)
+
     def pairs(parts):
         return [jnp.concatenate(parts[i : i + 2], axis=1) for i in range(0, nx, 2)]
 
@@ -353,8 +342,6 @@
 
     def arriving(o, carried):
         frm = o + back * (nz - 1 - 2 * o)
-        rcopy(ft_send, ft_buf.at[frm], ft_ss.at[0], ft_rs.at[frm], (frm, y, x, 1)).wait_recv()
-        rcopy(t_send, t_buf.at[frm], t_ss.at[0], t_rs.at[frm], (frm, y, x, 1)).wait_recv()
         return ft_buf[frm] * carried + t_buf[frm].astype(F32)
 
     mine = piece_of(me)
@@ -362,11 +349,18 @@
     def plane_send(g, k):
         to = lax.rem(me + k, pln)
         device = (z, to // nx, lax.rem(to, nx), g)
-        return rcopy(o_send.at[g], p_buf.at[mine], p_ss.at[g, k], p_rs.at[mine], device)
+        return rcopy(o_send.at[g], p_buf.at[mine], p_ss, p_rs, device)
 
     @pl.when(c == 1)
     def _():
         with scope("wait2"):
+            for n in range(1, nz):
+
+                @pl.when(z_order == n)
+                def _():
+                    arrived(ft_buf, n, ft_rs)
+                    arrived(t_buf, n, t_rs)
+
             carried = lax.fori_loop(0, z_order, arriving, jnp.zeros(t_send.shape, F32))
         with scope("send3"):
             o_send[...] = carried.astype(BF16)
@@ -377,31 +371,27 @@
     with scope("send_m"):
         to_column(m_send, m_recv, m_ss, m_rs)
 
+    some = pln // 2
     with scope("wait_1b"):
-        for j in range(pln // 2):
-
-            @pl.when((me != 2 * j) | (c == 0))
-            def _():
-                rcopy(l_send.at[0, 0], q_state.at[j], q_ss.at[0, 0], q_rs.at[2 * j], owner(2 * j)).wait_recv()
-
-            @pl.when(c == 0)
-            def _():
-                rcopy(
-                    l_send.at[0, 0], q_line.at[j], q_ss.at[0, 0], q_rs.at[2 * j + 1], owner(2 * j + 1)
-                ).wait_recv()
-
-            @pl.when((me != 2 * j + 1) & (c == 1))
-            def _():
-                rcopy(
-                    l_send.at[0, pl.ds(0, ny)], q_grad.at[j], q_ss.at[0, 0], q_rs.at[2 * j + 1], owner(2 * j + 1)
-                ).wait_recv()
 
         @pl.when(c == 0)
         def _():
-            from_line(r_send, rl, r_ss, r_rs)
+            arrived(q_state, some, q_rs.at[0])
+            arrived(q_line, some, q_rs.at[1])
+            arrived(rl, nx - 1, r_rs)
+
+        @pl.when((c == 1) & (back == 0))
+        def _():
+            arrived(q_state, some - 1, q_rs.at[0])
+            arrived(q_grad, some * ny, q_rs.at[1])
+
+        @pl.when((c == 1) & (back == 1))
+        def _():
+            arrived(q_state, some, q_rs.at[0])
+            arrived(q_grad, (some - 1) * ny, q_rs.at[1])
 
     with scope("wait_own"):
-        from_line(own_send, ownl, own_ss, own_rs)
+        arrived(ownl, nx - 1, own_rs)
     with scope("line_a"):
         state_in = q_state[...].astype(F32).reshape(HEAD, ch)
 
@@ -410,13 +400,14 @@
             grad_at = q_line[...].astype(F32).reshape(HEAD, ch)
             g_all[nx - 1] = grad_at
             for i in range(nx - 2, -1, -1):
-                grad_at = e_buf[0, y * nx + i + 1] * grad_at + rl[i + 1].astype(F32)
+                grad_at = e_buf[y * nx + i + 1] * grad_at + rl[i + 1].astype(F32)
                 g_all[i] = grad_at
 
         @pl.when(c == 1)
         def _():
             for i in range(nx):
-                g_all[i] = q_grad[:, i].astype(F32).reshape(HEAD, ch)
+                part = [q_grad[j * ny + i].astype(F32) for j in range(some)]
+                g_all[i] = jnp.concatenate(part, axis=0)
 
         parts = []
         for i in range(nx):
@@ -432,18 +423,16 @@
         to_column(a_send, a_recv, a_ss, a_rs)
 
     with scope("wait_m"):
-        m_plane = from_column(m_send.at[at_col], m_send, m_recv, m_ss, m_rs).T.astype(BF16)
+        m_plane = from_column(m_send.at[at_col], m_recv, m_rs).T.astype(BF16)
     with scope("wait3"):
-        for k in range(1, pln):
-            frm = lax.rem(me + k, pln)
-            part = piece_of(frm)
-            rcopy(o_send.at[0], p_buf.at[part], p_ss.at[0, k], p_rs.at[part], owner(frm)).wait_recv()
-
-        @pl.when(c == 0)
-        def _():
-            rcopy(o_send.at[0], p_buf.at[mine], p_ss.at[0, 0], p_rs.at[mine], owner(me)).wait_recv()
+        for core in (0, 1):
+
+            @pl.when(c == core)
+            def _():
+                arrived(p_buf, pln - core, p_rs)
+
     with scope("wait_a"):
-        a_plane = from_column(aacc.at[at_col], a_send, a_recv, a_ss, a_rs).T
+        a_plane = from_column(aacc.at[at_col], a_recv, a_rs).T
     with scope("send_z"):
         outer = p_buf[...].astype(F32).reshape(2 * HEAD, ch)
         state_out, grad_out = outer[:HEAD], outer[HEAD:]
@@ -453,7 +442,7 @@
         z_send[...] = w_sum.astype(BF16).reshape(z_send.shape)
         for k in range(1, nz):
             to = lax.rem(z + k, nz)
-            start(rcopy(z_send.at[to], z_recv.at[z], z_ss.at[k], z_rs.at[z], (to, y, x, c)))
+            rcopy(z_send.at[to], z_recv.at[z], z_ss, z_rs, (to, y, x, c)).start()
 
     with scope("value_grad"):
         own_after = after[nx - 1]
@@ -494,46 +483,47 @@
         gx_out[...] = (ig[c].astype(F32) + ig_recv[...].astype(F32)).astype(BF16)
 
     with scope("drain"):
-        for copy in sends[: 1 - nz]:
-            copy.wait_send()
+        left(xt, nx - 1, xt_ss)
+        left(kl, nx - 1, k_ss)
+        left(ownl, nx - 1, own_ss)
+        left(m_send, ny - 1, m_ss)
+        left(a_send, ny - 1, a_ss)
         ig_copy.wait_send()
 
         @pl.when(c == 0)
         def _():
-            for copy in piece_sends(0):
-                copy.wait_send()
-            for k in range(1, nx):
-                reach_sends(k).wait_send()
+            left(thin, pln, e_ss)
+            left(s_send, pln, s_ss)
+            left(rl, nx - 1, r_ss)
 
         @pl.when(c == 1)
         def _():
-            for k in range(1, nz):
-
-                @pl.when(z_order + k < nz)
+            left(thin, pln - 1, e_ss)
+            left(s_send, pln - 1, s_ss)
+            for n in range(1, nz):
+
+                @pl.when(nz - 1 - z_order == n)
                 def _():
-                    for copy in z_sends(k):
-                        copy.wait_send()
-
+                    left(ft_buf, n, ft_ss)
+                    left(t_buf, n, t_ss)
+
+            left(wide, pln, q_ss.at[0])
             for backward in (0, 1):
 
                 @pl.when(back == backward)
                 def _():
-                    for g, k in targets:
-                        carry_send(g, k, backward).wait_send()
+                    left(wide, (pln - 1) * (ny if backward else 1), q_ss.at[1])
 
             e_all.wait_send()
-            for g, k in targets:
-                plane_send(g, k).wait_send()
+            left(wide, 2 * pln - 1, p_ss)
 
     with scope("wait_z"):
+        arrived(z_recv, nz - 1, z_rs)
         w_last = w2[z]
         for k in range(1, nz):
-            frm = lax.rem(z + k, nz)
-            rcopy(z_send.at[0], z_recv.at[frm], z_ss.at[k], z_rs.at[frm], (frm, y, x, c)).wait_recv()
-            w_last = w_last + z_recv[frm].astype(F32)
+            w_last = w_last + z_recv[lax.rem(z + k, nz)].astype(F32)
         gw_out[...] = w_last
-        for copy in sends[1 - nz :]:
-            copy.wait_send()
+        left(z_send, nz - 1, z_ss)
 
 
 def write_out(*refs):
@@ -554,9 +544,10 @@
     scratch = [
         vm((tok, d_model), BF16), vm((ch, d_model), BF16),
         vm((ch, tok), BF16), vm((ch, tok), BF16), vm((ch, tok), BF16), vm((1, ch), F32),
+        vm((pln * ny, piece, ch), BF16), vm((pln, 1, ch), F32),
         vm((pln, piece, ch), BF16), vm((1, ch), F32),
-        vm((2, pln, piece, ch), BF16), vm((2, pln, 1, ch), F32),
-        vm((2, pln, piece, ch), BF16), vm((pln // 2, piece, ch), BF16), vm((pln // 2, nx, piece, ch), BF16),
+        vm((2 * pln, piece, ch), BF16), vm((2 * pln, 1, ch), F32),
+        vm((2 * pln, piece, ch), BF16), vm((pln // 2, piece, ch), BF16), vm((pln // 2 * ny, piece, ch), BF16),
         vm((pln // 2, piece, ch), BF16),
         vm((2, piece, ch), BF16), vm((2, 1, ch), F32),
         vm((nz, 2, piece, ch), BF16), vm((nz, 2, 1, ch), F32),
@@ -571,13 +562,8 @@
         vm((ny, ch, nz * rows), F32), vm((ny, ch, nz * rows), BF16), vm((ny, ch, nz * rows), BF16),
         vm((nz, rows, ch), F32), vm((nz, rows, ch), BF16), vm((nz, rows, ch), BF16),
         dma((6,)),
-        dma((pln,)), dma((2, pln)), dma((pln,)), dma((2, pln)), dma, dma, dma((2, pln)), dma((pln,)),
-        dma((nz,)), dma((nz,)), dma((nz,)), dma((nz,)),
-        dma((2, pln)), dma((pln,)),
-        *(dma((nx,)) for _ in range(8)),
-        *(dma((ny,)) for _ in range(4)),
-        dma((nz,)), dma((nz,)),
-        dma, dma,
+        *(dma for _ in range(6)), dma((2,)), dma((2,)),
+        *(dma for _ in range(4 + 2 + 8 + 4 + 2 + 2)),
     ]
     hbm, near = pl.BlockSpec(memory_space=pl.ANY), pl.BlockSpec(memory_space=pltpu.VMEM)
     results = pl.pallas_call(

time: 34.1 us -> 31.6 us (0.927)
  Pallas kernels: 33.3 us -> 30.9 us
    pallas_call x1, Pallas kernels: 32.5 us -> 30.1 us  [on_device(): pl.pallas_call(functools.partial(kernel, nz, ny, nx), out_shape=(vm((ch,...]
where the time goes in v8:
time: 31.6 us; the launch traced here: 31.5 us
  Pallas kernels  30.9 us (98%)
  between operations  0.64 us (2%)
    pallas_call x1, Pallas kernels, on_device(): pl.pallas_call(functools.partial(kernel, nz, ny, nx), out_shape=(vm((ch,...  30.1 us
    pallas_call x1, Pallas kernels, on_device(): pl.pallas_call(write_out, out_shape=tuple((jax.ShapeDtypeStruct(a.shape,...  0.77 us

profile of v8, /device:TPU:1, one launch (start us, length us, event | category | flops | bytes accessed | tf_op | source)
XLA Modules:
  0.0 31.5 jit_solution(16039006074196441236)
XLA Ops:
  0.6 30.1 %shard_map.93 = (bf16[192,128]{1,0:T(8,128)(2,1)S(1)}, bf16[192,128]{1,0:T(8,128)(2,1)S(1)}, bf16[64,2048]{1,0:T(8,128)(2,1)S(1)}, f32[16,192]{1,0:T(8,128)S(1)}) custom-call(bf16[128,2048]{1,0:T(8,128)(2,1)} %x_hbm.1, bf16[192,2048]{1,0:T(8,128)(2,1)} %bitcast.7, bf16[192,128]{1,0:T(8,128)(2,1)} %bitcast.8, bf16[192,128]{1,0:T(8,128)(2,1)} %bitcast.9, ...), custom_call_target="tpu_custom_call" | custom-call | tf_op jit(solution)/shard_map/pallas_call | solution.py:569
  30.7 0.8 %shard_map.94 = (bf16[192,128]{1,0:T(8,128)(2,1)}, bf16[192,128]{1,0:T(8,128)(2,1)}, bf16[64,2048]{1,0:T(8,128)(2,1)}, f32[16,192]{1,0:T(8,128)}) custom-call(bf16[192,128]{1,0:T(8,128)(2,1)S(1)} %get-tuple-element.12.refs_0_, bf16[192,128]{1,0:T(8,128)(2,1)S(1)} %get-tuple-element.13.refs_1_, bf16[64,2048]{1,0:T(8,128)(2,1)S(1)} %get-tuple-element.14.refs_2_, ...), custom_call_target="tpu_custom_call" | custom-call | tf_op jit(solution)/shard_map/pallas_call | solution.py:582

commit v9 on v8

--- a/solution.py
+++ b/solution.py
@@ -52,7 +52,17 @@
     z, y, x, c = (lax.axis_index(a) for a in SP_TP)
     me = y * nx + x
     back = lax.rem(me, 2)
+    zs, ys, xs = ([lax.rem(at + d, n) for d in range(n)] for at, n in ((z, nz), (y, ny), (x, nx)))
+    across = lambda d, n: min(d, n - d)
+    steps = [(dy, dx) for dy in range(ny) for dx in range(nx) if dy or dx]
+    steps.sort(key=lambda t: -across(t[0], ny) - across(t[1], nx))
+    others = [(ys[dy], xs[dx]) for dy, dx in steps]
+    everyone = others + [(y, x)]
+    z_steps = sorted(range(1, nz), key=lambda d: -across(d, nz))
+
     at_line, at_col = x * (1 - c) + y * c, y * (1 - c) + x * c
+    lines = [xs[d] * (1 - c) + ys[d] * c for d in range(nx)]
+    columns = [ys[d] * (1 - c) + xs[d] * c for d in range(ny)]
 
     def line(i):
         return (z, y * (1 - c) + i * c, i * (1 - c) + x * c, c)
@@ -61,16 +71,10 @@
         return (z, i * (1 - c) + y * c, x * (1 - c) + i * c, c)
 
     def spot(g, i):
-        return lax.rem(i, nx) * ny + i // nx if g else i
-
-    def owner(i):
-        return (z, i // nx, lax.rem(i, nx), 1)
-
-    def piece_of(i):
-        return i // 2 + lax.rem(i, 2) * (pln // 2)
-
-    def plane(i):
-        return (z, i // nx, lax.rem(i, nx), c)
+        return lax.rem(i, nx) * ny + lax.div(i, nx) if g else i
+
+    def piece_of(ty, tx):
+        return ty * (nx // 2) + lax.div(tx, 2) + lax.rem(tx, 2) * (pln // 2)
 
     def head_of(a, h):
         return a[HEAD * h : HEAD * (h + 1)]
@@ -88,30 +92,37 @@
 
     scope = jax.named_scope
     with scope("loads_barrier"):
-        barrier = pltpu.get_barrier_semaphore()
-
-        def greet(device):
-            pl.semaphore_signal(barrier, inc=1, device_id=device, device_id_type=LOGICAL)
-
-        for k in range(1, nz):
-            greet((lax.rem(z + k, nz), y, x, c))
-        for k in range(1, pln):
-            to = lax.rem(me + k, pln)
-            greet((z, to // nx, lax.rem(to, nx), 1 - c))
-
-            @pl.when((c == 1) | (to // nx == y) | (lax.rem(to, nx) == x))
-            def _():
-                greet(plane(to))
-
-        greet((z, y, x, 1 - c))
         loads = [
             pltpu.make_async_copy(src, dst, lsem.at[k])
             for k, (src, dst) in enumerate(
                 ((f_hbm, f_v), (q_hbm, q_v), (go_hbm, go_v), (x_hbm, x_v), (w_hbm, w_v), (lb_hbm, lb_v))
             )
         ]
-        for copy in loads:
-            copy.start()
+        for k in (0, 5, 1, 2, 3, 4):
+            loads[k].start()
+        barrier = pltpu.get_barrier_semaphore()
+
+        def greet(device):
+            pl.semaphore_signal(barrier, inc=1, device_id=device, device_id_type=LOGICAL)
+
+        for ty, tx in others:
+            greet((z, ty, tx, 1 - c))
+        for d in z_steps:
+            greet((zs[d], y, x, c))
+
+        @pl.when(c == 1)
+        def _():
+            for ty, tx in others:
+                greet((z, ty, tx, 1))
+
+        @pl.when(c == 0)
+        def _():
+            for tx in xs[1:]:
+                greet((z, y, tx, 0))
+            for ty in ys[1:]:
+                greet((z, ty, x, 0))
+
+        greet((z, y, x, 1 - c))
 
     lane = lax.broadcasted_iota(jnp.int32, (1, ch), 1)
     mf = [jnp.where((lane >= HEAD * h) & (lane < HEAD * (h + 1)), 1.0, 0.0).astype(F32) for h in range(heads)]
@@ -133,7 +144,6 @@
         loads[0].wait()
         f = f_v[...].astype(F32)
         f_neg = 1.0 / (1.0 + jnp.exp(f))
-        f_sig = 1.0 / (1.0 + jnp.exp(-f))
         k_rate = gap * f_neg
         logs = jnp.log1p(-k_rate)
         high = logs.astype(BF16)
@@ -143,10 +153,8 @@
         total = jnp.exp((nt(row_ones, high) + nt(row_ones, low))[:1])
         closing = cum[:, tok - 1 : tok]
         growth = jnp.exp(cum)
-        shrink = jnp.exp(-cum)
         remain = jnp.exp(closing - cum)
         e_send[...] = total
-        k_dec = (k_rate * shrink).astype(BF16)
         k_end = (k_rate * remain).astype(BF16)
         loads[1].wait()
         q = q_v[...].astype(F32)
@@ -165,8 +173,54 @@
         r_send[...] = reach.astype(BF16)
         k_send[...] = k_end
 
+    with scope("barrier_wait"):
+        pl.semaphore_wait(barrier, pln + nz - 1 + c * (pln - 1) + (1 - c) * (nx + ny - 2))
+
+    def to_line(source, target, send_sem, recv_sem):
+        for k in range(1, nx):
+            rcopy(source, target.at[at_line], send_sem, recv_sem, line(lines[k])).start()
+
+    def to_column(source, target, send_sem, recv_sem):
+        for k in range(1, ny):
+            to = columns[k]
+            rcopy(source.at[to], target.at[at_col], send_sem, recv_sem, column(to)).start()
+
+    def from_column(own, target, recv_sem):
+        arrived(target, ny - 1, recv_sem)
+        out = own[...].astype(F32)
+        for k in range(1, ny):
+            out = out + target[columns[k]].astype(F32)
+        return out
+
+    def piece_sends(ty, tx):
+        to = (z, ty, tx, 1)
+        return (
+            rcopy(e_send, e_buf.at[c * pln + me], e_ss, e_rs, to),
+            rcopy(s_send.at[piece_of(ty, tx)], s_buf.at[c * pln + me], s_ss, s_rs, to),
+        )
+
+    mine = piece_of(y, x)
+    with scope("send1"):
+        for ty, tx in others:
+            for copy in piece_sends(ty, tx):
+                copy.start()
+
+        @pl.when(c == 0)
+        def _():
+            for copy in piece_sends(y, x):
+                copy.start()
+
+        @pl.when(c == 1)
+        def _():
+            s_buf[pln + me] = s_send[mine]
+            e_buf[pln + me] = e_send[...]
+
+        to_line(k_send, kl, k_ss, k_rs)
+        kl[at_line] = k_end
+        rl[at_line] = r_send[...]
+
+    rows = d_model // (nz * ny * nx)
     with scope("turn"):
-        rows = d_model // (nz * ny * nx)
         per = tok // rows
         for b in range(d_model // tok):
             turned = x_v[:, tok * b : tok * (b + 1)].T
@@ -176,61 +230,19 @@
                 group, into = xx * (1 - c) + yy * c, yy * (1 - c) + xx * c
                 xt[group, into, zz] = turned[rows * g : rows * (g + 1)]
 
-    with scope("barrier_wait"):
-        pl.semaphore_wait(barrier, pln + nz - 1 + c * (pln - 1) + (1 - c) * (nx + ny - 2))
-
-    def to_line(source, target, send_sem, recv_sem):
         for k in range(1, nx):
-            rcopy(source, target.at[at_line], send_sem, recv_sem, line(lax.rem(at_line + k, nx))).start()
-
-    def to_column(source, target, send_sem, recv_sem):
-        for k in range(1, ny):
-            to = lax.rem(at_col + k, ny)
-            rcopy(source.at[to], target.at[at_col], send_sem, recv_sem, column(to)).start()
-
-    def from_column(own, target, recv_sem):
-        arrived(target, ny - 1, recv_sem)
-        out = own[...].astype(F32)
-        for k in range(1, ny):
-            out = out + target[lax.rem(at_col + k, ny)].astype(F32)
-        return out
-
-    def piece_sends(k):
-        to = lax.rem(me + k, pln)
-        return (
-            rcopy(e_send, e_buf.at[c * pln + me], e_ss, e_rs, owner(to)),
-            rcopy(s_send.at[piece_of(to)], s_buf.at[c * pln + me], s_ss, s_rs, owner(to)),
-        )
-
-    with scope("send1"):
-        for k in range(1, pln):
-            for copy in piece_sends(k):
-                copy.start()
+            to = lines[k]
+            rcopy(xt.at[to], xtl.at[at_line], xt_ss, xt_rs, line(to)).start()
 
         @pl.when(c == 0)
         def _():
-            for copy in piece_sends(0):
-                copy.start()
-
-        @pl.when(c == 1)
-        def _():
-            s_buf[pln + me] = s_send[piece_of(me)]
-            e_buf[pln + me] = e_send[...]
-
-        for k in range(1, nx):
-            to = lax.rem(at_line + k, nx)
-            rcopy(xt.at[to], xtl.at[at_line], xt_ss, xt_rs, line(to)).start()
-        to_line(k_send, kl, k_ss, k_rs)
-
-        @pl.when(c == 0)
-        def _():
             to_line(r_send, rl, r_ss, r_rs)
 
         xtl[at_line] = xt[at_line]
-        kl[at_line] = k_end
-        rl[at_line] = r_send[...]
 
     with scope("pairs_value"):
+        shrink = jnp.exp(-cum)
+        k_dec = (k_rate * shrink).astype(BF16)
         mixing = [jnp.where(lower, tn(head_of(q_dec, h), head_of(k_dec, h)), 0.0).astype(BF16) for h in range(heads)]
         gv_own = by_head(nn(head_of(go, h), mixing[h]) for h in range(heads))
         own_send[...] = gv_own.astype(BF16)
@@ -247,17 +259,17 @@
             rcopy(t_send, t_buf.at[z], t_ss, t_rs, (to, y, x, 1)),
         )
 
-    def carry_send(g, k, backward):
-        to = lax.rem(me + k, pln)
-        device = (z, to // nx, lax.rem(to, nx), g)
+    def carry_send(g, ty, tx, backward):
+        device = (z, ty, tx, g)
         if not backward:
-            return rcopy(l_send.at[g * pln + spot(g, to)], q_state.at[me // 2], q_ss.at[g], q_rs.at[0], device)
+            at = pln + tx * ny + ty if g else ty * nx + tx
+            return rcopy(l_send.at[at], q_state.at[me // 2], q_ss.at[g], q_rs.at[0], device)
         if g == 0:
-            return rcopy(l_send.at[to // nx * nx + nx - 1], q_line.at[me // 2], q_ss.at[0], q_rs.at[1], device)
-        first = pln + lax.rem(to, nx) * ny
-        return rcopy(l_send.at[pl.ds(first, ny)], q_grad.at[pl.ds(me // 2 * ny, ny)], q_ss.at[1], q_rs.at[1], device)
-
-    targets = [(0, k) for k in range(pln)] + [(1, k) for k in range(1, pln)]
+            return rcopy(l_send.at[ty * nx + nx - 1], q_line.at[me // 2], q_ss.at[0], q_rs.at[1], device)
+        rows_of = pl.ds(pln + tx * ny, ny)
+        return rcopy(l_send.at[rows_of], q_grad.at[pl.ds(me // 2 * ny, ny)], q_ss.at[1], q_rs.at[1], device)
+
+    targets = [(0, *t) for t in everyone] + [(1, *t) for t in others]
     plane_decays = e_buf.at[pl.ds(0, pln)]
     e_all = rcopy(plane_decays, plane_decays, ea_ss, ea_rs, (z, y, x, 1 - c))
 
@@ -290,14 +302,14 @@
 
                 @pl.when(back == backward)
                 def _():
-                    for g, k in targets:
-                        carry_send(g, k, backward).start()
+                    for target in targets:
+                        carry_send(*target, backward).start()
 
             e_all.start()
 
             @pl.when(back == 0)
             def _():
-                q_state[me // 2] = l_send[pln + spot(1, me)]
+                q_state[me // 2] = l_send[pln + x * ny + y]
 
             @pl.when(back == 1)
             def _():
@@ -344,12 +356,8 @@
         frm = o + back * (nz - 1 - 2 * o)
         return ft_buf[frm] * carried + t_buf[frm].astype(F32)
 
-    mine = piece_of(me)
-
-    def plane_send(g, k):
-        to = lax.rem(me + k, pln)
-        device = (z, to // nx, lax.rem(to, nx), g)
-        return rcopy(o_send.at[g], p_buf.at[mine], p_ss, p_rs, device)
+    def plane_send(g, ty, tx):
+        return rcopy(o_send.at[g], p_buf.at[mine], p_ss, p_rs, (z, ty, tx, g))
 
     @pl.when(c == 1)
     def _():
@@ -364,8 +372,8 @@
             carried = lax.fori_loop(0, z_order, arriving, jnp.zeros(t_send.shape, F32))
         with scope("send3"):
             o_send[...] = carried.astype(BF16)
-            for g, k in targets:
-                plane_send(g, k).start()
+            for target in targets:
+                plane_send(*target).start()
             p_buf[mine] = o_send[1]
 
     with scope("send_m"):
@@ -440,9 +448,8 @@
         w_sum = a_plane + nt(m_plane, bd_out)
         w2[...] = w_sum.reshape(w2.shape)
         z_send[...] = w_sum.astype(BF16).reshape(z_send.shape)
-        for k in range(1, nz):
-            to = lax.rem(z + k, nz)
-            rcopy(z_send.at[to], z_recv.at[z], z_ss, z_rs, (to, y, x, c)).start()
+        for d in z_steps:
+            rcopy(z_send.at[zs[d]], z_recv.at[z], z_ss, z_rs, (zs[d], y, x, c)).start()
 
     with scope("value_grad"):
         own_after = after[nx - 1]
@@ -476,7 +483,7 @@
         flow_high = flow.astype(BF16)
         flow_low = (flow - flow_high.astype(F32)).astype(BF16)
         g_decay = nn(flow_high, lower_ones) + nn(flow_low, lower_ones) + boundary
-        gf_out[...] = ((g_decay / (1.0 - k_rate) - g_key) * k_rate * f_sig).astype(BF16)
+        gf_out[...] = ((g_decay / (1.0 - k_rate) - g_key) * k_rate * (1.0 / (1.0 + jnp.exp(-f)))).astype(BF16)
 
     with scope("input_sum"):
         ig_copy.wait_recv()
@@ -521,7 +528,7 @@
         arrived(z_recv, nz - 1, z_rs)
         w_last = w2[z]
         for k in range(1, nz):
-            w_last = w_last + z_recv[lax.rem(z + k, nz)].astype(F32)
+            w_last = w_last + z_recv[zs[k]].astype(F32)
         gw_out[...] = w_last
         left(z_send, nz - 1, z_ss)
 

time: 31.6 us -> 31.3 us (level)
  Pallas kernels: 30.9 us -> 30.5 us
    pallas_call x1, Pallas kernels: 30.1 us -> 29.7 us  [on_device(): pl.pallas_call(functools.partial(kernel, nz, ny, nx), out_shape=(vm((ch,...]
where the time goes in v9:
time: 31.3 us; the launch traced here: 31.2 us
  Pallas kernels  30.5 us (97%)
  between operations  0.64 us (2%)
    pallas_call x1, Pallas kernels, on_device(): pl.pallas_call(functools.partial(kernel, nz, ny, nx), out_shape=(vm((ch,...  29.7 us
    pallas_call x1, Pallas kernels, on_device(): pl.pallas_call(write_out, out_shape=tuple((jax.ShapeDtypeStruct(a.shape,...  0.77 us

profile of v9, /device:TPU:1, one launch (start us, length us, event | category | flops | bytes accessed | tf_op | source)
XLA Modules:
  0.0 31.2 jit_solution(1982308575580196188)
XLA Ops:
  0.6 29.7 %shard_map.93 = (bf16[192,128]{1,0:T(8,128)(2,1)S(1)}, bf16[192,128]{1,0:T(8,128)(2,1)S(1)}, bf16[64,2048]{1,0:T(8,128)(2,1)S(1)}, f32[16,192]{1,0:T(8,128)S(1)}) custom-call(bf16[128,2048]{1,0:T(8,128)(2,1)} %x_hbm.1, bf16[192,2048]{1,0:T(8,128)(2,1)} %bitcast.7, bf16[192,128]{1,0:T(8,128)(2,1)} %bitcast.8, bf16[192,128]{1,0:T(8,128)(2,1)} %bitcast.9, ...), custom_call_target="tpu_custom_call" | custom-call | tf_op jit(solution)/shard_map/pallas_call | solution.py:576
  30.4 0.8 %shard_map.94 = (bf16[192,128]{1,0:T(8,128)(2,1)}, bf16[192,128]{1,0:T(8,128)(2,1)}, bf16[64,2048]{1,0:T(8,128)(2,1)}, f32[16,192]{1,0:T(8,128)}) custom-call(bf16[192,128]{1,0:T(8,128)(2,1)S(1)} %get-tuple-element.12.refs_0_, bf16[192,128]{1,0:T(8,128)(2,1)S(1)} %get-tuple-element.13.refs_1_, bf16[64,2048]{1,0:T(8,128)(2,1)S(1)} %get-tuple-element.14.refs_2_, ...), custom_call_target="tpu_custom_call" | custom-call | tf_op jit(solution)/shard_map/pallas_call | solution.py:589

commit v10 on v9

--- a/solution.py
+++ b/solution.py
@@ -38,7 +38,7 @@
     x_hbm, w_hbm, q_hbm, f_hbm, go_hbm, lb_hbm,
     gq_out, gf_out, gx_out, gw_out,
     x_v, w_v, q_v, f_v, go_v, lb_v, wide, thin,
-    s_send, e_send, s_buf, e_buf, l_send, q_state, q_grad, q_line, t_send, ft_send, t_buf, ft_buf, o_send, p_buf,
+    s_send, e_send, s_buf, e_buf, l_send, q_state, q_grad, q_line, t_send, ft_send, t_buf, ft_buf, o_send, p_buf, p_both, outer,
     xt, xtl, r_send, rl, k_send, kl, own_send, ownl, g_all, ig, ig_recv,
     m_send, m_recv, aacc, a_send, a_recv, w2, z_send, z_recv,
     lsem, s_ss, s_rs, e_ss, e_rs, ea_ss, ea_rs, q_ss, q_rs, t_ss, t_rs, ft_ss, ft_rs, p_ss, p_rs,
@@ -108,10 +108,12 @@
         for ty, tx in others:
             greet((z, ty, tx, 1 - c))
         for d in z_steps:
-            greet((zs[d], y, x, c))
+            greet((zs[d], y, x, 1))
 
         @pl.when(c == 1)
         def _():
+            for d in z_steps:
+                greet((zs[d], y, x, 0))
             for ty, tx in others:
                 greet((z, ty, tx, 1))
 
@@ -119,8 +121,6 @@
         def _():
             for tx in xs[1:]:
                 greet((z, y, tx, 0))
-            for ty in ys[1:]:
-                greet((z, ty, x, 0))
 
         greet((z, y, x, 1 - c))
 
@@ -174,7 +174,7 @@
         k_send[...] = k_end
 
     with scope("barrier_wait"):
-        pl.semaphore_wait(barrier, pln + nz - 1 + c * (pln - 1) + (1 - c) * (nx + ny - 2))
+        pl.semaphore_wait(barrier, pln + nz - 1 + c * (pln + nz - 2) + (1 - c) * (nx - 1))
 
     def to_line(source, target, send_sem, recv_sem):
         for k in range(1, nx):
@@ -183,14 +183,24 @@
     def to_column(source, target, send_sem, recv_sem):
         for k in range(1, ny):
             to = columns[k]
-            rcopy(source.at[to], target.at[at_col], send_sem, recv_sem, column(to)).start()
-
-    def from_column(own, target, recv_sem):
-        arrived(target, ny - 1, recv_sem)
+            device = (z, to * (1 - c) + y * c, x * (1 - c) + to * c, 1)
+            rcopy(source.at[to], target.at[c * ny + at_col], send_sem, recv_sem.at[c], device).start()
+
+        @pl.when(c == 0)
+        def _():
+            rcopy(source.at[y], target.at[y], send_sem, recv_sem.at[0], (z, y, x, 1)).start()
+
+    def from_column(g, own, target, recv_sem):
+        arrived(target, ny - g, recv_sem.at[g])
+        if g == 0:
+            out = target[0].astype(F32)
+            for k in range(1, ny):
+                out = out + target[k].astype(F32)
+            return out.T
         out = own[...].astype(F32)
         for k in range(1, ny):
-            out = out + target[columns[k]].astype(F32)
-        return out
+            out = out + target[ny + xs[k]].astype(F32)
+        return out.T
 
     def piece_sends(ty, tx):
         to = (z, ty, tx, 1)
@@ -357,7 +367,9 @@
         return ft_buf[frm] * carried + t_buf[frm].astype(F32)
 
     def plane_send(g, ty, tx):
-        return rcopy(o_send.at[g], p_buf.at[mine], p_ss, p_rs, (z, ty, tx, g))
+        if g:
+            return rcopy(o_send, p_both.at[mine], p_ss, p_rs, (z, ty, tx, 1))
+        return rcopy(o_send.at[0], p_buf.at[mine], p_ss, p_rs, (z, ty, tx, 0))
 
     @pl.when(c == 1)
     def _():
@@ -374,7 +386,7 @@
             o_send[...] = carried.astype(BF16)
             for target in targets:
                 plane_send(*target).start()
-            p_buf[mine] = o_send[1]
+            p_both[mine] = o_send[...]
 
     with scope("send_m"):
         to_column(m_send, m_recv, m_ss, m_rs)
@@ -398,8 +410,6 @@
             arrived(q_state, some, q_rs.at[0])
             arrived(q_grad, (some - 1) * ny, q_rs.at[1])
 
-    with scope("wait_own"):
-        arrived(ownl, nx - 1, own_rs)
     with scope("line_a"):
         state_in = q_state[...].astype(F32).reshape(HEAD, ch)
 
@@ -421,8 +431,11 @@
         for i in range(nx):
             grad_at = g_all[i]
             bd_in = by_head((grad_at * m).astype(BF16) for m in mf)
-            parts.append((ownl[i].astype(F32) + nn(bd_in, kl[i])).astype(BF16))
-        parts = pairs(parts)
+            parts.append(nn(bd_in, kl[i]))
+    with scope("wait_own"):
+        arrived(ownl, nx - 1, own_rs)
+    with scope("line_a2"):
+        parts = pairs([(ownl[i].astype(F32) + part).astype(BF16) for i, part in enumerate(parts)])
         a_sum = nt(parts[0], turned_of[0])
         for a, b in zip(parts[1:], turned_of[1:]):
             a_sum = a_sum + nt(a, b)
@@ -430,28 +443,33 @@
         to_chunks(a_send, a_sum)
         to_column(a_send, a_recv, a_ss, a_rs)
 
-    with scope("wait_m"):
-        m_plane = from_column(m_send.at[at_col], m_recv, m_rs).T.astype(BF16)
-    with scope("wait3"):
-        for core in (0, 1):
-
-            @pl.when(c == core)
-            def _():
-                arrived(p_buf, pln - core, p_rs)
-
-    with scope("wait_a"):
-        a_plane = from_column(aacc.at[at_col], a_recv, a_rs).T
-    with scope("send_z"):
-        outer = p_buf[...].astype(F32).reshape(2 * HEAD, ch)
-        state_out, grad_out = outer[:HEAD], outer[HEAD:]
-        bd_out = by_head((grad_out * m).astype(BF16) for m in mf)
-        w_sum = a_plane + nt(m_plane, bd_out)
-        w2[...] = w_sum.reshape(w2.shape)
-        z_send[...] = w_sum.astype(BF16).reshape(z_send.shape)
-        for d in z_steps:
-            rcopy(z_send.at[zs[d]], z_recv.at[z], z_ss, z_rs, (zs[d], y, x, c)).start()
+    @pl.when(c == 1)
+    def _():
+        with scope("wait_m"):
+            m_plane = [from_column(g, m_send.at[x], m_recv, m_rs).astype(BF16) for g in (0, 1)]
+        with scope("wait3"):
+            arrived(p_both, pln - 1, p_rs)
+        for g in (0, 1):
+            outer[g] = p_both[:, g].astype(F32).reshape(2 * HEAD, ch)
+            bd_out = by_head((outer[g, HEAD:] * m).astype(BF16) for m in mf)
+            with scope(f"wait_a{g}"):
+                a_plane = from_column(g, aacc.at[x], a_recv, a_rs)
+            with scope(f"send_z{g}"):
+                w_sum = a_plane + nt(m_plane[g], bd_out)
+                if g:
+                    w2[...] = w_sum.reshape(w2.shape)
+                z_send[pl.ds(g * nz, nz)] = w_sum.astype(BF16).reshape(nz, rows, ch)
+                for d in z_steps if g else z_steps + [0]:
+                    rcopy(z_send.at[g * nz + zs[d]], z_recv.at[z], z_ss, z_rs, (zs[d], y, x, g)).start()
+
+    @pl.when(c == 0)
+    def _():
+        with scope("wait3"):
+            arrived(p_buf, pln, p_rs)
+        outer[0] = p_buf[...].astype(F32).reshape(2 * HEAD, ch)
 
     with scope("value_grad"):
+        state_out, grad_out = outer[c, :HEAD], outer[c, HEAD:]
         own_after = after[nx - 1]
         for i in range(nx - 1):
             own_after = jnp.where(at_line == i, after[i], own_after)
@@ -493,8 +511,6 @@
         left(xt, nx - 1, xt_ss)
         left(kl, nx - 1, k_ss)
         left(ownl, nx - 1, own_ss)
-        left(m_send, ny - 1, m_ss)
-        left(a_send, ny - 1, a_ss)
         ig_copy.wait_send()
 
         @pl.when(c == 0)
@@ -502,9 +518,13 @@
             left(thin, pln, e_ss)
             left(s_send, pln, s_ss)
             left(rl, nx - 1, r_ss)
+            left(m_send, ny, m_ss)
+            left(a_send, ny, a_ss)
 
         @pl.when(c == 1)
         def _():
+            left(m_send, ny - 1, m_ss)
+            left(a_send, ny - 1, a_ss)
             left(thin, pln - 1, e_ss)
             left(s_send, pln - 1, s_ss)
             for n in range(1, nz):
@@ -522,15 +542,26 @@
                     left(wide, (pln - 1) * (ny if backward else 1), q_ss.at[1])
 
             e_all.wait_send()
-            left(wide, 2 * pln - 1, p_ss)
+            left(wide, 3 * pln - 2, p_ss)
 
     with scope("wait_z"):
-        arrived(z_recv, nz - 1, z_rs)
-        w_last = w2[z]
-        for k in range(1, nz):
-            w_last = w_last + z_recv[zs[k]].astype(F32)
-        gw_out[...] = w_last
-        left(z_send, nz - 1, z_ss)
+
+        @pl.when(c == 0)
+        def _():
+            arrived(z_recv, nz, z_rs)
+            w_last = z_recv[0].astype(F32)
+            for k in range(1, nz):
+                w_last = w_last + z_recv[k].astype(F32)
+            gw_out[...] = w_last
+
+        @pl.when(c == 1)
+        def _():
+            arrived(z_recv, nz - 1, z_rs)
+            w_last = w2[z]
+            for k in range(1, nz):
+                w_last = w_last + z_recv[zs[k]].astype(F32)
+            gw_out[...] = w_last
+            left(z_send, 2 * nz - 1, z_ss)
 
 
 def write_out(*refs):
@@ -551,26 +582,28 @@
     scratch = [
         vm((tok, d_model), BF16), vm((ch, d_model), BF16),
         vm((ch, tok), BF16), vm((ch, tok), BF16), vm((ch, tok), BF16), vm((1, ch), F32),
-        vm((pln * ny, piece, ch), BF16), vm((pln, 1, ch), F32),
+        vm((pln * (ny + 1), piece, ch), BF16), vm((pln, 1, ch), F32),
         vm((pln, piece, ch), BF16), vm((1, ch), F32),
         vm((2 * pln, piece, ch), BF16), vm((2 * pln, 1, ch), F32),
         vm((2 * pln, piece, ch), BF16), vm((pln // 2, piece, ch), BF16), vm((pln // 2 * ny, piece, ch), BF16),
         vm((pln // 2, piece, ch), BF16),
         vm((2, piece, ch), BF16), vm((2, 1, ch), F32),
         vm((nz, 2, piece, ch), BF16), vm((nz, 2, 1, ch), F32),
-        vm((2, piece, ch), BF16), vm((pln, piece, ch), BF16),
+        vm((2, piece, ch), BF16), vm((pln, piece, ch), BF16), vm((pln, 2, piece, ch), BF16),
+        vm((2, 2 * HEAD, ch), F32),
         vm((nx, ny, nz, rows, tok), BF16), vm((nx, ny, nz, rows, tok), BF16),
         vm((HEAD, ch), BF16), vm((nx, HEAD, ch), BF16),
         vm((ch, tok), BF16), vm((nx, ch, tok), BF16),
         vm((ch, tok), BF16), vm((nx, ch, tok), BF16),
         vm((nx, HEAD, ch), F32),
         vm((2, tok // 2, d_model), BF16), vm((tok // 2, d_model), BF16),
-        vm((ny, ch, nz * rows), BF16), vm((ny, ch, nz * rows), BF16),
-        vm((ny, ch, nz * rows), F32), vm((ny, ch, nz * rows), BF16), vm((ny, ch, nz * rows), BF16),
-        vm((nz, rows, ch), F32), vm((nz, rows, ch), BF16), vm((nz, rows, ch), BF16),
+        vm((ny, ch, nz * rows), BF16), vm((2 * ny, ch, nz * rows), BF16),
+        vm((ny, ch, nz * rows), F32), vm((ny, ch, nz * rows), BF16), vm((2 * ny, ch, nz * rows), BF16),
+        vm((nz, rows, ch), F32), vm((2 * nz, rows, ch), BF16), vm((nz, rows, ch), BF16),
         dma((6,)),
         *(dma for _ in range(6)), dma((2,)), dma((2,)),
-        *(dma for _ in range(4 + 2 + 8 + 4 + 2 + 2)),
+        *(dma for _ in range(4 + 2 + 8)),
+        dma, dma((2,)), dma, dma((2,)), dma, dma, dma, dma,
     ]
     hbm, near = pl.BlockSpec(memory_space=pl.ANY), pl.BlockSpec(memory_space=pltpu.VMEM)
     results = pl.pallas_call(

time: 31.3 us -> 32 us (1.022)
  Pallas kernels: 30.5 us -> 31.3 us
    pallas_call x1, Pallas kernels: 29.7 us -> 30.5 us  [on_device(): pl.pallas_call(functools.partial(kernel, nz, ny, nx), out_shape=(vm((ch,...]
where the time goes in v10:
time: 32 us; the launch traced here: 31.9 us
  Pallas kernels  31.3 us (98%)
  between operations  0.64 us (2%)
    pallas_call x1, Pallas kernels, on_device(): pl.pallas_call(functools.partial(kernel, nz, ny, nx), out_shape=(vm((ch,...  30.5 us
    pallas_call x1, Pallas kernels, on_device(): pl.pallas_call(write_out, out_shape=tuple((jax.ShapeDtypeStruct(a.shape,...  0.77 us

profile of v10, /device:TPU:1, one launch (start us, length us, event | category | flops | bytes accessed | tf_op | source)
XLA Modules:
  0.0 31.9 jit_solution(10561581728501614189)
XLA Ops:
  0.6 30.5 %shard_map.93 = (bf16[192,128]{1,0:T(8,128)(2,1)S(1)}, bf16[192,128]{1,0:T(8,128)(2,1)S(1)}, bf16[64,2048]{1,0:T(8,128)(2,1)S(1)}, f32[16,192]{1,0:T(8,128)S(1)}) custom-call(bf16[128,2048]{1,0:T(8,128)(2,1)} %x_hbm.1, bf16[192,2048]{1,0:T(8,128)(2,1)} %bitcast.7, bf16[192,128]{1,0:T(8,128)(2,1)} %bitcast.8, bf16[192,128]{1,0:T(8,128)(2,1)} %bitcast.9, ...), custom_call_target="tpu_custom_call" | custom-call | tf_op jit(solution)/shard_map/pallas_call | solution.py:609
  31.1 0.8 %shard_map.94 = (bf16[192,128]{1,0:T(8,128)(2,1)}, bf16[192,128]{1,0:T(8,128)(2,1)}, bf16[64,2048]{1,0:T(8,128)(2,1)}, f32[16,192]{1,0:T(8,128)}) custom-call(bf16[192,128]{1,0:T(8,128)(2,1)S(1)} %get-tuple-element.12.refs_0_, bf16[192,128]{1,0:T(8,128)(2,1)S(1)} %get-tuple-element.13.refs_1_, bf16[64,2048]{1,0:T(8,128)(2,1)S(1)} %get-tuple-element.14.refs_2_, ...), custom_call_target="tpu_custom_call" | custom-call | tf_op jit(solution)/shard_map/pallas_call | solution.py:622

commit v11 on v10

--- a/solution.py
+++ b/solution.py
@@ -51,7 +51,7 @@
     heads = ch // HEAD
     z, y, x, c = (lax.axis_index(a) for a in SP_TP)
     me = y * nx + x
-    back = lax.rem(me, 2)
+    back = lax.rem(x + y, 2)
     zs, ys, xs = ([lax.rem(at + d, n) for d in range(n)] for at, n in ((z, nz), (y, ny), (x, nx)))
     across = lambda d, n: min(d, n - d)
     steps = [(dy, dx) for dy in range(ny) for dx in range(nx) if dy or dx]
@@ -59,6 +59,7 @@
     others = [(ys[dy], xs[dx]) for dy, dx in steps]
     everyone = others + [(y, x)]
     z_steps = sorted(range(1, nz), key=lambda d: -across(d, nz))
+    far_first = sorted(range(1, nx), key=lambda d: -across(d, nx))
 
     at_line, at_col = x * (1 - c) + y * c, y * (1 - c) + x * c
     lines = [xs[d] * (1 - c) + ys[d] * c for d in range(nx)]
@@ -74,7 +75,7 @@
         return lax.rem(i, nx) * ny + lax.div(i, nx) if g else i
 
     def piece_of(ty, tx):
-        return ty * (nx // 2) + lax.div(tx, 2) + lax.rem(tx, 2) * (pln // 2)
+        return ty * (nx // 2) + lax.div(tx, 2) + lax.rem(tx + ty, 2) * (pln // 2)
 
     def head_of(a, h):
         return a[HEAD * h : HEAD * (h + 1)]
@@ -177,11 +178,11 @@
         pl.semaphore_wait(barrier, pln + nz - 1 + c * (pln + nz - 2) + (1 - c) * (nx - 1))
 
     def to_line(source, target, send_sem, recv_sem):
-        for k in range(1, nx):
+        for k in far_first:
             rcopy(source, target.at[at_line], send_sem, recv_sem, line(lines[k])).start()
 
     def to_column(source, target, send_sem, recv_sem):
-        for k in range(1, ny):
+        for k in far_first:
             to = columns[k]
             device = (z, to * (1 - c) + y * c, x * (1 - c) + to * c, 1)
             rcopy(source.at[to], target.at[c * ny + at_col], send_sem, recv_sem.at[c], device).start()
@@ -240,7 +241,7 @@
                 group, into = xx * (1 - c) + yy * c, yy * (1 - c) + xx * c
                 xt[group, into, zz] = turned[rows * g : rows * (g + 1)]
 
-        for k in range(1, nx):
+        for k in far_first:
             to = lines[k]
             rcopy(xt.at[to], xtl.at[at_line], xt_ss, xt_rs, line(to)).start()
 
@@ -257,7 +258,11 @@
         gv_own = by_head(nn(head_of(go, h), mixing[h]) for h in range(heads))
         own_send[...] = gv_own.astype(BF16)
         ownl[at_line] = own_send[...]
-        to_line(own_send, ownl, own_ss, own_rs)
+
+        @pl.when(c == 0)
+        def _():
+            to_line(own_send, ownl, own_ss, own_rs)
+
 
     z_order = z + back * (nz - 1 - 2 * z)
 
@@ -308,22 +313,14 @@
                     for copy in z_sends(k):
                         copy.start()
 
-            for backward in (0, 1):
-
-                @pl.when(back == backward)
-                def _():
-                    for target in targets:
-                        carry_send(*target, backward).start()
-
-            e_all.start()
-
-            @pl.when(back == 0)
-            def _():
-                q_state[me // 2] = l_send[pln + x * ny + y]
-
             @pl.when(back == 1)
             def _():
+                for target in targets:
+                    carry_send(*target, 1).start()
                 q_grad[pl.ds(me // 2 * ny, ny)] = l_send[pl.ds(pln + x * ny, ny)]
+
+            to_line(own_send, ownl, own_ss, own_rs)
+            e_all.start()
 
     with scope("pairs_query"):
         pairing = [jnp.where(upper, tn(head_of(v, h), head_of(go, h)), 0.0).astype(BF16) for h in range(heads)]
@@ -361,6 +358,7 @@
         for a, b in zip(scaled[1:], turned_of[1:]):
             m_sum = m_sum + nt(a, b)
         to_chunks(m_send, m_sum)
+        to_column(m_send, m_recv, m_ss, m_rs)
 
     def arriving(o, carried):
         frm = o + back * (nz - 1 - 2 * o)
@@ -384,34 +382,32 @@
             carried = lax.fori_loop(0, z_order, arriving, jnp.zeros(t_send.shape, F32))
         with scope("send3"):
             o_send[...] = carried.astype(BF16)
-            for target in targets:
+            for target in targets[pln:] + targets[:pln]:
                 plane_send(*target).start()
             p_both[mine] = o_send[...]
 
-    with scope("send_m"):
-        to_column(m_send, m_recv, m_ss, m_rs)
+            @pl.when(back == 0)
+            def _():
+                for target in targets:
+                    carry_send(*target, 0).start()
+                q_state[me // 2] = l_send[pln + x * ny + y]
+
 
     some = pln // 2
     with scope("wait_1b"):
 
         @pl.when(c == 0)
         def _():
-            arrived(q_state, some, q_rs.at[0])
             arrived(q_line, some, q_rs.at[1])
             arrived(rl, nx - 1, r_rs)
 
-        @pl.when((c == 1) & (back == 0))
-        def _():
-            arrived(q_state, some - 1, q_rs.at[0])
-            arrived(q_grad, some * ny, q_rs.at[1])
-
-        @pl.when((c == 1) & (back == 1))
-        def _():
-            arrived(q_state, some, q_rs.at[0])
-            arrived(q_grad, (some - 1) * ny, q_rs.at[1])
+        for odd in (0, 1):
+
+            @pl.when((c == 1) & (back == odd))
+            def _():
+                arrived(q_grad, (some - odd) * ny, q_rs.at[1])
 
     with scope("line_a"):
-        state_in = q_state[...].astype(F32).reshape(HEAD, ch)
 
         @pl.when(c == 0)
         def _():
@@ -445,17 +441,19 @@
 
     @pl.when(c == 1)
     def _():
-        with scope("wait_m"):
-            m_plane = [from_column(g, m_send.at[x], m_recv, m_rs).astype(BF16) for g in (0, 1)]
+        with scope("wait_m1"):
+            m_plane = from_column(1, m_send.at[x], m_recv, m_rs).astype(BF16)
         with scope("wait3"):
             arrived(p_both, pln - 1, p_rs)
-        for g in (0, 1):
+        for g in (1, 0):
             outer[g] = p_both[:, g].astype(F32).reshape(2 * HEAD, ch)
             bd_out = by_head((outer[g, HEAD:] * m).astype(BF16) for m in mf)
             with scope(f"wait_a{g}"):
-                a_plane = from_column(g, aacc.at[x], a_recv, a_rs)
+                if g == 0:
+                    m_plane = from_column(0, None, m_recv, m_rs).astype(BF16)
+                w_sum = nt(m_plane, bd_out)
+                w_sum = w_sum + from_column(g, aacc.at[x], a_recv, a_rs)
             with scope(f"send_z{g}"):
-                w_sum = a_plane + nt(m_plane[g], bd_out)
                 if g:
                     w2[...] = w_sum.reshape(w2.shape)
                 z_send[pl.ds(g * nz, nz)] = w_sum.astype(BF16).reshape(nz, rows, ch)
@@ -469,6 +467,13 @@
         outer[0] = p_buf[...].astype(F32).reshape(2 * HEAD, ch)
 
     with scope("value_grad"):
+        for even in (0, 1):
+
+            @pl.when((1 - back) * c == even)
+            def _():
+                arrived(q_state, some - even, q_rs.at[0])
+
+        state_in = q_state[...].astype(F32).reshape(HEAD, ch)
         state_out, grad_out = outer[c, :HEAD], outer[c, HEAD:]
         own_after = after[nx - 1]
         for i in range(nx - 1):

time: 32 us -> 30.3 us (0.947)
  Pallas kernels: 31.3 us -> 29.6 us
    pallas_call x1, Pallas kernels: 30.5 us -> 28.8 us  [on_device(): pl.pallas_call(functools.partial(kernel, nz, ny, nx), out_shape=(vm((ch,...]
where the time goes in v11:
time: 30.3 us; the launch traced here: 30.2 us
  Pallas kernels  29.6 us (98%)
  between operations  0.64 us (2%)
    pallas_call x1, Pallas kernels, on_device(): pl.pallas_call(functools.partial(kernel, nz, ny, nx), out_shape=(vm((ch,...  28.8 us
    pallas_call x1, Pallas kernels, on_device(): pl.pallas_call(write_out, out_shape=tuple((jax.ShapeDtypeStruct(a.shape,...  0.77 us

profile of v11, /device:TPU:1, one launch (start us, length us, event | category | flops | bytes accessed | tf_op | source)
XLA Modules:
  0.0 30.2 jit_solution(12713383224850994810)
XLA Ops:
  0.6 28.8 %shard_map.93 = (bf16[192,128]{1,0:T(8,128)(2,1)S(1)}, bf16[192,128]{1,0:T(8,128)(2,1)S(1)}, bf16[64,2048]{1,0:T(8,128)(2,1)S(1)}, f32[16,192]{1,0:T(8,128)S(1)}) custom-call(bf16[128,2048]{1,0:T(8,128)(2,1)} %x_hbm.1, bf16[192,2048]{1,0:T(8,128)(2,1)} %bitcast.7, bf16[192,128]{1,0:T(8,128)(2,1)} %bitcast.8, bf16[192,128]{1,0:T(8,128)(2,1)} %bitcast.9, ...), custom_call_target="tpu_custom_call" | custom-call | tf_op jit(solution)/shard_map/pallas_call | solution.py:614
  29.5 0.8 %shard_map.94 = (bf16[192,128]{1,0:T(8,128)(2,1)}, bf16[192,128]{1,0:T(8,128)(2,1)}, bf16[64,2048]{1,0:T(8,128)(2,1)}, f32[16,192]{1,0:T(8,128)}) custom-call(bf16[192,128]{1,0:T(8,128)(2,1)S(1)} %get-tuple-element.12.refs_0_, bf16[192,128]{1,0:T(8,128)(2,1)S(1)} %get-tuple-element.13.refs_1_, bf16[64,2048]{1,0:T(8,128)(2,1)S(1)} %get-tuple-element.14.refs_2_, ...), custom_call_target="tpu_custom_call" | custom-call | tf_op jit(solution)/shard_map/pallas_call | solution.py:627

commit v12 on v11

--- a/solution.py
+++ b/solution.py
@@ -37,11 +37,11 @@
     nz, ny, nx,
     x_hbm, w_hbm, q_hbm, f_hbm, go_hbm, lb_hbm,
     gq_out, gf_out, gx_out, gw_out,
-    x_v, w_v, q_v, f_v, go_v, lb_v, wide, thin,
-    s_send, e_send, s_buf, e_buf, l_send, q_state, q_grad, q_line, t_send, ft_send, t_buf, ft_buf, o_send, p_buf, p_both, outer,
+    x_v, w_v, q_v, f_v, go_v, lb_v, wide, thin, broad,
+    s_send, e_send, s_buf, e_buf, l_send, lg_send, q_grad, q_line, t_send, ft_send, t_buf, ft_buf, held_out, o_send, p_buf, p_both, outer, st_send, st_buf,
     xt, xtl, r_send, rl, k_send, kl, own_send, ownl, g_all, ig, ig_recv,
     m_send, m_recv, aacc, a_send, a_recv, w2, z_send, z_recv,
-    lsem, s_ss, s_rs, e_ss, e_rs, ea_ss, ea_rs, q_ss, q_rs, t_ss, t_rs, ft_ss, ft_rs, p_ss, p_rs,
+    lsem, s_ss, s_rs, e_ss, e_rs, ea_ss, ea_rs, q_ss, q_rs, t_ss, t_rs, ft_ss, ft_rs, p_ss, p_rs, st_ss, st_rs,
     xt_ss, xt_rs, r_ss, r_rs, k_ss, k_rs, own_ss, own_rs,
     m_ss, m_rs, a_ss, a_rs, z_ss, z_rs, ig_ss, ig_rs,
 ):
@@ -71,9 +71,6 @@
     def column(i):
         return (z, i * (1 - c) + y * c, x * (1 - c) + i * c, c)
 
-    def spot(g, i):
-        return lax.rem(i, nx) * ny + lax.div(i, nx) if g else i
-
     def piece_of(ty, tx):
         return ty * (nx // 2) + lax.div(tx, 2) + lax.rem(tx + ty, 2) * (pln // 2)
 
@@ -107,16 +104,16 @@
             pl.semaphore_signal(barrier, inc=1, device_id=device, device_id_type=LOGICAL)
 
         for ty, tx in others:
-            greet((z, ty, tx, 1 - c))
+            greet((z, ty, tx, 1))
         for d in z_steps:
             greet((zs[d], y, x, 1))
 
         @pl.when(c == 1)
         def _():
+            for ty, tx in others:
+                greet((z, ty, tx, 0))
             for d in z_steps:
                 greet((zs[d], y, x, 0))
-            for ty, tx in others:
-                greet((z, ty, tx, 1))
 
         @pl.when(c == 0)
         def _():
@@ -181,11 +178,13 @@
         for k in far_first:
             rcopy(source, target.at[at_line], send_sem, recv_sem, line(lines[k])).start()
 
+    def column_send(source, target, send_sem, recv_sem, to):
+        device = (z, to * (1 - c) + y * c, x * (1 - c) + to * c, 1)
+        return rcopy(source.at[to], target.at[c * ny + at_col], send_sem, recv_sem.at[c], device)
+
     def to_column(source, target, send_sem, recv_sem):
         for k in far_first:
-            to = columns[k]
-            device = (z, to * (1 - c) + y * c, x * (1 - c) + to * c, 1)
-            rcopy(source.at[to], target.at[c * ny + at_col], send_sem, recv_sem.at[c], device).start()
+            column_send(source, target, send_sem, recv_sem, columns[k]).start()
 
         @pl.when(c == 0)
         def _():
@@ -212,9 +211,15 @@
 
     mine = piece_of(y, x)
     with scope("send1"):
-        for ty, tx in others:
-            for copy in piece_sends(ty, tx):
-                copy.start()
+        for parity in (0, 1):
+
+            @pl.when(back == parity)
+            def _():
+                for want in (1 - parity, parity):
+                    for (dy, dx), target in zip(steps, others):
+                        if (dy + dx) % 2 == want:
+                            for copy in piece_sends(*target):
+                                copy.start()
 
         @pl.when(c == 0)
         def _():
@@ -274,15 +279,11 @@
             rcopy(t_send, t_buf.at[z], t_ss, t_rs, (to, y, x, 1)),
         )
 
-    def carry_send(g, ty, tx, backward):
+    def carry_send(g, ty, tx):
         device = (z, ty, tx, g)
-        if not backward:
-            at = pln + tx * ny + ty if g else ty * nx + tx
-            return rcopy(l_send.at[at], q_state.at[me // 2], q_ss.at[g], q_rs.at[0], device)
         if g == 0:
-            return rcopy(l_send.at[ty * nx + nx - 1], q_line.at[me // 2], q_ss.at[0], q_rs.at[1], device)
-        rows_of = pl.ds(pln + tx * ny, ny)
-        return rcopy(l_send.at[rows_of], q_grad.at[pl.ds(me // 2 * ny, ny)], q_ss.at[1], q_rs.at[1], device)
+            return rcopy(l_send.at[ty * nx + nx - 1], q_line.at[me // 2], q_ss.at[0], q_rs, device)
+        return rcopy(lg_send.at[tx], q_grad.at[me // 2], q_ss.at[1], q_rs, device)
 
     targets = [(0, *t) for t in everyone] + [(1, *t) for t in others]
     plane_decays = e_buf.at[pl.ds(0, pln)]
@@ -294,17 +295,24 @@
             arrived(e_buf, 2 * pln - 1, e_rs)
             arrived(s_buf, 2 * pln - 1, s_rs)
         with scope("scan1"):
-            for g in (0, 1):
-                held = jnp.zeros(t_send.shape[1:], F32)
-                factor = jnp.ones((1, ch), F32)
-                for o in range(pln):
-                    it = o + back * (pln - 1 - 2 * o)
-                    l_send[g * pln + spot(g, it)] = held.astype(BF16)
-                    decay = e_buf[g * pln + it]
-                    held = decay * held + s_buf[g * pln + it].astype(F32)
-                    factor = decay * factor
-                t_send[g] = held.astype(BF16)
-                ft_send[g] = factor
+            for parity in (0, 1):
+
+                @pl.when(back == parity)
+                def _():
+                    for g in (0, 1):
+                        held = jnp.zeros(t_send.shape[1:], F32)
+                        factor = jnp.ones((1, ch), F32)
+                        for it in range(pln - 1, -1, -1) if parity else range(pln):
+                            if g and parity:
+                                lg_send[it % nx, :, ch * (it // nx) : ch * (it // nx + 1)] = held.astype(BF16)
+                            else:
+                                l_send[g * pln + it] = held.astype(BF16)
+                            decay = e_buf[g * pln + it]
+                            held = decay * held + s_buf[g * pln + it].astype(F32)
+                            factor = decay * factor
+                        t_send[g] = held.astype(BF16)
+                        ft_send[g] = factor
+
         with scope("send2"):
             for k in range(1, nz):
 
@@ -316,8 +324,8 @@
             @pl.when(back == 1)
             def _():
                 for target in targets:
-                    carry_send(*target, 1).start()
-                q_grad[pl.ds(me // 2 * ny, ny)] = l_send[pl.ds(pln + x * ny, ny)]
+                    carry_send(*target).start()
+                q_grad[me // 2] = lg_send[x]
 
             to_line(own_send, ownl, own_ss, own_rs)
             e_all.start()
@@ -333,10 +341,9 @@
             e_all.wait_recv()
 
         decays = e_buf[pl.ds(c * pln, pln)]
-        before, after = jnp.ones((1, ch), F32), [jnp.ones((1, ch), F32)] * nx
+        after = [jnp.ones((1, ch), F32)] * nx
         ids = [line(i)[1] * nx + line(i)[2] for i in range(nx)]
         for i in range(pln):
-            before = before * jnp.where(i < me, decays[i], 1.0)
             after = [a * jnp.where(i > n, decays[i], 1.0) for a, n in zip(after, ids)]
 
     with scope("wait_line"):
@@ -366,8 +373,11 @@
 
     def plane_send(g, ty, tx):
         if g:
-            return rcopy(o_send, p_both.at[mine], p_ss, p_rs, (z, ty, tx, 1))
-        return rcopy(o_send.at[0], p_buf.at[mine], p_ss, p_rs, (z, ty, tx, 0))
+            return rcopy(o_send, p_both.at[me // 2], p_ss, p_rs, (z, ty, tx, 1))
+        return rcopy(o_send.at[0], p_buf.at[me // 2], p_ss, p_rs, (z, ty, tx, 0))
+
+    def state_send(g, ty, tx):
+        return rcopy(st_send.at[g * pln + ty * nx + tx], st_buf.at[me // 2], st_ss, st_rs, (z, ty, tx, g))
 
     @pl.when(c == 1)
     def _():
@@ -381,31 +391,28 @@
 
             carried = lax.fori_loop(0, z_order, arriving, jnp.zeros(t_send.shape, F32))
         with scope("send3"):
+            held_out[...] = carried
             o_send[...] = carried.astype(BF16)
-            for target in targets[pln:] + targets[:pln]:
-                plane_send(*target).start()
-            p_both[mine] = o_send[...]
-
-            @pl.when(back == 0)
+
+            @pl.when(back == 1)
             def _():
-                for target in targets:
-                    carry_send(*target, 0).start()
-                q_state[me // 2] = l_send[pln + x * ny + y]
-
+                for target in targets[pln:] + targets[:pln]:
+                    plane_send(*target).start()
+                p_both[me // 2] = o_send[...]
 
     some = pln // 2
     with scope("wait_1b"):
 
         @pl.when(c == 0)
         def _():
-            arrived(q_line, some, q_rs.at[1])
+            arrived(q_line, some, q_rs)
             arrived(rl, nx - 1, r_rs)
 
         for odd in (0, 1):
 
             @pl.when((c == 1) & (back == odd))
             def _():
-                arrived(q_grad, (some - odd) * ny, q_rs.at[1])
+                arrived(q_grad, some - odd, q_rs)
 
     with scope("line_a"):
 
@@ -420,8 +427,7 @@
         @pl.when(c == 1)
         def _():
             for i in range(nx):
-                part = [q_grad[j * ny + i].astype(F32) for j in range(some)]
-                g_all[i] = jnp.concatenate(part, axis=0)
+                g_all[i] = q_grad[:, :, ch * i : ch * (i + 1)].astype(F32).reshape(HEAD, ch)
 
         parts = []
         for i in range(nx):
@@ -432,27 +438,58 @@
         arrived(ownl, nx - 1, own_rs)
     with scope("line_a2"):
         parts = pairs([(ownl[i].astype(F32) + part).astype(BF16) for i, part in enumerate(parts)])
-        a_sum = nt(parts[0], turned_of[0])
-        for a, b in zip(parts[1:], turned_of[1:]):
-            a_sum = a_sum + nt(a, b)
-        to_chunks(aacc, a_sum)
-        to_chunks(a_send, a_sum)
-        to_column(a_send, a_recv, a_ss, a_rs)
+        def chunk_of(to):
+            pieces = pairs([xtl[i, to].reshape(nz * rows, tok) for i in range(nx)])
+            chunk = nt(parts[0], pieces[0])
+            for a, b in zip(parts[1:], pieces[1:]):
+                chunk = chunk + nt(a, b)
+            return chunk
+
+        for ks in (far_first[:1], far_first[1:] + [0]):
+            chunks = [chunk_of(columns[k]) for k in ks]
+            for k, chunk in zip(ks, chunks):
+                a_send[columns[k]] = chunk.astype(BF16)
+                if not k:
+                    aacc[...] = chunk
+            for k in ks:
+                if k:
+                    column_send(a_send, a_recv, a_ss, a_rs, columns[k]).start()
+
+        @pl.when(c == 0)
+        def _():
+            rcopy(a_send.at[y], a_recv.at[y], a_ss, a_rs.at[0], (z, y, x, 1)).start()
+
+    @pl.when((c == 1) & (back == 0))
+    def _():
+        with scope("states"):
+            for g in (0, 1):
+                start = held_out[g]
+                for i in range(pln):
+                    st_send[g * pln + i] = (l_send[g * pln + i].astype(F32) + start).astype(BF16)
+                    start = e_buf[g * pln + i] * start
+            for target in targets:
+                state_send(*target).start()
+            st_buf[me // 2] = st_send[pln + me]
 
     @pl.when(c == 1)
     def _():
         with scope("wait_m1"):
             m_plane = from_column(1, m_send.at[x], m_recv, m_rs).astype(BF16)
         with scope("wait3"):
-            arrived(p_both, pln - 1, p_rs)
+            for odd in (0, 1):
+
+                @pl.when(back == odd)
+                def _():
+                    arrived(p_both, some - odd, p_rs)
+
         for g in (1, 0):
-            outer[g] = p_both[:, g].astype(F32).reshape(2 * HEAD, ch)
-            bd_out = by_head((outer[g, HEAD:] * m).astype(BF16) for m in mf)
+            outer[g] = p_both[:, g].astype(F32).reshape(HEAD, ch)
+            bd_out = by_head((outer[g] * m).astype(BF16) for m in mf)
             with scope(f"wait_a{g}"):
                 if g == 0:
                     m_plane = from_column(0, None, m_recv, m_rs).astype(BF16)
                 w_sum = nt(m_plane, bd_out)
-                w_sum = w_sum + from_column(g, aacc.at[x], a_recv, a_rs)
+                w_sum = w_sum + from_column(g, aacc, a_recv, a_rs)
             with scope(f"send_z{g}"):
                 if g:
                     w2[...] = w_sum.reshape(w2.shape)
@@ -463,24 +500,14 @@
     @pl.when(c == 0)
     def _():
         with scope("wait3"):
-            arrived(p_buf, pln, p_rs)
-        outer[0] = p_buf[...].astype(F32).reshape(2 * HEAD, ch)
+            arrived(p_buf, some, p_rs)
+        outer[0] = p_buf[...].astype(F32).reshape(HEAD, ch)
 
     with scope("value_grad"):
-        for even in (0, 1):
-
-            @pl.when((1 - back) * c == even)
-            def _():
-                arrived(q_state, some - even, q_rs.at[0])
-
-        state_in = q_state[...].astype(F32).reshape(HEAD, ch)
-        state_out, grad_out = outer[c, :HEAD], outer[c, HEAD:]
         own_after = after[nx - 1]
         for i in range(nx - 1):
             own_after = jnp.where(at_line == i, after[i], own_after)
-        state = state_in + before * state_out
-        grad = g_all[at_line] + own_after * grad_out
-        bd_state = by_head((state * m).astype(BF16) for m in mf)
+        grad = g_all[at_line] + own_after * outer[c]
         bd_grad = by_head((grad * m).astype(BF16) for m in mf)
         value_grad = (gv_own + nn(bd_grad, k_end)).astype(BF16)
 
@@ -494,6 +521,14 @@
         ig_copy.start()
 
     with scope("query_forget"):
+        for even in (0, 1):
+
+            @pl.when((1 - back) * c == even)
+            def _():
+                arrived(st_buf, some - even, st_rs)
+
+        state = st_buf[...].astype(F32).reshape(HEAD, ch)
+        bd_state = by_head((state * m).astype(BF16) for m in mf)
         g_query = growth * (gq_own + tn(bd_state, go))
         g_key = shrink * gk_own + remain * tn(bd_grad, v)
         gq_out[...] = (g_query * (q_sig * (1.0 + q * (1.0 - q_sig)))).astype(BF16)
@@ -539,15 +574,17 @@
                     left(ft_buf, n, ft_ss)
                     left(t_buf, n, t_ss)
 
-            left(wide, pln, q_ss.at[0])
-            for backward in (0, 1):
-
-                @pl.when(back == backward)
-                def _():
-                    left(wide, (pln - 1) * (ny if backward else 1), q_ss.at[1])
-
             e_all.wait_send()
-            left(wide, 3 * pln - 2, p_ss)
+
+            @pl.when(back == 1)
+            def _():
+                left(wide, pln, q_ss.at[0])
+                left(broad, pln - 1, q_ss.at[1])
+                left(wide, 3 * pln - 2, p_ss)
+
+            @pl.when(back == 0)
+            def _():
+                left(st_send, 2 * pln - 1, st_ss)
 
     with scope("wait_z"):
 
@@ -588,14 +625,16 @@
         vm((tok, d_model), BF16), vm((ch, d_model), BF16),
         vm((ch, tok), BF16), vm((ch, tok), BF16), vm((ch, tok), BF16), vm((1, ch), F32),
         vm((pln * (ny + 1), piece, ch), BF16), vm((pln, 1, ch), F32),
+        vm((pln, piece, ny * ch), BF16),
         vm((pln, piece, ch), BF16), vm((1, ch), F32),
         vm((2 * pln, piece, ch), BF16), vm((2 * pln, 1, ch), F32),
-        vm((2 * pln, piece, ch), BF16), vm((pln // 2, piece, ch), BF16), vm((pln // 2 * ny, piece, ch), BF16),
-        vm((pln // 2, piece, ch), BF16),
+        vm((2 * pln, piece, ch), BF16), vm((nx, piece, ny * ch), BF16),
+        vm((pln // 2, piece, ny * ch), BF16), vm((pln // 2, piece, ch), BF16),
         vm((2, piece, ch), BF16), vm((2, 1, ch), F32),
         vm((nz, 2, piece, ch), BF16), vm((nz, 2, 1, ch), F32),
-        vm((2, piece, ch), BF16), vm((pln, piece, ch), BF16), vm((pln, 2, piece, ch), BF16),
-        vm((2, 2 * HEAD, ch), F32),
+        vm((2, piece, ch), F32), vm((2, piece, ch), BF16),
+        vm((pln // 2, piece, ch), BF16), vm((pln // 2, 2, piece, ch), BF16),
+        vm((2, HEAD, ch), F32), vm((2 * pln, piece, ch), BF16), vm((pln // 2, piece, ch), BF16),
         vm((nx, ny, nz, rows, tok), BF16), vm((nx, ny, nz, rows, tok), BF16),
         vm((HEAD, ch), BF16), vm((nx, HEAD, ch), BF16),
         vm((ch, tok), BF16), vm((nx, ch, tok), BF16),
@@ -603,11 +642,11 @@
         vm((nx, HEAD, ch), F32),
         vm((2, tok // 2, d_model), BF16), vm((tok // 2, d_model), BF16),
         vm((ny, ch, nz * rows), BF16), vm((2 * ny, ch, nz * rows), BF16),
-        vm((ny, ch, nz * rows), F32), vm((ny, ch, nz * rows), BF16), vm((2 * ny, ch, nz * rows), BF16),
+        vm((ch, nz * rows), F32), vm((ny, ch, nz * rows), BF16), vm((2 * ny, ch, nz * rows), BF16),
         vm((nz, rows, ch), F32), vm((2 * nz, rows, ch), BF16), vm((nz, rows, ch), BF16),
         dma((6,)),
-        *(dma for _ in range(6)), dma((2,)), dma((2,)),
-        *(dma for _ in range(4 + 2 + 8)),
+        *(dma for _ in range(6)), dma((2,)), dma,
+        *(dma for _ in range(4 + 2 + 2 + 8)),
         dma, dma((2,)), dma, dma((2,)), dma, dma, dma, dma,
     ]
     hbm, near = pl.BlockSpec(memory_space=pl.ANY), pl.BlockSpec(memory_space=pltpu.VMEM)

time: 30.3 us -> 30.4 us (level)
  no operation moved by 1% of the time
where the time goes in v12:
time: 30.4 us; the launch traced here: 30.3 us
  Pallas kernels  29.7 us (98%)
  between operations  0.64 us (2%)
    pallas_call x1, Pallas kernels, on_device(): pl.pallas_call(functools.partial(kernel, nz, ny, nx), out_shape=(vm((ch,...  28.9 us
    pallas_call x1, Pallas kernels, on_device(): pl.pallas_call(write_out, out_shape=tuple((jax.ShapeDtypeStruct(a.shape,...  0.77 us

profile of v12, /device:TPU:1, one launch (start us, length us, event | category | flops | bytes accessed | tf_op | source)
XLA Modules:
  0.0 30.3 jit_solution(12179113016714125545)
XLA Ops:
  0.6 28.9 %shard_map.93 = (bf16[192,128]{1,0:T(8,128)(2,1)S(1)}, bf16[192,128]{1,0:T(8,128)(2,1)S(1)}, bf16[64,2048]{1,0:T(8,128)(2,1)S(1)}, f32[16,192]{1,0:T(8,128)S(1)}) custom-call(bf16[128,2048]{1,0:T(8,128)(2,1)} %x_hbm.1, bf16[192,2048]{1,0:T(8,128)(2,1)} %bitcast.7, bf16[192,128]{1,0:T(8,128)(2,1)} %bitcast.8, bf16[192,128]{1,0:T(8,128)(2,1)} %bitcast.9, ...), custom_call_target="tpu_custom_call" | custom-call | tf_op jit(solution)/shard_map/pallas_call | solution.py:653
  29.6 0.8 %shard_map.94 = (bf16[192,128]{1,0:T(8,128)(2,1)}, bf16[192,128]{1,0:T(8,128)(2,1)}, bf16[64,2048]{1,0:T(8,128)(2,1)}, f32[16,192]{1,0:T(8,128)}) custom-call(bf16[192,128]{1,0:T(8,128)(2,1)S(1)} %get-tuple-element.12.refs_0_, bf16[192,128]{1,0:T(8,128)(2,1)S(1)} %get-tuple-element.13.refs_1_, bf16[64,2048]{1,0:T(8,128)(2,1)S(1)} %get-tuple-element.14.refs_2_, ...), custom_call_target="tpu_custom_call" | custom-call | tf_op jit(solution)/shard_map/pallas_call | solution.py:666

commit v13 on v12

--- a/solution.py
+++ b/solution.py
@@ -103,24 +103,20 @@
         def greet(device):
             pl.semaphore_signal(barrier, inc=1, device_id=device, device_id_type=LOGICAL)
 
-        for ty, tx in others:
-            greet((z, ty, tx, 1))
+        @pl.when(c == 1)
+        def _():
+            for ty, tx in others:
+                greet((z, ty, tx, 1))
+            for ty, tx in everyone:
+                greet((z, ty, tx, 0))
+
+        @pl.when(c == 0)
+        def _():
+            for tx in xs[1:]:
+                greet((z, y, tx, 0))
+
         for d in z_steps:
             greet((zs[d], y, x, 1))
-
-        @pl.when(c == 1)
-        def _():
-            for ty, tx in others:
-                greet((z, ty, tx, 0))
-            for d in z_steps:
-                greet((zs[d], y, x, 0))
-
-        @pl.when(c == 0)
-        def _():
-            for tx in xs[1:]:
-                greet((z, y, tx, 0))
-
-        greet((z, y, x, 1 - c))
 
     lane = lax.broadcasted_iota(jnp.int32, (1, ch), 1)
     mf = [jnp.where((lane >= HEAD * h) & (lane < HEAD * (h + 1)), 1.0, 0.0).astype(F32) for h in range(heads)]
@@ -172,7 +168,7 @@
         k_send[...] = k_end
 
     with scope("barrier_wait"):
-        pl.semaphore_wait(barrier, pln + nz - 1 + c * (pln + nz - 2) + (1 - c) * (nx - 1))
+        pl.semaphore_wait(barrier, c * (pln - 1 + 2 * (nz - 1)) + (1 - c) * (pln + nx - 1))
 
     def to_line(source, target, send_sem, recv_sem):
         for k in far_first:

time: 30.4 us -> 29.9 us (0.984)
  Pallas kernels: 29.7 us -> 29.1 us
    pallas_call x1, Pallas kernels: 28.9 us -> 28.3 us  [on_device(): pl.pallas_call(functools.partial(kernel, nz, ny, nx), out_shape=(vm((ch,...]
where the time goes in v13:
time: 29.9 us; the launch traced here: 29.7 us
  Pallas kernels  29.1 us (97%)
  between operations  0.64 us (2%)
    pallas_call x1, Pallas kernels, on_device(): pl.pallas_call(functools.partial(kernel, nz, ny, nx), out_shape=(vm((ch,...  28.3 us
    pallas_call x1, Pallas kernels, on_device(): pl.pallas_call(write_out, out_shape=tuple((jax.ShapeDtypeStruct(a.shape,...  0.77 us

profile of v13, /device:TPU:1, one launch (start us, length us, event | category | flops | bytes accessed | tf_op | source)
XLA Modules:
  0.0 29.7 jit_solution(11640060339775687097)
XLA Ops:
  0.6 28.3 %shard_map.93 = (bf16[192,128]{1,0:T(8,128)(2,1)S(1)}, bf16[192,128]{1,0:T(8,128)(2,1)S(1)}, bf16[64,2048]{1,0:T(8,128)(2,1)S(1)}, f32[16,192]{1,0:T(8,128)S(1)}) custom-call(bf16[128,2048]{1,0:T(8,128)(2,1)} %x_hbm.1, bf16[192,2048]{1,0:T(8,128)(2,1)} %bitcast.7, bf16[192,128]{1,0:T(8,128)(2,1)} %bitcast.8, bf16[192,128]{1,0:T(8,128)(2,1)} %bitcast.9, ...), custom_call_target="tpu_custom_call" | custom-call | tf_op jit(solution)/shard_map/pallas_call | solution.py:649
  29.0 0.8 %shard_map.94 = (bf16[192,128]{1,0:T(8,128)(2,1)}, bf16[192,128]{1,0:T(8,128)(2,1)}, bf16[64,2048]{1,0:T(8,128)(2,1)}, f32[16,192]{1,0:T(8,128)}) custom-call(bf16[192,128]{1,0:T(8,128)(2,1)S(1)} %get-tuple-element.12.refs_0_, bf16[192,128]{1,0:T(8,128)(2,1)S(1)} %get-tuple-element.13.refs_1_, bf16[64,2048]{1,0:T(8,128)(2,1)S(1)} %get-tuple-element.14.refs_2_, ...), custom_call_target="tpu_custom_call" | custom-call | tf_op jit(solution)/shard_map/pallas_call | solution.py:662

commit v14 on v13

--- a/solution.py
+++ b/solution.py
@@ -164,7 +164,9 @@
         v = nt(w_v[...], x_v[...]).astype(BF16)
         update = folded(nt(v, k_end))
         s_send[...] = jnp.concatenate([update, reach], axis=0).reshape(s_send.shape).astype(BF16)
-        r_send[...] = reach.astype(BF16)
+        narrow, low_half = 2 * HEAD, HEAD // 2
+        rest = jnp.concatenate([reach[:low_half, narrow:], reach[low_half:, narrow:]], axis=1)
+        r_send[...] = jnp.concatenate([reach[:, :narrow], rest], axis=0).astype(BF16)
         k_send[...] = k_end
 
     with scope("barrier_wait"):
@@ -417,7 +419,11 @@
             grad_at = q_line[...].astype(F32).reshape(HEAD, ch)
             g_all[nx - 1] = grad_at
             for i in range(nx - 2, -1, -1):
-                grad_at = e_buf[y * nx + i + 1] * grad_at + rl[i + 1].astype(F32)
+                near_reach = rl[i + 1].astype(F32)
+                rest = near_reach[HEAD:]
+                rest = jnp.concatenate([rest[:, :HEAD], rest[:, HEAD:]], axis=0)
+                near_reach = jnp.concatenate([near_reach[:HEAD], rest], axis=1)
+                grad_at = e_buf[y * nx + i + 1] * grad_at + near_reach
                 g_all[i] = grad_at
 
         @pl.when(c == 1)
@@ -470,7 +476,7 @@
     @pl.when(c == 1)
     def _():
         with scope("wait_m1"):
-            m_plane = from_column(1, m_send.at[x], m_recv, m_rs).astype(BF16)
+            m_plane = [from_column(g, m_send.at[x], m_recv, m_rs).astype(BF16) for g in (0, 1)]
         with scope("wait3"):
             for odd in (0, 1):
 
@@ -478,14 +484,14 @@
                 def _():
                     arrived(p_both, some - odd, p_rs)
 
+            from_plane = []
+            for g in (0, 1):
+                outer[g] = p_both[:, g].astype(F32).reshape(HEAD, ch)
+                bd_out = by_head((outer[g] * m).astype(BF16) for m in mf)
+                from_plane.append(nt(m_plane[g], bd_out))
         for g in (1, 0):
-            outer[g] = p_both[:, g].astype(F32).reshape(HEAD, ch)
-            bd_out = by_head((outer[g] * m).astype(BF16) for m in mf)
             with scope(f"wait_a{g}"):
-                if g == 0:
-                    m_plane = from_column(0, None, m_recv, m_rs).astype(BF16)
-                w_sum = nt(m_plane, bd_out)
-                w_sum = w_sum + from_column(g, aacc, a_recv, a_rs)
+                w_sum = from_plane[g] + from_column(g, aacc, a_recv, a_rs)
             with scope(f"send_z{g}"):
                 if g:
                     w2[...] = w_sum.reshape(w2.shape)
@@ -632,7 +638,7 @@
         vm((pln // 2, piece, ch), BF16), vm((pln // 2, 2, piece, ch), BF16),
         vm((2, HEAD, ch), F32), vm((2 * pln, piece, ch), BF16), vm((pln // 2, piece, ch), BF16),
         vm((nx, ny, nz, rows, tok), BF16), vm((nx, ny, nz, rows, tok), BF16),
-        vm((HEAD, ch), BF16), vm((nx, HEAD, ch), BF16),
+        vm((ch // 2, 2 * HEAD), BF16), vm((nx, ch // 2, 2 * HEAD), BF16),
         vm((ch, tok), BF16), vm((nx, ch, tok), BF16),
         vm((ch, tok), BF16), vm((nx, ch, tok), BF16),
         vm((nx, HEAD, ch), F32),

time: 29.9 us -> 29.9 us (level)
  no operation moved by 1% of the time
where the time goes in v14:
time: 29.9 us; the launch traced here: 29.8 us
  Pallas kernels  29.2 us (98%)
  between operations  0.64 us (2%)
    pallas_call x1, Pallas kernels, on_device(): pl.pallas_call(functools.partial(kernel, nz, ny, nx), out_shape=(vm((ch,...  28.4 us
    pallas_call x1, Pallas kernels, on_device(): pl.pallas_call(write_out, out_shape=tuple((jax.ShapeDtypeStruct(a.shape,...  0.77 us

profile of v14, /device:TPU:1, one launch (start us, length us, event | category | flops | bytes accessed | tf_op | source)
XLA Modules:
  0.0 29.8 jit_solution(17902437349002076005)
XLA Ops:
  0.6 28.4 %shard_map.93 = (bf16[192,128]{1,0:T(8,128)(2,1)S(1)}, bf16[192,128]{1,0:T(8,128)(2,1)S(1)}, bf16[64,2048]{1,0:T(8,128)(2,1)S(1)}, f32[16,192]{1,0:T(8,128)S(1)}) custom-call(bf16[128,2048]{1,0:T(8,128)(2,1)} %x_hbm.1, bf16[192,2048]{1,0:T(8,128)(2,1)} %bitcast.7, bf16[192,128]{1,0:T(8,128)(2,1)} %bitcast.8, bf16[192,128]{1,0:T(8,128)(2,1)} %bitcast.9, ...), custom_call_target="tpu_custom_call" | custom-call | tf_op jit(solution)/shard_map/pallas_call | solution.py:655
  29.0 0.8 %shard_map.94 = (bf16[192,128]{1,0:T(8,128)(2,1)}, bf16[192,128]{1,0:T(8,128)(2,1)}, bf16[64,2048]{1,0:T(8,128)(2,1)}, f32[16,192]{1,0:T(8,128)}) custom-call(bf16[192,128]{1,0:T(8,128)(2,1)S(1)} %get-tuple-element.12.refs_0_, bf16[192,128]{1,0:T(8,128)(2,1)S(1)} %get-tuple-element.13.refs_1_, bf16[64,2048]{1,0:T(8,128)(2,1)S(1)} %get-tuple-element.14.refs_2_, ...), custom_call_target="tpu_custom_call" | custom-call | tf_op jit(solution)/shard_map/pallas_call | solution.py:668

commit v15 on v14

--- a/solution.py
+++ b/solution.py
@@ -125,6 +125,12 @@
     lower, upper = row >= col, col >= row
     lower_ones = jnp.where(lower, 1.0, 0.0).astype(BF16)
     upper_ones = jnp.where(upper, 1.0, 0.0).astype(BF16)
+
+    mb = [m.astype(BF16) for m in mf]
+
+    def block_diagonal(a):
+        a = a.astype(BF16)
+        return by_head(a * m for m in mb)
 
     def folded(full):
         out = full[:HEAD] * mf[0]
@@ -434,7 +440,7 @@
         parts = []
         for i in range(nx):
             grad_at = g_all[i]
-            bd_in = by_head((grad_at * m).astype(BF16) for m in mf)
+            bd_in = block_diagonal(grad_at)
             parts.append(nn(bd_in, kl[i]))
     with scope("wait_own"):
         arrived(ownl, nx - 1, own_rs)
@@ -487,15 +493,19 @@
             from_plane = []
             for g in (0, 1):
                 outer[g] = p_both[:, g].astype(F32).reshape(HEAD, ch)
-                bd_out = by_head((outer[g] * m).astype(BF16) for m in mf)
+                bd_out = block_diagonal(outer[g])
                 from_plane.append(nt(m_plane[g], bd_out))
         for g in (1, 0):
             with scope(f"wait_a{g}"):
                 w_sum = from_plane[g] + from_column(g, aacc, a_recv, a_rs)
             with scope(f"send_z{g}"):
+                wide_part = w_sum[:, : 2 * HEAD].reshape(nz, rows, 2 * HEAD)
+                rest = w_sum[:, 2 * HEAD :].reshape(nz, 2, rows // 2, HEAD)
+                rest = jnp.concatenate([rest[:, 0], rest[:, 1]], axis=2)
+                packed = jnp.concatenate([wide_part, rest], axis=1)
                 if g:
-                    w2[...] = w_sum.reshape(w2.shape)
-                z_send[pl.ds(g * nz, nz)] = w_sum.astype(BF16).reshape(nz, rows, ch)
+                    w2[...] = packed
+                z_send[pl.ds(g * nz, nz)] = packed.astype(BF16)
                 for d in z_steps if g else z_steps + [0]:
                     rcopy(z_send.at[g * nz + zs[d]], z_recv.at[z], z_ss, z_rs, (zs[d], y, x, g)).start()
 
@@ -510,7 +520,7 @@
         for i in range(nx - 1):
             own_after = jnp.where(at_line == i, after[i], own_after)
         grad = g_all[at_line] + own_after * outer[c]
-        bd_grad = by_head((grad * m).astype(BF16) for m in mf)
+        bd_grad = block_diagonal(grad)
         value_grad = (gv_own + nn(bd_grad, k_end)).astype(BF16)
 
     with scope("input_grad"):
@@ -530,7 +540,7 @@
                 arrived(st_buf, some - even, st_rs)
 
         state = st_buf[...].astype(F32).reshape(HEAD, ch)
-        bd_state = by_head((state * m).astype(BF16) for m in mf)
+        bd_state = block_diagonal(state)
         g_query = growth * (gq_own + tn(bd_state, go))
         g_key = shrink * gk_own + remain * tn(bd_grad, v)
         gq_out[...] = (g_query * (q_sig * (1.0 + q * (1.0 - q_sig)))).astype(BF16)
@@ -588,6 +598,11 @@
             def _():
                 left(st_send, 2 * pln - 1, st_ss)
 
+    def unpacked(total):
+        gw_out[:, : 2 * HEAD] = total[:rows]
+        gw_out[: rows // 2, 2 * HEAD :] = total[rows:, :HEAD]
+        gw_out[rows // 2 :, 2 * HEAD :] = total[rows:, HEAD:]
+
     with scope("wait_z"):
 
         @pl.when(c == 0)
@@ -596,7 +611,7 @@
             w_last = z_recv[0].astype(F32)
             for k in range(1, nz):
                 w_last = w_last + z_recv[k].astype(F32)
-            gw_out[...] = w_last
+            unpacked(w_last)
 
         @pl.when(c == 1)
         def _():
@@ -604,7 +619,7 @@
             w_last = w2[z]
             for k in range(1, nz):
                 w_last = w_last + z_recv[zs[k]].astype(F32)
-            gw_out[...] = w_last
+            unpacked(w_last)
             left(z_send, 2 * nz - 1, z_ss)
 
 
@@ -645,7 +660,8 @@
         vm((2, tok // 2, d_model), BF16), vm((tok // 2, d_model), BF16),
         vm((ny, ch, nz * rows), BF16), vm((2 * ny, ch, nz * rows), BF16),
         vm((ch, nz * rows), F32), vm((ny, ch, nz * rows), BF16), vm((2 * ny, ch, nz * rows), BF16),
-        vm((nz, rows, ch), F32), vm((2 * nz, rows, ch), BF16), vm((nz, rows, ch), BF16),
+        vm((nz, rows * 3 // 2, 2 * HEAD), F32),
+        vm((2 * nz, rows * 3 // 2, 2 * HEAD), BF16), vm((nz, rows * 3 // 2, 2 * HEAD), BF16),
         dma((6,)),
         *(dma for _ in range(6)), dma((2,)), dma,
         *(dma for _ in range(4 + 2 + 2 + 8)),

time: 29.9 us -> 30 us (level)
  no operation moved by 1% of the time
where the time goes in v15:
time: 30 us; the launch traced here: 29.9 us
  Pallas kernels  29.3 us (98%)
  between operations  0.64 us (2%)
    pallas_call x1, Pallas kernels, on_device(): pl.pallas_call(functools.partial(kernel, nz, ny, nx), out_shape=(vm((ch,...  28.5 us
    pallas_call x1, Pallas kernels, on_device(): pl.pallas_call(write_out, out_shape=tuple((jax.ShapeDtypeStruct(a.shape,...  0.77 us

profile of v15, /device:TPU:1, one launch (start us, length us, event | category | flops | bytes accessed | tf_op | source)
XLA Modules:
  0.0 29.9 jit_solution(13553812466446308255)
XLA Ops:
  0.6 28.5 %shard_map.93 = (bf16[192,128]{1,0:T(8,128)(2,1)S(1)}, bf16[192,128]{1,0:T(8,128)(2,1)S(1)}, bf16[64,2048]{1,0:T(8,128)(2,1)S(1)}, f32[16,192]{1,0:T(8,128)S(1)}) custom-call(bf16[128,2048]{1,0:T(8,128)(2,1)} %x_hbm.1, bf16[192,2048]{1,0:T(8,128)(2,1)} %bitcast.7, bf16[192,128]{1,0:T(8,128)(2,1)} %bitcast.8, bf16[192,128]{1,0:T(8,128)(2,1)} %bitcast.9, ...), custom_call_target="tpu_custom_call" | custom-call | tf_op jit(solution)/shard_map/pallas_call | solution.py:671
  29.2 0.8 %shard_map.94 = (bf16[192,128]{1,0:T(8,128)(2,1)}, bf16[192,128]{1,0:T(8,128)(2,1)}, bf16[64,2048]{1,0:T(8,128)(2,1)}, f32[16,192]{1,0:T(8,128)}) custom-call(bf16[192,128]{1,0:T(8,128)(2,1)S(1)} %get-tuple-element.12.refs_0_, bf16[192,128]{1,0:T(8,128)(2,1)S(1)} %get-tuple-element.13.refs_1_, bf16[64,2048]{1,0:T(8,128)(2,1)S(1)} %get-tuple-element.14.refs_2_, ...), custom_call_target="tpu_custom_call" | custom-call | tf_op jit(solution)/shard_map/pallas_call | solution.py:684

commit v16 on v15

--- a/solution.py
+++ b/solution.py
@@ -453,7 +453,7 @@
                 chunk = chunk + nt(a, b)
             return chunk
 
-        for ks in (far_first[:1], far_first[1:] + [0]):
+        for ks in (far_first[:1], far_first[1:], [0]):
             chunks = [chunk_of(columns[k]) for k in ks]
             for k, chunk in zip(ks, chunks):
                 a_send[columns[k]] = chunk.astype(BF16)

time: 30 us -> 29.9 us (level)
  no operation moved by 1% of the time
where the time goes in v16:
time: 29.9 us; the launch traced here: 29.8 us
  Pallas kernels  29.2 us (98%)
  between operations  0.64 us (2%)
    pallas_call x1, Pallas kernels, on_device(): pl.pallas_call(functools.partial(kernel, nz, ny, nx), out_shape=(vm((ch,...  28.4 us
    pallas_call x1, Pallas kernels, on_device(): pl.pallas_call(write_out, out_shape=tuple((jax.ShapeDtypeStruct(a.shape,...  0.77 us

profile of v16, /device:TPU:1, one launch (start us, length us, event | category | flops | bytes accessed | tf_op | source)
XLA Modules:
  0.0 29.8 jit_solution(737571200039632582)
XLA Ops:
  0.6 28.4 %shard_map.93 = (bf16[192,128]{1,0:T(8,128)(2,1)S(1)}, bf16[192,128]{1,0:T(8,128)(2,1)S(1)}, bf16[64,2048]{1,0:T(8,128)(2,1)S(1)}, f32[16,192]{1,0:T(8,128)S(1)}) custom-call(bf16[128,2048]{1,0:T(8,128)(2,1)} %x_hbm.1, bf16[192,2048]{1,0:T(8,128)(2,1)} %bitcast.7, bf16[192,128]{1,0:T(8,128)(2,1)} %bitcast.8, bf16[192,128]{1,0:T(8,128)(2,1)} %bitcast.9, ...), custom_call_target="tpu_custom_call" | custom-call | tf_op jit(solution)/shard_map/pallas_call | solution.py:671
  29.0 0.8 %shard_map.94 = (bf16[192,128]{1,0:T(8,128)(2,1)}, bf16[192,128]{1,0:T(8,128)(2,1)}, bf16[64,2048]{1,0:T(8,128)(2,1)}, f32[16,192]{1,0:T(8,128)}) custom-call(bf16[192,128]{1,0:T(8,128)(2,1)S(1)} %get-tuple-element.12.refs_0_, bf16[192,128]{1,0:T(8,128)(2,1)S(1)} %get-tuple-element.13.refs_1_, bf16[64,2048]{1,0:T(8,128)(2,1)S(1)} %get-tuple-element.14.refs_2_, ...), custom_call_target="tpu_custom_call" | custom-call | tf_op jit(solution)/shard_map/pallas_call | solution.py:684

commit v17 on v15

--- a/solution.py
+++ b/solution.py
@@ -107,6 +107,12 @@
         def _():
             for ty, tx in others:
                 greet((z, ty, tx, 1))
+
+        for d in z_steps:
+            greet((zs[d], y, x, 1))
+
+        @pl.when(c == 1)
+        def _():
             for ty, tx in everyone:
                 greet((z, ty, tx, 0))
 
@@ -114,9 +120,6 @@
         def _():
             for tx in xs[1:]:
                 greet((z, y, tx, 0))
-
-        for d in z_steps:
-            greet((zs[d], y, x, 1))
 
     lane = lax.broadcasted_iota(jnp.int32, (1, ch), 1)
     mf = [jnp.where((lane >= HEAD * h) & (lane < HEAD * (h + 1)), 1.0, 0.0).astype(F32) for h in range(heads)]

time: 30 us -> 30.1 us (level)
  no operation moved by 1% of the time
where the time goes in v17:
time: 30.1 us; the launch traced here: 30 us
  Pallas kernels  29.3 us (97%)
  between operations  0.64 us (2%)
    pallas_call x1, Pallas kernels, on_device(): pl.pallas_call(functools.partial(kernel, nz, ny, nx), out_shape=(vm((ch,...  28.6 us
    pallas_call x1, Pallas kernels, on_device(): pl.pallas_call(write_out, out_shape=tuple((jax.ShapeDtypeStruct(a.shape,...  0.77 us

profile of v17, /device:TPU:1, one launch (start us, length us, event | category | flops | bytes accessed | tf_op | source)
XLA Modules:
  0.0 30.0 jit_solution(14995893823539507069)
XLA Ops:
  0.6 28.6 %shard_map.93 = (bf16[192,128]{1,0:T(8,128)(2,1)S(1)}, bf16[192,128]{1,0:T(8,128)(2,1)S(1)}, bf16[64,2048]{1,0:T(8,128)(2,1)S(1)}, f32[16,192]{1,0:T(8,128)S(1)}) custom-call(bf16[128,2048]{1,0:T(8,128)(2,1)} %x_hbm.1, bf16[192,2048]{1,0:T(8,128)(2,1)} %bitcast.7, bf16[192,128]{1,0:T(8,128)(2,1)} %bitcast.8, bf16[192,128]{1,0:T(8,128)(2,1)} %bitcast.9, ...), custom_call_target="tpu_custom_call" | custom-call | tf_op jit(solution)/shard_map/pallas_call | solution.py:674
  29.2 0.8 %shard_map.94 = (bf16[192,128]{1,0:T(8,128)(2,1)}, bf16[192,128]{1,0:T(8,128)(2,1)}, bf16[64,2048]{1,0:T(8,128)(2,1)}, f32[16,192]{1,0:T(8,128)}) custom-call(bf16[192,128]{1,0:T(8,128)(2,1)S(1)} %get-tuple-element.12.refs_0_, bf16[192,128]{1,0:T(8,128)(2,1)S(1)} %get-tuple-element.13.refs_1_, bf16[64,2048]{1,0:T(8,128)(2,1)S(1)} %get-tuple-element.14.refs_2_, ...), custom_call_target="tpu_custom_call" | custom-call | tf_op jit(solution)/shard_map/pallas_call | solution.py:687

commit v18 on v15

--- a/solution.py
+++ b/solution.py
@@ -327,7 +327,7 @@
 
             @pl.when(back == 1)
             def _():
-                for target in targets:
+                for target in targets[pln:] + targets[:pln]:
                     carry_send(*target).start()
                 q_grad[me // 2] = lg_send[x]
 

time: 30 us -> 29.9 us (level)
  Pallas kernels: 29.3 us -> 29 us
where the time goes in v18:
time: 29.9 us; the launch traced here: 29.7 us
  Pallas kernels  29 us (97%)
  between operations  0.64 us (2%)
    pallas_call x1, Pallas kernels, on_device(): pl.pallas_call(functools.partial(kernel, nz, ny, nx), out_shape=(vm((ch,...  28.2 us
    pallas_call x1, Pallas kernels, on_device(): pl.pallas_call(write_out, out_shape=tuple((jax.ShapeDtypeStruct(a.shape,...  0.77 us

profile of v18, /device:TPU:1, one launch (start us, length us, event | category | flops | bytes accessed | tf_op | source)
XLA Modules:
  0.0 29.7 jit_solution(17591115137937273885)
XLA Ops:
  0.6 28.2 %shard_map.93 = (bf16[192,128]{1,0:T(8,128)(2,1)S(1)}, bf16[192,128]{1,0:T(8,128)(2,1)S(1)}, bf16[64,2048]{1,0:T(8,128)(2,1)S(1)}, f32[16,192]{1,0:T(8,128)S(1)}) custom-call(bf16[128,2048]{1,0:T(8,128)(2,1)} %x_hbm.1, bf16[192,2048]{1,0:T(8,128)(2,1)} %bitcast.7, bf16[192,128]{1,0:T(8,128)(2,1)} %bitcast.8, bf16[192,128]{1,0:T(8,128)(2,1)} %bitcast.9, ...), custom_call_target="tpu_custom_call" | custom-call | tf_op jit(solution)/shard_map/pallas_call | solution.py:671
  28.9 0.8 %shard_map.94 = (bf16[192,128]{1,0:T(8,128)(2,1)}, bf16[192,128]{1,0:T(8,128)(2,1)}, bf16[64,2048]{1,0:T(8,128)(2,1)}, f32[16,192]{1,0:T(8,128)}) custom-call(bf16[192,128]{1,0:T(8,128)(2,1)S(1)} %get-tuple-element.12.refs_0_, bf16[192,128]{1,0:T(8,128)(2,1)S(1)} %get-tuple-element.13.refs_1_, bf16[64,2048]{1,0:T(8,128)(2,1)S(1)} %get-tuple-element.14.refs_2_, ...), custom_call_target="tpu_custom_call" | custom-call | tf_op jit(solution)/shard_map/pallas_call | solution.py:684
